TPU v7x, 512 devices: a whole 4x8x8 slice. The times are simulated.
512 devices in a mesh: sp: 32 (over z, x), tp: 16 (over y, core).
Axes of the slice: x: 4, y: 8, z: 8, core: 2. Of those that a mesh axis runs over, the one named last changes fastest.
Arguments:
- resid: bfloat16 [4096, 2048], P('sp'), may hold values from -6 to 6
- norm_gain: float32 [2048], replicated, may hold values from 0.1 to 1.9
- cotangent: bfloat16 [4096, 2048], P('sp'), may hold values from -6 to 6
- route_ids: int32 [4096, 2], P('sp'), may hold values from 0 to 31, all different within a row; in each aligned block of 128 rows (0 to 127, 128 to 255, ...) at most 12 rows name the same one
- route_weight: float32 [4096, 2], P('sp'), may hold values from 0.25 to 2.25
- expert_gate: bfloat16 [32, 2048, 2048], P('sp', None, 'tp'), may hold values from -0.125 to 0.125
- expert_up: bfloat16 [32, 2048, 2048], P('sp', None, 'tp'), may hold values from -0.125 to 0.125
- expert_down: bfloat16 [32, 2048, 2048], P('sp', 'tp'), may hold values from -0.125 to 0.125
- out_proj: bfloat16 [2048, 4096], P('sp', 'tp'), may hold values from -0.09375 to 0.09375
- mixed: bfloat16 [4096, 4096], P('sp', 'tp'), may hold values from -6 to 6
- query: bfloat16 [4096, 2048], P('sp', 'tp'), may hold values from -6 to 6
- key: bfloat16 [4096, 2048], P('sp', 'tp'), may hold values from -1.5 to 1.5
- value: bfloat16 [4096, 4096], P('sp', 'tp'), may hold values from -6 to 6
- log_decay: float32 [4096, 2048], P('sp', 'tp'), may hold values from -1 to 0, as said below
- span_state: float32 [32, 16, 128, 256], P('sp', 'tp'), may hold values from -24 to 24
Outputs:
- grad_expert_gate: bfloat16 [32, 2048, 2048], P('sp', None, 'tp')
- grad_expert_up: bfloat16 [32, 2048, 2048], P('sp', None, 'tp')
- grad_expert_down: bfloat16 [32, 2048, 2048], P('sp', 'tp')
- grad_out_proj: float32 [2048, 4096], P('sp', 'tp')
- grad_query: bfloat16 [4096, 2048], P('sp', 'tp')
- grad_key: bfloat16 [4096, 2048], P('sp', 'tp')
- grad_value: bfloat16 [4096, 4096], P('sp', 'tp')
- grad_log_decay: float32 [4096, 2048], P('sp', 'tp')
Inputs may be any that keep to these rules, and one draw needn't show every extreme that they name: `route_ids`: A row names 2 different experts. Within each aligned block of 128 rows (the rows of one index of sp) no expert is named by more than 12 rows, and in every draw some expert is named by exactly 12 rows of some block. `log_decay`: every entry is zero or negative.
All inputs are finite; a program needn't handle non-finite values.
Results may differ from a plain program's by a relative error of at most 0.023.
Values may be sent and summed in bfloat16 or wider, within the bound.
No kernel may reach another device: no remote copies, remote signals or barrier semaphores. Data moves between devices by JAX's collectives and lax.ppermute only.
A program may use at most 64 MiB of HBM per device.

v0:
```python
import jax
import jax.numpy as jnp
from jax import lax
from jax.sharding import Mesh
from jax.sharding import PartitionSpec as P

KEY_CHANNELS = 128
DV = 256
TOP = 2
BLOCK = 64
SP = ("sp_0", "sp_1")


epsilon = 1e-06


def sent_together(arrays, axis, split_dim, concat_dim, along):
    widths = [a.shape[along] for a in arrays]
    both = jnp.concatenate(arrays, axis=along)
    filled = lax.all_to_all(both, axis, split_axis=split_dim, concat_axis=concat_dim, tiled=True)
    return tuple(jnp.split(filled, [sum(widths[:k]) for k in range(1, len(widths))], axis=along))


def sent_together_2(arrays, axis, dim, along):
    widths = [a.shape[along] for a in arrays]
    both = jnp.concatenate(arrays, axis=along)
    filled = lax.all_gather(both, axis, axis=dim, tiled=True)
    return tuple(jnp.split(filled, [sum(widths[:k]) for k in range(1, len(widths))], axis=along))


def in_blocks(array, dim, devices):
    before, after = (array.shape[:dim], array.shape[dim + 1 :])
    return jnp.moveaxis(array.reshape(*before, devices, -1, *after), dim, 0)


def sum_at_owner(array, axis, dim):
    devices = lax.axis_size(axis)
    tiles = lax.all_to_all(in_blocks(array, dim, devices), axis, 0, 0, tiled=True)
    return jnp.sum(tiles.astype(jnp.float32), axis=0)


def whole_of(array, axes, dim):
    filled = array
    for number in range(len(axes) - 1, -1, -1):
        filled = lax.all_gather(filled, axes[number], axis=dim, tiled=True)
    return filled


def filled_with(array, identity):
    return jax.tree.map(
        lambda a, e: jnp.broadcast_to(jnp.asarray(e, a.dtype), a.shape), array, identity
    )


def prefix_by_axis(array, axes, combine, identity):
    before = start = filled_with(array, identity)
    running = array
    for axis in reversed(axes):
        devices, place = (lax.axis_size(axis), lax.axis_index(axis))
        pieces = jax.tree.map(
            lambda part, kind: lax.all_gather(part.astype(kind), axis),
            running,
            (jnp.bfloat16, jnp.bfloat16),
        )
        inside, running = (start, start)
        for k in reversed(range(devices)):
            passed = k > place
            running = combine(
                running, jax.tree.map(lambda part, own: part[k].astype(own.dtype), pieces, array)
            )
            inside = jax.tree.map(lambda new, old: jnp.where(passed, new, old), running, inside)
        before = combine(inside, before)
    return before


def into_blocks(values):
    return values.reshape(values.shape[0] // BLOCK, BLOCK, values.shape[1])


def span_forward(query_rows, key_rows, value_rows, grad_rows, decay_rows, entry_state):
    query_blk = into_blocks(query_rows)
    key_blk = into_blocks(key_rows)
    value_blk = into_blocks(value_rows)
    grad_blk = into_blocks(grad_rows)
    cumlog = jnp.cumsum(into_blocks(decay_rows), axis=1)
    block_total = cumlog[:, -1, :]
    to_end = jnp.exp(block_total[:, None, :] - cumlog)
    inner_part = jnp.einsum("nsd,nsj->ndj", key_blk * to_end, value_blk)

    def forward_step(carry_state, step_item):
        piece_part, block_sum = step_item
        return (jnp.exp(block_sum)[:, None] * carry_state + piece_part, carry_state)

    end_state, starts = lax.scan(forward_step, entry_state, (inner_part, block_total))
    own_part = jnp.einsum("ntd,ntj->ndj", query_blk * jnp.exp(cumlog), grad_blk)

    def backward_step(carry_state, step_item):
        piece_part, block_sum = step_item
        return (jnp.exp(block_sum)[:, None] * carry_state + piece_part, carry_state)

    start_cot, after_cot = lax.scan(
        backward_step, jnp.zeros_like(entry_state), (own_part, block_total), reverse=True
    )
    span_total = jnp.sum(block_total, axis=0)
    later_log = span_total[None, :] - jnp.cumsum(block_total, axis=0)
    return ((cumlog, starts, after_cot, later_log, end_state), (jnp.exp(span_total), start_cot))


def span_backward(query_rows, key_rows, value_rows, grad_rows, kept_terms, exit_cot):
    cumlog, starts, after_cot, later_log, end_state = kept_terms
    query_blk = into_blocks(query_rows)
    key_blk = into_blocks(key_rows)
    value_blk = into_blocks(value_rows)
    grad_blk = into_blocks(grad_rows)
    exit_cots = after_cot + jnp.exp(later_log)[:, :, None] * exit_cot
    causal = jnp.arange(BLOCK)[:, None] >= jnp.arange(BLOCK)[None, :]
    decays = jnp.exp(
        jnp.where(causal[None, :, :, None], cumlog[:, :, None, :] - cumlog[:, None, :, :], -jnp.inf)
    )
    scores = jnp.einsum("ntd,nsd,ntsd->nts", query_blk, key_blk, decays)
    grad_scores = jnp.einsum("ntj,nsj->nts", grad_blk, value_blk)
    grad_query = jnp.exp(cumlog) * jnp.einsum("ntj,ndj->ntd", grad_blk, starts)
    grad_query = grad_query + jnp.einsum("nts,nsd,ntsd->ntd", grad_scores, key_blk, decays)
    to_end = jnp.exp(cumlog[:, -1:, :] - cumlog)
    grad_key = jnp.einsum("nts,ntd,ntsd->nsd", grad_scores, query_blk, decays)
    grad_key = grad_key + to_end * jnp.einsum("nsj,ndj->nsd", value_blk, exit_cots)
    grad_value = jnp.einsum("nts,ntj->nsj", scores, grad_blk)
    grad_value = grad_value + jnp.einsum("nsd,ndj->nsj", key_blk * to_end, exit_cots)
    length = query_rows.shape[0]
    key_width = query_rows.shape[1]
    per_position = (query_blk * grad_query - key_blk * grad_key).reshape(length, key_width)
    grad_log = (
        jnp.flip(jnp.cumsum(jnp.flip(per_position, 0), 0), 0)
        + jnp.sum(end_state * exit_cot, axis=1)[None, :]
    )
    return (
        grad_query.reshape(length, key_width),
        grad_key.reshape(length, key_width),
        grad_value.reshape(length, value_rows.shape[1]),
        grad_log,
    )


def join_later(earlier, later):
    return (earlier[0] * later[0], later[1] + later[0][..., None] * earlier[1])


def on_device(
    resid,
    norm_gain,
    cotangent,
    route_ids,
    route_weight,
    expert_gate,
    expert_up,
    expert_down,
    out_proj,
    mixed,
    query,
    key,
    value,
    log_decay,
    span_state,
):
    tokens_here = resid.shape[0]
    model_width = resid.shape[1]
    sp_count = lax.axis_size(SP)
    tp_count = lax.axis_size("tp")
    experts = sp_count * expert_gate.shape[0]
    capacity = 3 * tokens_here // experts
    resid_f = resid.astype(jnp.float32)
    inverse_rms = lax.rsqrt(jnp.mean(resid_f * resid_f, axis=1, keepdims=True) + epsilon)
    unit_rows = resid_f * inverse_rms
    normed = (unit_rows * norm_gain).astype(jnp.bfloat16)
    pair_expert = route_ids.reshape(-1)
    onehot = (pair_expert[:, None] == jnp.arange(experts, dtype=jnp.int32)[None, :]).astype(
        jnp.int32
    )
    slot_rank = jnp.sum((jnp.cumsum(onehot, axis=0) - onehot) * onehot, axis=1)
    slot_of = pair_expert * capacity + slot_rank
    slot_pairs = slot_of[None, :] == jnp.arange(experts * capacity, dtype=jnp.int32)[:, None]
    slot_tokens = jnp.any(slot_pairs.reshape(experts * capacity, tokens_here, TOP), axis=2).astype(
        jnp.bfloat16
    )
    slot_weight = jnp.sum(jnp.where(slot_pairs, route_weight.reshape(1, -1), 0.0), axis=1)
    column_share = model_width // tp_count
    offset = lax.axis_index("tp") * column_share
    rows_in = jnp.dot(
        slot_tokens,
        lax.dynamic_slice_in_dim(normed, offset, column_share, 1),
        preferred_element_type=jnp.float32,
    ).astype(jnp.bfloat16)
    rows_cot = (
        jnp.dot(
            slot_tokens,
            lax.dynamic_slice_in_dim(cotangent, offset, column_share, 1),
            preferred_element_type=jnp.float32,
        )
        * slot_weight[:, None]
    )
    arrived = sent_together(
        (
            rows_in.reshape(experts, capacity, -1),
            rows_cot.astype(jnp.bfloat16).reshape(experts, capacity, -1),
        ),
        SP,
        0,
        1,
        2,
    )
    expert_in, expert_cot = sent_together_2((arrived[0], arrived[1]), "tp", 2, 0)
    gate_pre = jnp.einsum(
        "erd,edf->erf", expert_in, expert_gate, preferred_element_type=jnp.float32
    )
    up_pre = jnp.einsum("erd,edf->erf", expert_in, expert_up, preferred_element_type=jnp.float32)
    gate_sig = jax.nn.sigmoid(gate_pre)
    hidden = (gate_pre * gate_sig * up_pre).astype(jnp.bfloat16)
    grad_hidden = jnp.einsum(
        "erd,efd->erf", expert_cot, expert_down, preferred_element_type=jnp.float32
    )
    grad_up_act = (grad_hidden * gate_pre * gate_sig).astype(jnp.bfloat16)
    grad_gate_act = (grad_hidden * up_pre * gate_sig * (1.0 + gate_pre * (1.0 - gate_sig))).astype(
        jnp.bfloat16
    )
    grad_down_w = jnp.einsum("erf,erd->efd", hidden, expert_cot, preferred_element_type=jnp.float32)
    grad_gate_w = jnp.einsum(
        "erd,erf->edf", expert_in, grad_gate_act, preferred_element_type=jnp.float32
    )
    grad_up_w = jnp.einsum(
        "erd,erf->edf", expert_in, grad_up_act, preferred_element_type=jnp.float32
    )
    partial_value = jnp.einsum(
        "erf,edf->erd", grad_gate_act, expert_gate, preferred_element_type=jnp.float32
    )
    partial_value = partial_value + jnp.einsum(
        "erf,edf->erd", grad_up_act, expert_up, preferred_element_type=jnp.float32
    )
    partial_short = partial_value.astype(jnp.bfloat16)
    summed = sum_at_owner(partial_short, "tp", 2).astype(jnp.bfloat16)
    returned = lax.all_to_all(summed, SP, split_axis=1, concat_axis=0, tiled=True)
    flat_rows = returned.reshape(experts * capacity, -1)
    grad_normed = lax.all_gather(
        lax.dot_general(
            slot_tokens, flat_rows, (((0,), (0,)), ((), ())), preferred_element_type=jnp.float32
        ).astype(jnp.bfloat16),
        "tp",
        axis=1,
        tiled=True,
    ).astype(jnp.float32)
    scaled = grad_normed * norm_gain
    grad_resid = cotangent.astype(jnp.float32) + inverse_rms * (
        scaled - unit_rows * jnp.mean(scaled * unit_rows, axis=1, keepdims=True)
    )
    grad_resid = grad_resid.astype(jnp.bfloat16)
    resid_cols = grad_resid
    grad_out_proj = sum_at_owner(
        lax.dot_general(
            resid_cols, mixed, (((0,), (0,)), ((), ())), preferred_element_type=jnp.float32
        ).astype(jnp.bfloat16),
        SP,
        0,
    )
    resid_cols = grad_resid
    grad_mixed = jnp.dot(
        resid_cols, whole_of(out_proj, SP, 0), preferred_element_type=jnp.float32
    ).astype(jnp.bfloat16)
    head_count = query.shape[1] // KEY_CHANNELS
    query_scale = KEY_CHANNELS ** (-0.5)

    def heads_first(values, head_depth):
        return values.reshape(tokens_here, head_count, head_depth).transpose(1, 0, 2)

    query_rows = heads_first(query, KEY_CHANNELS).astype(jnp.float32) * query_scale
    key_rows = heads_first(key, KEY_CHANNELS).astype(jnp.float32)
    value_rows = heads_first(value, DV).astype(jnp.float32)
    grad_rows = heads_first(grad_mixed, DV).astype(jnp.float32)
    decay_rows = heads_first(log_decay, KEY_CHANNELS)
    kept_terms, summary = jax.vmap(span_forward)(
        query_rows, key_rows, value_rows, grad_rows, decay_rows, span_state[0]
    )
    identity = (jnp.ones_like(summary[0]), jnp.zeros_like(summary[1]))
    carried = prefix_by_axis((summary[0], summary[1]), SP, join_later, identity)
    head_grads = jax.vmap(span_backward)(
        query_rows, key_rows, value_rows, grad_rows, kept_terms, carried[1]
    )

    def tokens_first(values):
        return values.transpose(1, 0, 2).reshape(tokens_here, -1)

    grad_query = (tokens_first(head_grads[0]) * query_scale).astype(jnp.bfloat16)
    grad_key = tokens_first(head_grads[1]).astype(jnp.bfloat16)
    grad_value = tokens_first(head_grads[2]).astype(jnp.bfloat16)
    grad_log_decay = tokens_first(head_grads[3])
    return (
        grad_gate_w.astype(jnp.bfloat16),
        grad_up_w.astype(jnp.bfloat16),
        grad_down_w.astype(jnp.bfloat16),
        grad_out_proj,
        grad_query,
        grad_key,
        grad_value,
        grad_log_decay,
    )


def solution(mesh):
    finer = Mesh(mesh.devices.reshape(8, 4, mesh.shape["tp"]), ("sp_0", "sp_1", "tp"))
    in_specs = (
        P(SP, None),
        P(),
        P(SP, None),
        P(SP, None),
        P(SP, None),
        P(SP, None, "tp"),
        P(SP, None, "tp"),
        P(SP, "tp", None),
        P(SP, "tp"),
        P(SP, "tp"),
        P(SP, "tp"),
        P(SP, "tp"),
        P(SP, "tp"),
        P(SP, "tp"),
        P(SP, "tp", None, None),
    )
    out_specs = (
        P(SP, None, "tp"),
        P(SP, None, "tp"),
        P(SP, "tp", None),
        P(SP, "tp"),
        P(SP, "tp"),
        P(SP, "tp"),
        P(SP, "tp"),
        P(SP, "tp"),
    )
    return jax.shard_map(
        on_device, mesh=finer, in_specs=in_specs, out_specs=out_specs, check_vma=False
    )
```

profile of v0, /device:TPU:2, one launch (start us, length us, event | category | flops | bytes accessed | tf_op | source)
XLA Modules:
  0.0 247.1 jit_solution(6670565938437105491)
XLA Ops:
  7.2 0.8 copy.119
  8.4 0.6 reduce-window.6
  9.0 0.2 slice_reduce_fusion
  9.5 0.7 multiply_add_fusion.1
  10.3 0.8 copy.123
  11.4 0.9 fusion.12
  12.3 1.2 fusion.17
  13.6 1.2 convert_multiply_fusion
  14.9 0.2 convolution_convert_fusion.4
  15.1 24.5 %all_to_all.31 = bf16[32,12,256]{2,1,0:T(8,128)(2,1)S(1)} all-to-all(bf16[32,12,256]{2,1,0:T(8,128)(2,1)S(1)} %pad_maximum_fusion), channel_id=1, replica_groups=mesh['sp_0'=8,'sp_1'=4,'tp'=16] {'sp_0','sp_1'}, dimensions={0} | all-to-all | bytes 393216 | tf_op jit(solution)/shard_map/all_to_all | solution.py:20
  39.7 0.7 pad_maximum_fusion.1
  40.5 13.0 %all_gather.32 = bf16[256,256]{1,0:T(8,128)(2,1)} all-gather(bf16[64,256]{1,0:T(8,128)(2,1)S(1)} %copy-done.18), channel_id=1, replica_groups=mesh['sp_0'=8,'sp_1'=4,'tp'=16] {'sp_1'}, dimensions={0}, use_global_device_ids=true | all-gather | bytes 163840 | tf_op jit(solution)/shard_map/all_gather | solution.py:45
  53.6 0.6 slice_reduce_fusion.1
  54.2 8.7 %all-gather.2 = bf16[4,1,128]{2,1,0:T(2,128)(2,1)S(1)} all-gather(bf16[1,1,128]{2,1,0:T(2,128)(2,1)S(1)} %convert_bitcast_fusion.14), channel_id=3, replica_groups=mesh['sp_0'=8,'sp_1'=4,'tp'=16] {'sp_1'}, dimensions={0}, use_global_device_ids=true | all-gather | bytes 1280 | tf_op jit(solution)/shard_map/all_gather | solution.py:61
  62.9 0.6 fusion.111
  63.5 0.6 broadcast_multiply_fusion
  64.1 14.5 %all_gather.38 = bf16[8,1,128]{2,1,0:T(2,128)(2,1)S(1)} all-gather(bf16[1,1,128]{2,1,0:T(2,128)(2,1)S(1)} %get-tuple-element.285), channel_id=1, replica_groups=mesh['sp_0'=8,'sp_1'=4,'tp'=16] {'sp_0'}, dimensions={0}, use_global_device_ids=true | all-gather | bytes 2304 | tf_op jit(solution)/shard_map/all_gather | solution.py:61
  78.5 0.6 fusion.100
  79.1 5.1 %all-gather.6.cloned.1.call-done = bf16[2,384,2048]{2,1,0:T(8,128)(2,1)} async-done(((bf16[2,384,128]{2,1,0:T(8,128)(2,1)}), bf16[2,384,2048]{2,1,0:T(8,128)(2,1)}) %all-gather.6.cloned.1.call-update) | async-done | bytes 3145744 | tf_op jit(solution)/shard_map/all_gather | solution.py:27
  84.2 2.1 fusion.18
  86.4 2.0 fusion.19
  88.5 0.6 multiply_convert_fusion.1
  89.1 0.6 fusion.20
  89.7 0.6 fusion.10
  90.3 0.4 copy.152
  90.7 1.6 copy.161
  92.4 5.0 %all-to-all-start.1 = ((bf16[16,1,384,128]{3,2,1,0:T(8,128)(2,1)}), bf16[16,1,384,128]{3,2,1,0:T(8,128)(2,1)S(1)}, u32[]{:S(2)}, u32[]{:S(2)}) async-start(bf16[16,1,384,128]{3,2,1,0:T(8,128)(2,1)} %bitcast.405), calls=%async_computation.1 | async-start | bytes 3145728 | tf_op jit(solution)/shard_map/all_to_all | solution.py:38
  97.4 0.2 convolution_bitcast_fusion.1
  97.7 0.6 fusion.107
  98.3 4.4 %fusion.4 = (bf16[2,64,64]{2,1,0:T(8,128)(2,1)}, f32[2,64,128,64]{2,3,1,0:T(8,128)}) fusion(f32[2,128,64]{1,2,0:T(8,128)S(1)} %get-tuple-element.274, f32[2,128,64]{1,2,0:T(8,128)S(1)} %bitcast.415, f32[2,64,128]{2,1,0:T(8,128)S(1)} %bitcast.407, pred[64,64]{1,0:T(8,128)(4,1)S(1)} %iota_compare_fusion.2), kind=kLoop, calls=%fused_computation.11 | loop fusion | flops 5234688 | bytes 4411392 | tf_op jit(solution)/shard_map/vmap(ntd,nsd,ntsd->nts)/dot_general | solution.py:120
  102.7 0.3 while.29
  103.0 2.8 %fusion.7 = bf16[1,2048,128]{2,1,0:T(8,128)(2,1)} fusion(bf16[384,128]{1,0:T(8,128)(2,1)S(1)} %get-tuple-element.263, bf16[2,384,2048]{2,1,0:T(8,128)(2,1)} %all-gather.6.cloned.1.call-done), kind=kOutput, calls=%fused_computation.22 | convolution fusion | flops 201588736 | bytes 2195456 | tf_op jit(solution)/shard_map/erd,erf->edf/dot_general | solution.py:226
  105.8 2.8 %fusion.9 = bf16[1,128,2048]{2,1,0:T(8,128)(2,1)} fusion(bf16[2,384,2048]{2,1,0:T(8,128)(2,1)} %all-gather.6.cloned.1.call-done, f32[384,128]{1,0:T(8,128)} %copy-done.10, f32[384,128]{1,0:T(8,128)S(1)} %copy-done.9), kind=kOutput, calls=%fused_computation.24 | convolution fusion | flops 201883648 | bytes 2490368 | tf_op jit(solution)/shard_map/erf,erd->efd/dot_general | solution.py:225
  108.7 26.5 %all-to-all-done.1 = bf16[16,1,384,128]{3,2,1,0:T(8,128)(2,1)S(1)} async-done(((bf16[16,1,384,128]{3,2,1,0:T(8,128)(2,1)}), bf16[16,1,384,128]{3,2,1,0:T(8,128)(2,1)S(1)}, u32[]{:S(2)}, u32[]{:S(2)}) %all-to-all-start.1) | async-done | bytes 1572896 | tf_op jit(solution)/shard_map/all_to_all | solution.py:38
  135.2 0.2 reduce_sum.83
  135.4 0.2 copy.162
  135.6 0.5 broadcast.602
  136.1 1.2 reduce.13
  137.3 0.7 reshape.1332
  138.0 10.5 %all-to-all-start.2 = ((bf16[32,2,768]{2,1,0:T(2,128)(2,1)}), bf16[32,2,768]{2,1,0:T(2,128)(2,1)S(1)}, u32[]{:S(2)}, u32[]{:S(2)}) async-start(bf16[32,2,768]{2,1,0:T(2,128)(2,1)} %reshape.1332), calls=%async_computation.2 | async-start | bytes 196608 | tf_op jit(solution)/shard_map/all_to_all | solution.py:240
  148.5 2.8 %fusion.8 = bf16[1,2048,128]{2,1,0:T(8,128)(2,1)} fusion(bf16[384,128]{1,0:T(8,128)(2,1)} %copy-done.14, bf16[2,384,2048]{2,1,0:T(8,128)(2,1)} %all-gather.6.cloned.1.call-done), kind=kOutput, calls=%fused_computation.23 | convolution fusion | flops 201588736 | bytes 2195456 | tf_op jit(solution)/shard_map/erd,erf->edf/dot_general | solution.py:229
  151.4 6.2 %all-to-all-done.2 = bf16[32,2,768]{2,1,0:T(2,128)(2,1)S(1)} async-done(((bf16[32,2,768]{2,1,0:T(2,128)(2,1)}), bf16[32,2,768]{2,1,0:T(2,128)(2,1)S(1)}, u32[]{:S(2)}, u32[]{:S(2)}) %all-to-all-start.2) | async-done | bytes 98336 | tf_op jit(solution)/shard_map/all_to_all | solution.py:240
  157.6 0.2 convolution_convert_fusion.6
  157.9 16.9 %all_gather.31 = bf16[128,2048]{1,0:T(8,128)(2,1)S(1)} all-gather(bf16[128,128]{1,0:T(8,128)(2,1)S(1)} %convolution_convert_fusion.6), channel_id=1, replica_groups=mesh['sp_0'=8,'sp_1'=4,'tp'=16] {'tp'}, dimensions={1}, use_global_device_ids=true | all-gather | bytes 557056 | tf_op jit(solution)/shard_map/all_gather | solution.py:242
  174.7 0.3 multiply_reduce_fusion.1
  175.1 0.4 add_convert_fusion.1
  175.5 1.5 convolution_convert_fusion
  177.0 5.5 %all-to-all-start.3 = ((bf16[32,64,256]{2,1,0:T(8,128)(2,1)}), bf16[32,64,256]{2,1,0:T(8,128)(2,1)S(1)}, u32[]{:S(2)}, u32[]{:S(2)}) async-start(bf16[32,64,256]{2,1,0:T(8,128)(2,1)} %bitcast.409), calls=%async_computation.3 | async-start | bytes 2097152 | tf_op jit(solution)/shard_map/all_to_all | solution.py:38
  182.5 1.5 convolution_convert_fusion.5
  184.1 0.2 convolution_bitcast_fusion
  184.4 0.3 while.30
  184.8 14.4 %all-gather = bf16[4,128,256]{2,1,0:T(8,128)(2,1)S(1)} all-gather(bf16[1,128,256]{2,1,0:T(8,128)(2,1)S(1)} %convert_element_type.545), channel_id=2, replica_groups=mesh['sp_0'=8,'sp_1'=4,'tp'=16] {'sp_1'}, dimensions={0}, use_global_device_ids=true | all-gather | bytes 327680 | tf_op jit(solution)/shard_map/all_gather | solution.py:61
  199.4 28.9 %all_gather.37 = bf16[8,1,128,256]{3,2,1,0:T(8,128)(2,1)S(1)} all-gather(bf16[1,1,128,256]{3,2,1,0:T(8,128)(2,1)S(1)} %fusion.78), channel_id=1, replica_groups=mesh['sp_0'=8,'sp_1'=4,'tp'=16] {'sp_0'}, dimensions={0}, use_global_device_ids=true | all-gather | bytes 589824 | tf_op jit(solution)/shard_map/all_gather | solution.py:61
  228.3 0.3 fusion.48
  228.9 4.9 %fusion.5 = f32[2,64,128]{2,1,0:T(8,128)S(1)} fusion(f32[2,64,128,64]{2,3,1,0:T(8,128)} %get-tuple-element.267, f32[2,64,128]{2,1,0:T(8,128)S(1)} %get-tuple-element.275, f32[2,64,64]{2,1,0:T(8,128)S(1)} %copy.128), kind=kLoop, calls=%fused_computation.13 | loop fusion | flops 3129344 | bytes 4358144 | tf_op jit(solution)/shard_map/vmap(nts,nsd,ntsd->ntd)/dot_general | solution.py:123
  234.0 0.2 fusion.16
  234.1 2.0 multiply_reduce_fusion
  236.1 0.9 multiply_subtract_fusion
  237.0 0.2 reduce_window_sum.55
  237.3 0.4 fusion.38
  237.7 0.6 add_bitcast_fusion
  238.4 0.2 fusion.28
  238.6 0.8 fusion.13
  239.5 0.8 convert_reduce_fusion
  (155 shorter events, 2.7 us)
Async XLA Ops:
  7.2 77.1 %copy-start = (bf16[1,2048,128]{2,1,0:T(8,128)(2,1)S(1)}, bf16[1,2048,128]{2,1,0:T(8,128)(2,1)}, u32[]{:S(2)}) copy-start(bf16[1,2048,128]{2,1,0:T(8,128)(2,1)} %param.24) | copy-start | bytes 1572868
  7.2 7.6 %copy-start.17 = (f32[2048]{0:T(1024)S(1)}, f32[2048]{0:T(1024)}, u32[]{:S(2)}) copy-start(f32[2048]{0:T(1024)} %param.20) | copy-start | bytes 24580
  7.2 77.0 %all-gather.6.cloned.1.call-start = ((), (), s32[]{:S(2)}) async-start(), calls=%async_computation.4 | async-start | bytes 3342336 | tf_op jit(solution)/shard_map/all_gather | solution.py:27
  7.2 33.2 %copy-start.18 = (bf16[64,256]{1,0:T(8,128)(2,1)S(1)}, bf16[64,256]{1,0:T(8,128)(2,1)}, u32[]{:S(2)}) copy-start(bf16[64,256]{1,0:T(8,128)(2,1)} %param.27) | copy-start | bytes 98308
  9.2 44.3 %copy-start.16 = (f32[128,128]{1,0:T(8,128)S(1)}, f32[128,128]{1,0:T(8,128)}, u32[]{:S(2)}) copy-start(f32[128,128]{1,0:T(8,128)} %param.32) | copy-start | bytes 196612
  13.6 65.5 %copy-start.43 = (f32[128]{0:T(128)}, f32[128]{0:T(128)S(1)}, u32[]{:S(2)}) copy-start(f32[128]{0:T(128)S(1)} %add_rsqrt_fusion) | copy-start | bytes 1540
  14.9 71.5 %copy-start.7 = (bf16[1,2048,128]{2,1,0:T(8,128)(2,1)S(1)}, bf16[1,2048,128]{2,1,0:T(8,128)(2,1)}, u32[]{:S(2)}) copy-start(bf16[1,2048,128]{2,1,0:T(8,128)(2,1)} %param.25) | copy-start | bytes 1572868
  40.4 48.0 %copy-start.49 = (bf16[1,128,2048]{2,1,0:T(8,128)(2,1)S(1)}, bf16[1,128,2048]{2,1,0:T(8,128)(2,1)}, u32[]{:S(2)}) copy-start(bf16[1,128,2048]{2,1,0:T(8,128)(2,1)} %param.26) | copy-start | bytes 1572868
  40.4 142.1 %all-gather.8.cloned.1.call-start = ((), (), s32[]{:S(2)}) async-start(), calls=%async_computation.5 | async-start | bytes 1179648 | tf_op jit(solution)/shard_map/all_gather | solution.py:45
  63.5 164.8 %copy-start.19 = (f32[128]{0:T(128)}, f32[128]{0:T(128)S(1)}, u32[]{:S(2)}) copy-start(f32[128]{0:T(128)S(1)} %get-tuple-element.286) | copy-start | bytes 1540
  84.2 4.2 %copy-start.3 = (bf16[2,384,2048]{2,1,0:T(8,128)(2,1)S(1)}, bf16[2,384,2048]{2,1,0:T(8,128)(2,1)}, u32[]{:S(2)}) copy-start(bf16[2,384,2048]{2,1,0:T(8,128)(2,1)} %all-gather.6.cloned.1.call-done) | copy-start | bytes 9437188
  86.4 2.7 %copy-start.8 = (f32[384,128]{1,0:T(8,128)}, f32[384,128]{1,0:T(8,128)S(1)}, u32[]{:S(2)}) copy-start(f32[384,128]{1,0:T(8,128)S(1)} %fusion.18) | copy-start | bytes 589828
  88.5 1.2 copy-start.10
  89.1 1.2 copy-start.14
  90.7 6.8 %copy-start.4 = (bf16[128,256]{1,0:T(8,128)(2,1)S(1)}, bf16[128,256]{1,0:T(8,128)(2,1)}, u32[]{:S(2)}) copy-start(bf16[128,256]{1,0:T(8,128)(2,1)} %param.31) | copy-start | bytes 196612
  90.7 6.7 %copy-start.6 = (bf16[128,128]{1,0:T(8,128)(2,1)S(1)}, bf16[128,128]{1,0:T(8,128)(2,1)}, u32[]{:S(2)}) copy-start(bf16[128,128]{1,0:T(8,128)(2,1)} %param.30) | copy-start | bytes 98308
  90.7 7.6 %copy-start.12 = (bf16[128,128]{1,0:T(8,128)(2,1)S(1)}, bf16[128,128]{1,0:T(8,128)(2,1)}, u32[]{:S(2)}) copy-start(bf16[128,128]{1,0:T(8,128)(2,1)} %param.29) | copy-start | bytes 98308
  92.4 42.8 %all-to-all-start.1 = ((bf16[16,1,384,128]{3,2,1,0:T(8,128)(2,1)}), bf16[16,1,384,128]{3,2,1,0:T(8,128)(2,1)S(1)}, u32[]{:S(2)}, u32[]{:S(2)}) async-start(bf16[16,1,384,128]{3,2,1,0:T(8,128)(2,1)} %bitcast.405), calls=%async_computation.1 | async-start | bytes 3145728 | tf_op jit(solution)/shard_map/all_to_all | solution.py:38
  97.3 5.4 %copy-start.1 = (f32[1,1,128,256]{3,2,1,0:T(8,128)S(1)}, f32[1,1,128,256]{3,2,1,0:T(8,128)}, u32[]{:S(2)}) copy-start(f32[1,1,128,256]{3,2,1,0:T(8,128)} %param.33) | copy-start | bytes 393220
  97.3 5.4 %copy-start.47 = (f32[2,1,128]{2,1,0:T(1,128)S(1)}, f32[2,1,128]{2,1,0:T(1,128)}, u32[]{:S(2)}) copy-start(f32[2,1,128]{2,1,0:T(1,128)} %get-tuple-element.373) | copy-start | bytes 3076
  102.7 3.1 %copy-start.9 = (f32[384,128]{1,0:T(8,128)S(1)}, f32[384,128]{1,0:T(8,128)}, u32[]{:S(2)}) copy-start(f32[384,128]{1,0:T(8,128)} %copy-done.8) | copy-start | bytes 589828
  108.7 66.1 %copy-start.2 = (bf16[128,2048]{1,0:T(8,128)(2,1)S(1)}, bf16[128,2048]{1,0:T(8,128)(2,1)}, u32[]{:S(2)}) copy-start(bf16[128,2048]{1,0:T(8,128)(2,1)} %param.19) | copy-start | bytes 1572868
  108.7 66.1 %copy-start.44 = (f32[128]{0:T(128)S(1)}, f32[128]{0:T(128)}, u32[]{:S(2)}) copy-start(f32[128]{0:T(128)} %copy-done.43) | copy-start | bytes 1540
  135.4 39.6 %copy-start.5 = (bf16[128,2048]{1,0:T(8,128)(2,1)S(1)}, bf16[128,2048]{1,0:T(8,128)(2,1)}, u32[]{:S(2)}) copy-start(bf16[128,2048]{1,0:T(8,128)(2,1)} %param.21) | copy-start | bytes 1572868
  138.0 19.5 %all-to-all-start.2 = ((bf16[32,2,768]{2,1,0:T(2,128)(2,1)}), bf16[32,2,768]{2,1,0:T(2,128)(2,1)S(1)}, u32[]{:S(2)}, u32[]{:S(2)}) async-start(bf16[32,2,768]{2,1,0:T(2,128)(2,1)} %reshape.1332), calls=%async_computation.2 | async-start | bytes 196608 | tf_op jit(solution)/shard_map/all_to_all | solution.py:240
  148.5 27.0 %copy-start.15 = (bf16[128,256]{1,0:T(8,128)(2,1)S(1)}, bf16[128,256]{1,0:T(8,128)(2,1)}, u32[]{:S(2)}) copy-start(bf16[128,256]{1,0:T(8,128)(2,1)} %param.28) | copy-start | bytes 196612
  175.5 8.9 %copy-start.48 = (f32[2,1,128]{2,1,0:T(1,128)S(1)}, f32[2,1,128]{2,1,0:T(1,128)}, u32[]{:S(2)}) copy-start(f32[2,1,128]{2,1,0:T(1,128)} %get-tuple-element.373) | copy-start | bytes 3076
  177.0 62.5 %all-to-all-start.3 = ((bf16[32,64,256]{2,1,0:T(8,128)(2,1)}), bf16[32,64,256]{2,1,0:T(8,128)(2,1)S(1)}, u32[]{:S(2)}, u32[]{:S(2)}) async-start(bf16[32,64,256]{2,1,0:T(8,128)(2,1)} %bitcast.409), calls=%async_computation.3 | async-start | bytes 2097152 | tf_op jit(solution)/shard_map/all_to_all | solution.py:38
  182.5 16.7 %copy-start.21 = (f32[128]{0:T(128)S(1)}, f32[128]{0:T(128)}, u32[]{:S(2)}) copy-start(f32[128]{0:T(128)} %get-tuple-element.287) | copy-start | bytes 1540
  182.5 16.7 %copy-start.23 = (f32[128]{0:T(128)S(1)}, f32[128]{0:T(128)}, u32[]{:S(2)}) copy-start(f32[128]{0:T(128)} %get-tuple-element.288) | copy-start | bytes 1540
  182.5 16.7 %copy-start.25 = (f32[128]{0:T(128)S(1)}, f32[128]{0:T(128)}, u32[]{:S(2)}) copy-start(f32[128]{0:T(128)} %get-tuple-element.283) | copy-start | bytes 1540
  184.1 44.2 %copy-start.27 = (f32[128]{0:T(128)S(1)}, f32[128]{0:T(128)}, u32[]{:S(2)}) copy-start(f32[128]{0:T(128)} %get-tuple-element.276) | copy-start | bytes 1540
  184.1 44.2 %copy-start.29 = (f32[128]{0:T(128)S(1)}, f32[128]{0:T(128)}, u32[]{:S(2)}) copy-start(f32[128]{0:T(128)} %get-tuple-element.277) | copy-start | bytes 1540
  184.1 44.2 %copy-start.31 = (f32[128]{0:T(128)S(1)}, f32[128]{0:T(128)}, u32[]{:S(2)}) copy-start(f32[128]{0:T(128)} %get-tuple-element.278) | copy-start | bytes 1540
  184.1 44.2 %copy-start.33 = (f32[128]{0:T(128)S(1)}, f32[128]{0:T(128)}, u32[]{:S(2)}) copy-start(f32[128]{0:T(128)} %get-tuple-element.279) | copy-start | bytes 1540
  184.1 44.2 %copy-start.35 = (f32[128]{0:T(128)S(1)}, f32[128]{0:T(128)}, u32[]{:S(2)}) copy-start(f32[128]{0:T(128)} %get-tuple-element.280) | copy-start | bytes 1540
  184.1 44.2 %copy-start.37 = (f32[128]{0:T(128)S(1)}, f32[128]{0:T(128)}, u32[]{:S(2)}) copy-start(f32[128]{0:T(128)} %get-tuple-element.281) | copy-start | bytes 1540
  184.1 44.2 %copy-start.39 = (f32[128]{0:T(128)S(1)}, f32[128]{0:T(128)}, u32[]{:S(2)}) copy-start(f32[128]{0:T(128)} %get-tuple-element.282) | copy-start | bytes 1540
  184.1 44.2 %copy-start.41 = (f32[128]{0:T(128)S(1)}, f32[128]{0:T(128)}, u32[]{:S(2)}) copy-start(f32[128]{0:T(128)} %get-tuple-element.284) | copy-start | bytes 1540
  184.1 44.2 %copy-start.45 = (f32[128]{0:T(128)S(1)}, f32[128]{0:T(128)}, u32[]{:S(2)}) copy-start(f32[128]{0:T(128)} %fusion.100) | copy-start | bytes 1540
  228.9 7.2 %copy-start.13 = (bf16[128,128]{1,0:T(8,128)(2,1)S(1)}, bf16[128,128]{1,0:T(8,128)(2,1)}, u32[]{:S(2)}) copy-start(bf16[128,128]{1,0:T(8,128)(2,1)} %param.29) | copy-start | bytes 98308
  233.8 3.4 %copy-start.20 = (f32[128]{0:T(128)S(1)}, f32[128]{0:T(128)}, u32[]{:S(2)}) copy-start(f32[128]{0:T(128)} %copy-done.19) | copy-start | bytes 1540
  233.8 3.4 %copy-start.22 = (f32[128]{0:T(128)S(1)}, f32[128]{0:T(128)}, u32[]{:S(2)}) copy-start(f32[128]{0:T(128)} %get-tuple-element.287) | copy-start | bytes 1540
  233.9 3.4 %copy-start.24 = (f32[128]{0:T(128)S(1)}, f32[128]{0:T(128)}, u32[]{:S(2)}) copy-start(f32[128]{0:T(128)} %get-tuple-element.288) | copy-start | bytes 1540
  233.9 3.4 %copy-start.26 = (f32[128]{0:T(128)S(1)}, f32[128]{0:T(128)}, u32[]{:S(2)}) copy-start(f32[128]{0:T(128)} %get-tuple-element.283) | copy-start | bytes 1540
  233.9 3.4 %copy-start.28 = (f32[128]{0:T(128)S(1)}, f32[128]{0:T(128)}, u32[]{:S(2)}) copy-start(f32[128]{0:T(128)} %get-tuple-element.276) | copy-start | bytes 1540
  233.9 3.4 %copy-start.30 = (f32[128]{0:T(128)S(1)}, f32[128]{0:T(128)}, u32[]{:S(2)}) copy-start(f32[128]{0:T(128)} %get-tuple-element.277) | copy-start | bytes 1540
  233.9 3.4 %copy-start.32 = (f32[128]{0:T(128)S(1)}, f32[128]{0:T(128)}, u32[]{:S(2)}) copy-start(f32[128]{0:T(128)} %get-tuple-element.278) | copy-start | bytes 1540
  233.9 3.4 %copy-start.34 = (f32[128]{0:T(128)S(1)}, f32[128]{0:T(128)}, u32[]{:S(2)}) copy-start(f32[128]{0:T(128)} %get-tuple-element.279) | copy-start | bytes 1540
  233.9 3.4 %copy-start.36 = (f32[128]{0:T(128)S(1)}, f32[128]{0:T(128)}, u32[]{:S(2)}) copy-start(f32[128]{0:T(128)} %get-tuple-element.280) | copy-start | bytes 1540
  233.9 3.4 %copy-start.38 = (f32[128]{0:T(128)S(1)}, f32[128]{0:T(128)}, u32[]{:S(2)}) copy-start(f32[128]{0:T(128)} %get-tuple-element.281) | copy-start | bytes 1540
  233.9 3.4 %copy-start.40 = (f32[128]{0:T(128)S(1)}, f32[128]{0:T(128)}, u32[]{:S(2)}) copy-start(f32[128]{0:T(128)} %get-tuple-element.282) | copy-start | bytes 1540
  233.9 3.4 %copy-start.42 = (f32[128]{0:T(128)S(1)}, f32[128]{0:T(128)}, u32[]{:S(2)}) copy-start(f32[128]{0:T(128)} %get-tuple-element.284) | copy-start | bytes 1540
  234.0 3.4 %copy-start.46 = (f32[128]{0:T(128)S(1)}, f32[128]{0:T(128)}, u32[]{:S(2)}) copy-start(f32[128]{0:T(128)} %fusion.100) | copy-start | bytes 1540
  234.0 4.7 %copy-start.11 = (bf16[2,64,64]{2,1,0:T(8,128)(2,1)S(1)}, bf16[2,64,64]{2,1,0:T(8,128)(2,1)}, u32[]{:S(2)}) copy-start(bf16[2,64,64]{2,1,0:T(8,128)(2,1)} %get-tuple-element.266) | copy-start | bytes 49156
Sparse Core Ops, SparseCore 0:
  40.5 43.6 all-gather.5
  86.3 41.2 all-gather.7
where the time goes:
time: 248 us; the launch traced here: 247 us
  blocking collectives  121 us (49%)
  waiting for transfers between devices  37.9 us (15%)
  other arithmetic  24.2 us (10%)
  matrix products  21.5 us (9%)
  starting transfers between devices  21 us (8%)
  between operations  15.1 us (6%)
  local copies, waits for them, and re-layouts  6.53 us (3%)
    all_gather x4, blocking collectives, prefix_by_axis(): lax.all_gather(part.astype(kind), axis)  66.5 us
    all_to_all x2, waiting for transfers between devices, sum_at_owner(): lax.all_to_all(in_blocks(array, dim, devices), axis, 0, 0, tiled=True)  26.5 us
    all_to_all x1, blocking collectives, sent_together(): lax.all_to_all(both, axis, split_axis=split_dim, concat_axis=concat_dim,...  24.5 us
    all_gather x1, blocking collectives, on_device(): lax.all_gather(lax.dot_general(slot_tokens, flat_rows, (((0,), (0,)), (()...  16.9 us
    all_gather x1, blocking collectives, whole_of(): filled = lax.all_gather(filled, axes[number], axis=dim, tiled=True)  13 us
    all_to_all x1, starting transfers between devices, on_device(): lax.all_to_all(summed, SP, split_axis=1, concat_axis=0, tiled=True)  10.5 us
    all_to_all x2, starting transfers between devices, sum_at_owner(): lax.all_to_all(in_blocks(array, dim, devices), axis, 0, 0, tiled=True)  10.4 us
    all_to_all x1, waiting for transfers between devices, on_device(): lax.all_to_all(summed, SP, split_axis=1, concat_axis=0, tiled=True)  6.16 us
  transfers between devices with their start and end apart: 5, of which 3 were waited for; matrix products, arithmetic and copies ran while one was open for 17% of the time, Pallas kernels for 0%

commit v1 on v0

v1 whole, which is shorter than its diff:
```python
import jax
import jax.numpy as jnp
from jax import lax
from jax.sharding import Mesh
from jax.sharding import PartitionSpec as P

KEY_CHANNELS = 128
DV = 256
TOP = 2
BLOCK = 64
SP = ("z", "x")
TP = ("y", "c")


epsilon = 1e-06


def sum_parts(tiles):
    return jnp.sum(tiles.astype(jnp.float32), axis=0)


def later_sum(states, decays, place):
    count = states.shape[0]
    total = jnp.zeros(states.shape[1:], jnp.float32)
    factor = jnp.ones(decays.shape[1:], jnp.float32)
    for k in range(count):
        later = k > place
        total = total + jnp.where(later, factor, 0.0)[:, None] * states[k].astype(jnp.float32)
        factor = jnp.where(later, factor * decays[k], factor)
    return total, factor


def to_all(array, axis):
    count = lax.axis_size(axis)
    copies = jnp.broadcast_to(array[None], (count, *array.shape))
    return lax.all_to_all(copies, axis, 0, 0, tiled=True)


def with_decay(state, decay):
    row = jnp.pad(decay[None, :], ((0, 7), (0, DV - KEY_CHANNELS)))
    return jnp.concatenate([state, row], axis=0).astype(jnp.bfloat16)


def split_decay(filled):
    decays = filled[:, KEY_CHANNELS, :KEY_CHANNELS].astype(jnp.float32)
    return filled[:, :KEY_CHANNELS], decays


def into_blocks(values):
    return values.reshape(values.shape[0] // BLOCK, BLOCK, values.shape[1])


def span_forward(query_rows, key_rows, value_rows, grad_rows, decay_rows, entry_state):
    query_blk = into_blocks(query_rows)
    key_blk = into_blocks(key_rows)
    value_blk = into_blocks(value_rows)
    grad_blk = into_blocks(grad_rows)
    cumlog = jnp.cumsum(into_blocks(decay_rows), axis=1)
    block_total = cumlog[:, -1, :]
    to_end = jnp.exp(block_total[:, None, :] - cumlog)
    inner_part = jnp.einsum("nsd,nsj->ndj", key_blk * to_end, value_blk)

    def forward_step(carry_state, step_item):
        piece_part, block_sum = step_item
        return (jnp.exp(block_sum)[:, None] * carry_state + piece_part, carry_state)

    end_state, starts = lax.scan(forward_step, entry_state, (inner_part, block_total))
    own_part = jnp.einsum("ntd,ntj->ndj", query_blk * jnp.exp(cumlog), grad_blk)

    def backward_step(carry_state, step_item):
        piece_part, block_sum = step_item
        return (jnp.exp(block_sum)[:, None] * carry_state + piece_part, carry_state)

    start_cot, after_cot = lax.scan(
        backward_step, jnp.zeros_like(entry_state), (own_part, block_total), reverse=True
    )
    span_total = jnp.sum(block_total, axis=0)
    later_log = span_total[None, :] - jnp.cumsum(block_total, axis=0)
    return ((cumlog, starts, after_cot, later_log, end_state), (jnp.exp(span_total), start_cot))


def span_backward(query_rows, key_rows, value_rows, grad_rows, kept_terms, exit_cot):
    cumlog, starts, after_cot, later_log, end_state = kept_terms
    query_blk = into_blocks(query_rows)
    key_blk = into_blocks(key_rows)
    value_blk = into_blocks(value_rows)
    grad_blk = into_blocks(grad_rows)
    exit_cots = after_cot + jnp.exp(later_log)[:, :, None] * exit_cot
    causal = jnp.arange(BLOCK)[:, None] >= jnp.arange(BLOCK)[None, :]
    decays = jnp.exp(
        jnp.where(causal[None, :, :, None], cumlog[:, :, None, :] - cumlog[:, None, :, :], -jnp.inf)
    )
    scores = jnp.einsum("ntd,nsd,ntsd->nts", query_blk, key_blk, decays)
    grad_scores = jnp.einsum("ntj,nsj->nts", grad_blk, value_blk)
    grad_query = jnp.exp(cumlog) * jnp.einsum("ntj,ndj->ntd", grad_blk, starts)
    grad_query = grad_query + jnp.einsum("nts,nsd,ntsd->ntd", grad_scores, key_blk, decays)
    to_end = jnp.exp(cumlog[:, -1:, :] - cumlog)
    grad_key = jnp.einsum("nts,ntd,ntsd->nsd", grad_scores, query_blk, decays)
    grad_key = grad_key + to_end * jnp.einsum("nsj,ndj->nsd", value_blk, exit_cots)
    grad_value = jnp.einsum("nts,ntj->nsj", scores, grad_blk)
    grad_value = grad_value + jnp.einsum("nsd,ndj->nsj", key_blk * to_end, exit_cots)
    length = query_rows.shape[0]
    key_width = query_rows.shape[1]
    per_position = (query_blk * grad_query - key_blk * grad_key).reshape(length, key_width)
    grad_log = (
        jnp.flip(jnp.cumsum(jnp.flip(per_position, 0), 0), 0)
        + jnp.sum(end_state * exit_cot, axis=1)[None, :]
    )
    return (
        grad_query.reshape(length, key_width),
        grad_key.reshape(length, key_width),
        grad_value.reshape(length, value_rows.shape[1]),
        grad_log,
    )


def on_device(
    resid,
    norm_gain,
    cotangent,
    route_ids,
    route_weight,
    expert_gate,
    expert_up,
    expert_down,
    out_proj,
    mixed,
    query,
    key,
    value,
    log_decay,
    span_state,
):
    tokens_here = resid.shape[0]
    model_width = resid.shape[1]
    half = model_width // 2
    sp_count = lax.axis_size(SP)
    y_count = lax.axis_size("y")
    experts = sp_count * expert_gate.shape[0]
    capacity = 3 * tokens_here // experts
    slots = experts * capacity
    core = lax.axis_index("c")
    resid_f = resid.astype(jnp.float32)
    inverse_rms = lax.rsqrt(jnp.mean(resid_f * resid_f, axis=1, keepdims=True) + epsilon)
    unit_rows = resid_f * inverse_rms
    normed = (unit_rows * norm_gain).astype(jnp.bfloat16)
    pair_expert = route_ids.reshape(-1)
    onehot = (pair_expert[:, None] == jnp.arange(experts, dtype=jnp.int32)[None, :]).astype(
        jnp.int32
    )
    slot_rank = jnp.sum((jnp.cumsum(onehot, axis=0) - onehot) * onehot, axis=1)
    slot_of = (pair_expert * capacity + slot_rank).reshape(tokens_here, TOP)
    slot_a, slot_b = slot_of[:, 0], slot_of[:, 1]
    packed = lax.broadcasted_iota(jnp.int32, (2 * slots, 2 * tokens_here), 0)
    aim_a = jnp.concatenate([2 * slot_a, 2 * slot_a + 1])[None, :]
    aim_b = jnp.concatenate([2 * slot_b, 2 * slot_b + 1])[None, :]
    hit_a, hit_b = packed == aim_a, packed == aim_b
    weight_a = jnp.concatenate([route_weight[:, 0]] * 2)[None, :]
    weight_b = jnp.concatenate([route_weight[:, 1]] * 2)[None, :]
    slot_weight = jnp.sum(
        jnp.where(hit_a, weight_a, 0.0) + jnp.where(hit_b, weight_b, 0.0), axis=1, keepdims=True
    )
    scale = jnp.where(core == 0, 1.0, slot_weight)
    chosen = jnp.where(core == 0, normed, cotangent)
    rows_two = jnp.concatenate([chosen[:, :half], chosen[:, half:]], axis=0)
    sent = jnp.dot((hit_a | hit_b).astype(jnp.bfloat16), rows_two, preferred_element_type=jnp.float32)
    sent = (sent * scale).astype(jnp.bfloat16).reshape(sp_count, 2 * capacity, half)
    own = lax.all_to_all(sent, SP, 0, 0, tiled=True).reshape(2 * slots, half)
    other = lax.ppermute(own, "c", [(0, 1), (1, 0)])
    rows_in = jnp.where(core == 0, own, other)
    rows_cot = jnp.where(core == 0, other, own)

    gate_w, up_w, down_w = expert_gate[0], expert_up[0], expert_down[0]
    width = gate_w.shape[1]
    into_w = jnp.concatenate([gate_w[:half], gate_w[half:], up_w[:half], up_w[half:]], axis=1)
    down_two = jnp.concatenate([down_w[:, :half], down_w[:, half:]], axis=0)
    pre = jnp.dot(rows_in, into_w, preferred_element_type=jnp.float32)
    gate_pre = pre[:, :width] + jnp.roll(pre[:, width : 2 * width], -1, axis=0)
    up_pre = pre[:, 2 * width : 3 * width] + jnp.roll(pre[:, 3 * width :], -1, axis=0)
    hid = lax.dot_general(
        rows_cot, down_two, (((1,), (1,)), ((), ())), preferred_element_type=jnp.float32
    )
    grad_hidden = hid[:, :width] + jnp.roll(hid[:, width:], -1, axis=0)
    gate_sig = jax.nn.sigmoid(gate_pre)
    first = (lax.broadcasted_iota(jnp.int32, (2 * slots, 1), 0) % 2) == 0

    def kept(values):
        return jnp.where(first, values, 0.0).astype(jnp.bfloat16)

    hidden = kept(gate_pre * gate_sig * up_pre)
    grad_up_act = kept(grad_hidden * gate_pre * gate_sig)
    grad_gate_act = kept(grad_hidden * up_pre * gate_sig * (1.0 + gate_pre * (1.0 - gate_sig)))
    acts = jnp.concatenate([grad_gate_act, grad_up_act], axis=1)
    pick = (
        lax.broadcasted_iota(jnp.int32, (slots, 2 * slots), 1)
        == 2 * lax.broadcasted_iota(jnp.int32, (slots, 2 * slots), 0)
    ).astype(jnp.bfloat16)
    acts = jnp.dot(pick, acts, preferred_element_type=jnp.float32).astype(jnp.bfloat16)
    out_w = jnp.concatenate([gate_w, up_w], axis=1).reshape(y_count, 2, width, 2 * width)
    out_own = jnp.where(core == 0, out_w[:, 0], out_w[:, 1]).reshape(half, 2 * width)
    out_other = jnp.where(core == 0, out_w[:, 1], out_w[:, 0]).reshape(half, 2 * width)

    def onto(weights):
        return lax.dot_general(
            acts, weights, (((1,), (1,)), ((), ())), preferred_element_type=jnp.float32
        )

    passed = lax.ppermute(onto(out_other).astype(jnp.bfloat16), "c", [(0, 1), (1, 0)])
    pair_sum = (onto(out_own) + passed.astype(jnp.float32)).astype(jnp.bfloat16)
    parts = pair_sum.reshape(slots, y_count, width).transpose(1, 0, 2)
    summed = sum_parts(lax.all_to_all(parts, "y", 0, 0, tiled=True)).astype(jnp.bfloat16)

    def beside(values):
        return jnp.concatenate([values, jnp.roll(values, 1, axis=0)], axis=1)

    grad_in_w = lax.dot_general(
        rows_in,
        jnp.concatenate([beside(grad_gate_act), beside(grad_up_act)], axis=1),
        (((0,), (0,)), ((), ())),
        preferred_element_type=jnp.float32,
    ).astype(jnp.bfloat16)
    grad_gate_w = jnp.concatenate([grad_in_w[:, :width], grad_in_w[:, width : 2 * width]], axis=0)
    grad_up_w = jnp.concatenate(
        [grad_in_w[:, 2 * width : 3 * width], grad_in_w[:, 3 * width :]], axis=0
    )
    grad_out_w = lax.dot_general(
        beside(hidden), rows_cot, (((0,), (0,)), ((), ())), preferred_element_type=jnp.float32
    ).astype(jnp.bfloat16)
    grad_down_w = jnp.concatenate([grad_out_w[:width], grad_out_w[width:]], axis=1)

    out_proj_here, own_tied = lax.optimization_barrier((out_proj, rows_in))
    out_proj_all = to_all(out_proj_here, SP).reshape(model_width, -1)

    returned = lax.all_to_all(
        summed.reshape(experts, capacity, -1), SP, split_axis=0, concat_axis=0, tiled=True
    )
    flat_rows = returned.reshape(slots, -1)
    slot_index = lax.broadcasted_iota(jnp.int32, (slots, tokens_here), 0)
    slot_tokens = ((slot_index == slot_a[None, :]) | (slot_index == slot_b[None, :])).astype(
        jnp.bfloat16
    )
    grad_normed = lax.all_gather(
        lax.dot_general(
            slot_tokens, flat_rows, (((0,), (0,)), ((), ())), preferred_element_type=jnp.float32
        ).astype(jnp.bfloat16),
        ("y", "c"),
        axis=1,
        tiled=True,
    ).astype(jnp.float32)
    scaled = grad_normed * norm_gain
    grad_resid = cotangent.astype(jnp.float32) + inverse_rms * (
        scaled - unit_rows * jnp.mean(scaled * unit_rows, axis=1, keepdims=True)
    )
    grad_resid = grad_resid.astype(jnp.bfloat16)
    grad_mixed = jnp.dot(grad_resid, out_proj_all, preferred_element_type=jnp.float32).astype(
        jnp.bfloat16
    )
    share = lax.dot_general(
        grad_resid, mixed, (((0,), (0,)), ((), ())), preferred_element_type=jnp.float32
    ).astype(jnp.bfloat16)
    grad_out_proj = sum_parts(
        lax.all_to_all(
            share.reshape(sp_count, model_width // sp_count, -1), SP, 0, 0, tiled=True
        )
    )
    head_count = query.shape[1] // KEY_CHANNELS
    query_scale = KEY_CHANNELS ** (-0.5)

    def heads_first(values, head_depth):
        return values.reshape(tokens_here, head_count, head_depth).transpose(1, 0, 2)

    query_rows = heads_first(query, KEY_CHANNELS).astype(jnp.float32) * query_scale
    key_rows = heads_first(key, KEY_CHANNELS).astype(jnp.float32)
    value_rows = heads_first(value, DV).astype(jnp.float32)
    grad_rows = heads_first(grad_mixed, DV).astype(jnp.float32)
    decay_rows = heads_first(log_decay, KEY_CHANNELS)
    kept_terms, summary = jax.vmap(span_forward)(
        query_rows, key_rows, value_rows, grad_rows, decay_rows, span_state[0]
    )
    own_decay, own_state = summary[0][0], summary[1][0]
    near_states, near_decays = split_decay(to_all(with_decay(own_state, own_decay), "x"))
    near_sum, near_factor = later_sum(near_states, near_decays, lax.axis_index("x"))
    group_sum, group_factor = later_sum(near_states, near_decays, -1)
    far_states, far_decays = split_decay(to_all(with_decay(group_sum, group_factor), "z"))
    far_sum, _ = later_sum(far_states, far_decays, lax.axis_index("z"))
    exit_cot = near_sum + near_factor[:, None] * far_sum
    head_grads = jax.vmap(span_backward)(
        query_rows, key_rows, value_rows, grad_rows, kept_terms, exit_cot[None]
    )

    def tokens_first(values):
        return values.transpose(1, 0, 2).reshape(tokens_here, -1)

    grad_query = (tokens_first(head_grads[0]) * query_scale).astype(jnp.bfloat16)
    grad_key = tokens_first(head_grads[1]).astype(jnp.bfloat16)
    grad_value = tokens_first(head_grads[2]).astype(jnp.bfloat16)
    grad_log_decay = tokens_first(head_grads[3])
    return (
        grad_gate_w[None],
        grad_up_w[None],
        grad_down_w[None],
        grad_out_proj,
        grad_query,
        grad_key,
        grad_value,
        grad_log_decay,
    )


def solution(mesh):
    finer = Mesh(mesh.devices.reshape(8, 4, 8, 2), ("z", "x", "y", "c"))
    in_specs = (
        P(SP, None),
        P(),
        P(SP, None),
        P(SP, None),
        P(SP, None),
        P(SP, None, TP),
        P(SP, None, TP),
        P(SP, TP, None),
        P(SP, TP),
        P(SP, TP),
        P(SP, TP),
        P(SP, TP),
        P(SP, TP),
        P(SP, TP),
        P(SP, TP, None, None),
    )
    out_specs = (
        P(SP, None, TP),
        P(SP, None, TP),
        P(SP, TP, None),
        P(SP, TP),
        P(SP, TP),
        P(SP, TP),
        P(SP, TP),
        P(SP, TP),
    )
    return jax.shard_map(
        on_device, mesh=finer, in_specs=in_specs, out_specs=out_specs, check_vma=False
    )
```

time: 248 us -> 224 us (0.903)
  blocking collectives: 121 us -> 16.1 us
  waiting for transfers between devices: 37.9 us -> 97 us
  starting transfers between devices: 21 us -> 50.6 us
  between operations: 15.1 us -> 1.53 us
  other arithmetic: 24.2 us -> 29.2 us
  matrix products: 21.5 us -> 16.6 us
  local copies, waits for them, and re-layouts: 6.53 us -> 11.3 us
    all_gather x5 -> x0, blocking collectives: 79.5 us -> none  [the longest x4 66.5 us: prefix_by_axis(): lax.all_gather(part.astype(kind), axis)]
    all_to_all x3 -> x7, waiting for transfers between devices: 32.7 us -> 96.4 us  [the longest x1 35.7 us: on_device(): own = lax.all_to_all(sent, SP, 0, 0, tiled=True).reshape(2 * slots, half)]
    all_to_all x3 -> x7, starting transfers between devices: 20.9 us -> 46.4 us  [the longest x3 14.1 us: to_all(): return lax.all_to_all(copies, axis, 0, 0, tiled=True)]
    all_to_all x1 -> x0, blocking collectives: 24.5 us -> none  [sent_together(): lax.all_to_all(both, axis, split_axis=split_dim, concat_axis=concat_dim,...]
    all_gather x2 -> x0, waiting for transfers between devices: 5.13 us -> none  [the longest x1 5.11 us: sent_together_2(): filled = lax.all_gather(both, axis, axis=dim, tiled=True)]
    dot_general x12 -> x10, matrix products: 18.5 us -> 13.6 us  [the longest x2 2.85 us: onto(): lax.dot_general(acts, weights, (((1,), (1,)), ((), ())), preferred_elemen...]
    ppermute x0 -> x2, starting transfers between devices: none -> 4.2 us  [the longest x1 2.29 us: on_device(): lax.ppermute(onto(out_other).astype(jnp.bfloat16), 'c', [(0, 1), (1, 0)])]
    select_n x0 -> x10, other arithmetic: none -> 3.57 us  [the longest x1 2.27 us: on_device(): jnp.where(core == 0, out_w[:, 1], out_w[:, 0]).reshape(half, 2 * width)]
  transfers between devices with their start and end apart: 5 -> 9, of which waited for: 3 -> 8; matrix products, arithmetic and copies ran while one was open for 17% -> 15% of each run, Pallas kernels for 0% -> 0%
where the time goes in v1:
time: 224 us; the launch traced here: 222 us
  waiting for transfers between devices  97 us (43%)
  starting transfers between devices  50.6 us (23%)
  other arithmetic  29.2 us (13%)
  matrix products  16.6 us (7%)
  blocking collectives  16.1 us (7%)
  local copies, waits for them, and re-layouts  11.3 us (5%)
    all_to_all x1, waiting for transfers between devices, on_device(): own = lax.all_to_all(sent, SP, 0, 0, tiled=True).reshape(2 * slots, half)  35.7 us
    all_to_all x1, waiting for transfers between devices, on_device(): lax.all_to_all(share.reshape(sp_count, model_width // sp_count, -1), SP,...  20.1 us
    all_to_all x3, waiting for transfers between devices, to_all(): return lax.all_to_all(copies, axis, 0, 0, tiled=True)  19.1 us
    all_gather x1, blocking collectives, on_device(): lax.all_gather(lax.dot_general(slot_tokens, flat_rows, (((0,), (0,)), (()...  16.1 us
    all_to_all x1, waiting for transfers between devices, on_device(): lax.all_to_all(parts, 'y', 0, 0, tiled=True)  14.4 us
    all_to_all x3, starting transfers between devices, to_all(): return lax.all_to_all(copies, axis, 0, 0, tiled=True)  14.1 us
    all_to_all x1, starting transfers between devices, on_device(): own = lax.all_to_all(sent, SP, 0, 0, tiled=True).reshape(2 * slots, half)  13.6 us
    all_to_all x1, waiting for transfers between devices, on_device(): lax.all_to_all(summed.reshape(experts, capacity, -1), SP, split_axis=0, c...  7.14 us
  transfers between devices with their start and end apart: 9, of which 8 were waited for; matrix products, arithmetic and copies ran while one was open for 15% of the time, Pallas kernels for 0%

profile of v1, /device:TPU:2, one launch (start us, length us, event | category | flops | bytes accessed | tf_op | source)
XLA Modules:
  0.0 222.4 jit_solution(10590077181551964781)
XLA Ops:
  0.7 0.9 copy.91
  1.8 0.8 slice_bitcast_fusion.11
  2.6 0.6 reduce-window.6
  3.7 0.7 multiply_add_fusion
  4.5 1.2 fusion.22
  6.2 1.0 fusion.48
  7.2 1.8 multiply_convert_fusion
  9.0 13.6 %all-to-all-start = ((bf16[32,24,1024]{2,1,0:T(8,128)(2,1)}), bf16[32,24,1024]{2,1,0:T(8,128)(2,1)S(1)}, u32[]{:S(2)}, u32[]{:S(2)}) async-start(bf16[32,24,1024]{2,1,0:T(8,128)(2,1)} %bitcast.383), calls=%async_computation | async-start | bytes 3145728 | tf_op jit(solution)/shard_map/all_to_all | solution.py:168
  22.7 0.6 iota_multiply_fusion
  23.3 0.7 broadcast_convert_fusion
  24.0 0.6 slice_reduce_fusion.1
  24.8 0.5 convert_bitcast_fusion.13
  25.3 35.7 %all-to-all-done = bf16[32,24,1024]{2,1,0:T(8,128)(2,1)S(1)} async-done(((bf16[32,24,1024]{2,1,0:T(8,128)(2,1)}), bf16[32,24,1024]{2,1,0:T(8,128)(2,1)S(1)}, u32[]{:S(2)}, u32[]{:S(2)}) %all-to-all-start) | async-done | bytes 1572896 | tf_op jit(solution)/shard_map/all_to_all | solution.py:168
  61.0 1.9 collective-permute-start
  63.0 2.3 %broadcast_select_fusion.4 = (bf16[8,1,128,256]{3,2,1,0:T(8,128)(2,1)S(1)}, bf16[8,1,128,256]{3,2,1,0:T(8,128)(2,1)}) fusion(pred[]{:T(512)S(6)} %eq.83, bf16[8,2,128,128]{3,2,1,0:T(8,128)(2,1)S(1)} %bitcast.376, bf16[8,2,128,128]{3,2,1,0:T(8,128)(2,1)} %bitcast.377), kind=kLoop, calls=%fused_computation.94 | loop fusion | flops 3670016 | bytes 2097153 | tf_op jit(solution)/shard_map/jit(_where)/select_n | solution.py:201
  65.2 0.6 slice_bitcast_fusion.13
  65.9 0.7 convert_bitcast_fusion.11
  67.0 1.0 fusion.23
  68.2 2.0 fusion.45
  70.3 0.9 select_convert_fusion
  71.5 0.3 copy-done.35
  71.8 0.4 fusion.11
  72.2 1.3 convolution_convert_fusion.2
  73.5 2.3 %collective-permute-start.1 = (bf16[384,1024]{1,0:T(8,128)(2,1)}, bf16[384,1024]{1,0:T(8,128)(2,1)}, u32[]{:S(2)}, u32[]{:S(2)}) collective-permute-start(bf16[384,1024]{1,0:T(8,128)(2,1)} %convolution_convert_fusion.2), channel_id=1, source_target_pairs={{0,1},{1,0},{2,3},{3,2},{4,5},{5,4},{6,7},{7,6},{8,9},{9,8},{10,11... | collective-permute-start | bytes 2359304 | tf_op jit(solution)/shard_map/ppermute | solution.py:208
  75.8 1.5 while.29
  75.9 0.6 bitcast_dynamic-update-slice_fusion.4
  76.6 0.6 bitcast_dynamic-update-slice_fusion.4
  77.4 0.6 collective-permute-done.1
  78.0 1.5 fusion.31
  79.6 1.1 copy.125
  80.7 7.1 %all-to-all-start.1 = ((bf16[8,384,128]{2,1,0:T(8,128)(2,1)}), bf16[8,384,128]{2,1,0:T(8,128)(2,1)S(1)}, u32[]{:S(2)}, u32[]{:S(2)}) async-start(bf16[8,384,128]{2,1,0:T(8,128)(2,1)} %bitcast.374), calls=%async_computation.1 | async-start | bytes 1572864 | tf_op jit(solution)/shard_map/all_to_all | solution.py:211
  87.9 4.4 %fusion.4 = (bf16[2,64,64]{2,1,0:T(8,128)(2,1)}, f32[2,64,128,64]{2,3,1,0:T(8,128)}) fusion(f32[2,128,64]{1,2,0:T(8,128)S(1)} %copy-done.21, f32[2,128,64]{1,2,0:T(8,128)S(1)} %bitcast.384, f32[2,64,128]{2,1,0:T(8,128)S(1)} %bitcast.371, pred[64,64]{1,0:T(8,128)(4,1)S(1)} %iota_compare_fusion.10), kind=kLoop, calls=%fused_computation.11 | loop fusion | flops 5234688 | bytes 4411392 | tf_op jit(solution)/shard_map/vmap(ntd,nsd,ntsd->nts)/dot_general | solution.py:93
  92.3 1.0 convolution_convert_fusion.1
  93.3 1.0 fusion.147
  94.3 2.8 %convolution_convert_fusion.3 = bf16[256,1024]{1,0:T(8,128)(2,1)} fusion(bf16[768,1024]{1,0:T(8,128)(2,1)} %collective-permute-done, bf16[768,1024]{1,0:T(8,128)(2,1)S(1)} %bitcast.370, pred[]{:T(512)S(6)} %eq.83, bf16[767,128]{1,0:T(8,128)(2,1)S(1)} %bitcast.395, bf16[1,128]{1,0:T(2,128)(2,1)S(1)} %slice.339, bf16[768,128]{1,0:T(8,128)(2,1)S(1)} %copy-done.22), kind=kOutput, calls=%fused_computation.30 | convolution fusion | flops 404881408 | bytes 4063233 | tf_op jit(solution)/shard_map/dot_general | solution.py:226
  97.1 14.4 %all-to-all-done.1 = bf16[8,384,128]{2,1,0:T(8,128)(2,1)S(1)} async-done(((bf16[8,384,128]{2,1,0:T(8,128)(2,1)}), bf16[8,384,128]{2,1,0:T(8,128)(2,1)S(1)}, u32[]{:S(2)}, u32[]{:S(2)}) %all-to-all-start.1) | async-done | bytes 786464 | tf_op jit(solution)/shard_map/all_to_all | solution.py:211
  111.6 0.7 reshape.961
  112.3 6.5 %all-to-all-start.2 = ((bf16[32,12,128]{2,1,0:T(8,128)(2,1)}), bf16[32,12,128]{2,1,0:T(8,128)(2,1)S(1)}, u32[]{:S(2)}, u32[]{:S(2)}) async-start(bf16[32,12,128]{2,1,0:T(8,128)(2,1)} %reshape.961), calls=%async_computation.2 | async-start | bytes 262144 | tf_op jit(solution)/shard_map/all_to_all | solution.py:234
  118.8 1.9 maximum_bitcast_fusion
  120.7 7.1 %all-to-all-done.2 = bf16[32,12,128]{2,1,0:T(8,128)(2,1)S(1)} async-done(((bf16[32,12,128]{2,1,0:T(8,128)(2,1)}), bf16[32,12,128]{2,1,0:T(8,128)(2,1)S(1)}, u32[]{:S(2)}, u32[]{:S(2)}) %all-to-all-start.2) | async-done | bytes 98336 | tf_op jit(solution)/shard_map/all_to_all | solution.py:234
  127.8 1.2 broadcast_in_dim.169
  129.0 5.6 %all-to-all-start.4 = ((bf16[32,64,256]{2,1,0:T(8,128)(2,1)}), bf16[32,64,256]{2,1,0:T(8,128)(2,1)S(1)}, u32[]{:S(2)}, u32[]{:S(2)}) async-start(bf16[32,64,256]{2,1,0:T(8,128)(2,1)} %broadcast_in_dim.169), calls=%async_computation.4 | async-start | bytes 2097152 | tf_op jit(solution)/shard_map/all_to_all | solution.py:36
  134.6 0.8 maximum_bitcast_fusion.1
  135.5 0.8 maximum_bitcast_fusion.2
  136.7 16.1 %all_gather.3 = bf16[128,2048]{1,0:T(8,128)(2,1)S(1)} all-gather(bf16[128,128]{1,0:T(8,128)(2,1)S(1)} %convolution_convert_fusion.5), channel_id=1, replica_groups=mesh['z'=8,'x'=4,'y'=8,'c'=2] {'y','c'}, dimensions={1}, use_global_device_ids=true | all-gather | bytes 557056 | tf_op jit(solution)/shard_map/all_gather | solution.py:242
  153.1 0.4 fusion.21
  153.6 8.0 %all-to-all-done.4 = bf16[32,64,256]{2,1,0:T(8,128)(2,1)S(1)} async-done(((bf16[32,64,256]{2,1,0:T(8,128)(2,1)}), bf16[32,64,256]{2,1,0:T(8,128)(2,1)S(1)}, u32[]{:S(2)}, u32[]{:S(2)}) %all-to-all-start.4) | async-done | bytes 1048608 | tf_op jit(solution)/shard_map/all_to_all | solution.py:36
  162.2 0.3 while.30
  162.8 0.7 broadcast_in_dim.173
  163.5 4.9 %all-to-all-start.5 = ((bf16[4,136,256]{2,1,0:T(8,128)(2,1)}), bf16[4,136,256]{2,1,0:T(8,128)(2,1)S(1)}, u32[]{:S(2)}, u32[]{:S(2)}) async-start(bf16[4,136,256]{2,1,0:T(8,128)(2,1)} %broadcast_in_dim.173), calls=%async_computation.5 | async-start | bytes 557056 | tf_op jit(solution)/shard_map/all_to_all | solution.py:36
  168.7 5.1 %all-to-all-done.5 = bf16[4,136,256]{2,1,0:T(8,128)(2,1)S(1)} async-done(((bf16[4,136,256]{2,1,0:T(8,128)(2,1)}), bf16[4,136,256]{2,1,0:T(8,128)(2,1)S(1)}, u32[]{:S(2)}, u32[]{:S(2)}) %all-to-all-start.5) | async-done | bytes 278560 | tf_op jit(solution)/shard_map/all_to_all | solution.py:36
  174.0 0.9 broadcast_in_dim.175
  174.8 3.5 %all-to-all-start.6 = ((bf16[8,136,256]{2,1,0:T(8,128)(2,1)}), bf16[8,136,256]{2,1,0:T(8,128)(2,1)S(1)}, u32[]{:S(2)}, u32[]{:S(2)}) async-start(bf16[8,136,256]{2,1,0:T(8,128)(2,1)} %broadcast_in_dim.175), calls=%async_computation.6 | async-start | bytes 1114112 | tf_op jit(solution)/shard_map/all_to_all | solution.py:36
  178.4 5.0 %fusion.5 = f32[2,64,128]{2,1,0:T(8,128)S(1)} fusion(f32[2,64,128,64]{2,3,1,0:T(8,128)} %get-tuple-element.289, f32[2,64,128]{2,1,0:T(8,128)S(1)} %copy-done.20, f32[2,64,64]{2,1,0:T(8,128)S(1)} %copy.98), kind=kLoop, calls=%fused_computation.13 | loop fusion | flops 3129344 | bytes 4358144 | tf_op jit(solution)/shard_map/vmap(nts,nsd,ntsd->ntd)/dot_general | solution.py:96
  183.6 1.4 convolution_convert_fusion
  185.0 2.0 multiply_reduce_fusion
  187.0 6.0 %all-to-all-done.6 = bf16[8,136,256]{2,1,0:T(8,128)(2,1)S(1)} async-done(((bf16[8,136,256]{2,1,0:T(8,128)(2,1)}), bf16[8,136,256]{2,1,0:T(8,128)(2,1)S(1)}, u32[]{:S(2)}, u32[]{:S(2)}) %all-to-all-start.6) | async-done | bytes 557088 | tf_op jit(solution)/shard_map/all_to_all | solution.py:36
  193.0 5.0 %all-to-all-start.3 = ((bf16[32,64,256]{2,1,0:T(8,128)(2,1)}), bf16[32,64,256]{2,1,0:T(8,128)(2,1)S(1)}, u32[]{:S(2)}, u32[]{:S(2)}) async-start(bf16[32,64,256]{2,1,0:T(8,128)(2,1)} %bitcast.28), calls=%async_computation.3 | async-start | bytes 2097152 | tf_op jit(solution)/shard_map/all_to_all | solution.py:262
  198.4 0.9 multiply_subtract_fusion
  199.5 0.3 fusion.81
  199.8 0.6 add_bitcast_fusion
  200.7 0.8 fusion.12
  201.6 20.1 %all-to-all-done.3 = bf16[32,64,256]{2,1,0:T(8,128)(2,1)S(1)} async-done(((bf16[32,64,256]{2,1,0:T(8,128)(2,1)}), bf16[32,64,256]{2,1,0:T(8,128)(2,1)S(1)}, u32[]{:S(2)}, u32[]{:S(2)}) %all-to-all-start.3) | async-done | bytes 1048608 | tf_op jit(solution)/shard_map/all_to_all | solution.py:262
  221.6 0.8 convert_reduce_fusion
  (157 shorter events, 6.1 us)
Async XLA Ops:
  0.6 182.9 %copy-start = (bf16[128,256]{1,0:T(8,128)(2,1)S(1)}, bf16[128,256]{1,0:T(8,128)(2,1)}, u32[]{:S(2)}) copy-start(bf16[128,256]{1,0:T(8,128)(2,1)} %param.28) | copy-start | bytes 196612
  0.6 5.5 %copy-start.2 = (bf16[128,2048]{1,0:T(8,128)(2,1)S(1)}, bf16[128,2048]{1,0:T(8,128)(2,1)}, u32[]{:S(2)}) copy-start(bf16[128,2048]{1,0:T(8,128)(2,1)} %param.19) | copy-start | bytes 1572868
  0.7 5.5 %copy-start.6 = (bf16[128,2048]{1,0:T(8,128)(2,1)S(1)}, bf16[128,2048]{1,0:T(8,128)(2,1)}, u32[]{:S(2)}) copy-start(bf16[128,2048]{1,0:T(8,128)(2,1)} %param.21) | copy-start | bytes 1572868
  5.7 0.5 copy-start.33
  9.0 13.6 %copy-start.31 = (f32[128,128]{1,0:T(8,128)S(1)}, f32[128,128]{1,0:T(8,128)}, u32[]{:S(2)}) copy-start(f32[128,128]{1,0:T(8,128)} %param.32) | copy-start | bytes 196612
  9.0 15.6 %copy-start.13 = (bf16[128,256]{1,0:T(8,128)(2,1)S(1)}, bf16[128,256]{1,0:T(8,128)(2,1)}, u32[]{:S(2)}) copy-start(bf16[128,256]{1,0:T(8,128)(2,1)} %param.31) | copy-start | bytes 196612
  9.0 15.6 %copy-start.18 = (bf16[128,128]{1,0:T(8,128)(2,1)S(1)}, bf16[128,128]{1,0:T(8,128)(2,1)}, u32[]{:S(2)}) copy-start(bf16[128,128]{1,0:T(8,128)(2,1)} %param.30) | copy-start | bytes 98308
  9.0 54.0 %copy-start.3 = (bf16[1,2048,128]{2,1,0:T(8,128)(2,1)S(1)}, bf16[1,2048,128]{2,1,0:T(8,128)(2,1)}, u32[]{:S(2)}) copy-start(bf16[1,2048,128]{2,1,0:T(8,128)(2,1)} %param.25) | copy-start | bytes 1572868
  9.0 52.0 %all-to-all-start = ((bf16[32,24,1024]{2,1,0:T(8,128)(2,1)}), bf16[32,24,1024]{2,1,0:T(8,128)(2,1)S(1)}, u32[]{:S(2)}, u32[]{:S(2)}) async-start(bf16[32,24,1024]{2,1,0:T(8,128)(2,1)} %bitcast.383), calls=%async_computation | async-start | bytes 3145728 | tf_op jit(solution)/shard_map/all_to_all | solution.py:168
  22.6 43.2 %copy-start.28 = (bf16[128,128]{1,0:T(8,128)(2,1)S(1)}, bf16[128,128]{1,0:T(8,128)(2,1)}, u32[]{:S(2)}) copy-start(bf16[128,128]{1,0:T(8,128)(2,1)} %param.29) | copy-start | bytes 98308
  61.0 5.7 %collective-permute-start = (bf16[768,1024]{1,0:T(8,128)(2,1)S(1)}, bf16[768,1024]{1,0:T(8,128)(2,1)}, u32[]{:S(2)}, u32[]{:S(2)}) collective-permute-start(bf16[768,1024]{1,0:T(8,128)(2,1)S(1)} %bitcast.368), channel_id=1, source_target_pairs={{0,1},{1,0},{2,3},{3,2},{4,5},{5,4},{6,7},{7,6},{8,9},{9,8},{10,11... | collective-permute-start | bytes 4718600 | tf_op jit(solution)/shard_map/ppermute | solution.py:169
  62.9 3.6 %copy-start.16 = (bf16[1,128,2048]{2,1,0:T(8,128)(2,1)S(1)}, bf16[1,128,2048]{2,1,0:T(8,128)(2,1)}, u32[]{:S(2)}) copy-start(bf16[1,128,2048]{2,1,0:T(8,128)(2,1)} %param.26) | copy-start | bytes 1572868
  63.0 3.6 %copy-start.4 = (bf16[1,2048,128]{2,1,0:T(8,128)(2,1)S(1)}, bf16[1,2048,128]{2,1,0:T(8,128)(2,1)}, u32[]{:S(2)}) copy-start(bf16[1,2048,128]{2,1,0:T(8,128)(2,1)} %param.24) | copy-start | bytes 1572868
  65.9 21.9 %copy-start.11 = (f32[128,128]{1,0:T(8,128)}, f32[128,128]{1,0:T(8,128)S(1)}, u32[]{:S(2)}) copy-start(f32[128,128]{1,0:T(8,128)S(1)} %convert_multiply_fusion.18) | copy-start | bytes 196612
  67.0 1.1 copy-start.8
  71.1 0.7 copy-start.35
  71.4 4.4 %copy-start.23 = (bf16[768,128]{1,0:T(8,128)(2,1)}, bf16[768,128]{1,0:T(8,128)(2,1)S(1)}, u32[]{:S(2)}) copy-start(bf16[768,128]{1,0:T(8,128)(2,1)S(1)} %get-tuple-element.266) | copy-start | bytes 589828
  71.4 4.4 %copy-start.25 = (bf16[768,128]{1,0:T(8,128)(2,1)}, bf16[768,128]{1,0:T(8,128)(2,1)S(1)}, u32[]{:S(2)}) copy-start(bf16[768,128]{1,0:T(8,128)(2,1)S(1)} %get-tuple-element.267) | copy-start | bytes 589828
  71.4 4.4 %copy-start.1 = (f32[1,1,128,256]{3,2,1,0:T(8,128)S(1)}, f32[1,1,128,256]{3,2,1,0:T(8,128)}, u32[]{:S(2)}) copy-start(f32[1,1,128,256]{3,2,1,0:T(8,128)} %param.33) | copy-start | bytes 393220
  71.5 4.4 %copy-start.36 = (f32[2,1,128]{2,1,0:T(1,128)S(1)}, f32[2,1,128]{2,1,0:T(1,128)}, u32[]{:S(2)}) copy-start(f32[2,1,128]{2,1,0:T(1,128)} %get-tuple-element.408) | copy-start | bytes 3076
  73.5 4.5 %collective-permute-start.1 = (bf16[384,1024]{1,0:T(8,128)(2,1)}, bf16[384,1024]{1,0:T(8,128)(2,1)}, u32[]{:S(2)}, u32[]{:S(2)}) collective-permute-start(bf16[384,1024]{1,0:T(8,128)(2,1)} %convolution_convert_fusion.2), channel_id=1, source_target_pairs={{0,1},{1,0},{2,3},{3,2},{4,5},{5,4},{6,7},{7,6},{8,9},{9,8},{10,11... | collective-permute-start | bytes 2359304 | tf_op jit(solution)/shard_map/ppermute | solution.py:208
  75.8 2.2 copy-start.5
  79.6 8.2 %copy-start.21 = (f32[2,128,64]{1,2,0:T(8,128)S(1)}, f32[2,128,64]{1,2,0:T(8,128)}, u32[]{:S(2)}) copy-start(f32[2,128,64]{1,2,0:T(8,128)} %get-tuple-element.296) | copy-start | bytes 196612
  80.7 30.8 %all-to-all-start.1 = ((bf16[8,384,128]{2,1,0:T(8,128)(2,1)}), bf16[8,384,128]{2,1,0:T(8,128)(2,1)S(1)}, u32[]{:S(2)}, u32[]{:S(2)}) async-start(bf16[8,384,128]{2,1,0:T(8,128)(2,1)} %bitcast.374), calls=%async_computation.1 | async-start | bytes 1572864 | tf_op jit(solution)/shard_map/all_to_all | solution.py:211
  87.8 4.4 %copy-start.26 = (bf16[768,128]{1,0:T(8,128)(2,1)S(1)}, bf16[768,128]{1,0:T(8,128)(2,1)}, u32[]{:S(2)}) copy-start(bf16[768,128]{1,0:T(8,128)(2,1)} %copy-done.25) | copy-start | bytes 589828
  87.8 4.4 %copy-start.24 = (bf16[768,128]{1,0:T(8,128)(2,1)S(1)}, bf16[768,128]{1,0:T(8,128)(2,1)}, u32[]{:S(2)}) copy-start(bf16[768,128]{1,0:T(8,128)(2,1)} %copy-done.23) | copy-start | bytes 589828
  87.8 4.4 %copy-start.22 = (bf16[768,128]{1,0:T(8,128)(2,1)S(1)}, bf16[768,128]{1,0:T(8,128)(2,1)}, u32[]{:S(2)}) copy-start(bf16[768,128]{1,0:T(8,128)(2,1)} %get-tuple-element.264) | copy-start | bytes 589828
  87.8 4.4 %copy-start.9 = (bf16[768,1024]{1,0:T(8,128)(2,1)S(1)}, bf16[768,1024]{1,0:T(8,128)(2,1)}, u32[]{:S(2)}) copy-start(bf16[768,1024]{1,0:T(8,128)(2,1)} %copy-done.8) | copy-start | bytes 4718596
  97.1 30.7 %copy-start.32 = (bf16[64,256]{1,0:T(8,128)(2,1)S(1)}, bf16[64,256]{1,0:T(8,128)(2,1)}, u32[]{:S(2)}) copy-start(bf16[64,256]{1,0:T(8,128)(2,1)} %param.27) | copy-start | bytes 98308
  112.3 15.5 %all-to-all-start.2 = ((bf16[32,12,128]{2,1,0:T(8,128)(2,1)}), bf16[32,12,128]{2,1,0:T(8,128)(2,1)S(1)}, u32[]{:S(2)}, u32[]{:S(2)}) async-start(bf16[32,12,128]{2,1,0:T(8,128)(2,1)} %reshape.961), calls=%async_computation.2 | async-start | bytes 262144 | tf_op jit(solution)/shard_map/all_to_all | solution.py:234
  120.7 13.9 %copy-start.10 = (bf16[1024,128]{1,0:T(8,128)(2,1)S(1)}, bf16[1024,128]{1,0:T(8,128)(2,1)}, u32[]{:S(2)}) copy-start(bf16[1024,128]{1,0:T(8,128)(2,1)} %get-tuple-element.275) | copy-start | bytes 786436
  129.0 6.5 %copy-start.17 = (bf16[256,1024]{1,0:T(8,128)(2,1)S(1)}, bf16[256,1024]{1,0:T(8,128)(2,1)}, u32[]{:S(2)}) copy-start(bf16[256,1024]{1,0:T(8,128)(2,1)} %convolution_convert_fusion.3) | copy-start | bytes 1572868
  129.0 32.6 %all-to-all-start.4 = ((bf16[32,64,256]{2,1,0:T(8,128)(2,1)}), bf16[32,64,256]{2,1,0:T(8,128)(2,1)S(1)}, u32[]{:S(2)}, u32[]{:S(2)}) async-start(bf16[32,64,256]{2,1,0:T(8,128)(2,1)} %broadcast_in_dim.169), calls=%async_computation.4 | async-start | bytes 2097152 | tf_op jit(solution)/shard_map/all_to_all | solution.py:36
  134.6 1.8 copy-start.39
  134.6 1.8 copy-start.40
  135.5 17.3 %copy-start.30 = (f32[2048]{0:T(1024)S(1)}, f32[2048]{0:T(1024)}, u32[]{:S(2)}) copy-start(f32[2048]{0:T(1024)} %param.20) | copy-start | bytes 24580
  135.5 17.3 %copy-start.34 = (f32[128]{0:T(128)S(1)}, f32[128]{0:T(128)}, u32[]{:S(2)}) copy-start(f32[128]{0:T(128)} %copy-done.33) | copy-start | bytes 1540
  135.5 17.6 %copy-start.7 = (bf16[128,2048]{1,0:T(8,128)(2,1)S(1)}, bf16[128,2048]{1,0:T(8,128)(2,1)}, u32[]{:S(2)}) copy-start(bf16[128,2048]{1,0:T(8,128)(2,1)} %param.21) | copy-start | bytes 1572868
  153.1 8.8 %copy-start.12 = (f32[128,128]{1,0:T(8,128)S(1)}, f32[128,128]{1,0:T(8,128)}, u32[]{:S(2)}) copy-start(f32[128,128]{1,0:T(8,128)} %copy-done.11) | copy-start | bytes 196612
  153.6 8.6 %copy-start.37 = (f32[2,1,128]{2,1,0:T(1,128)S(1)}, f32[2,1,128]{2,1,0:T(1,128)}, u32[]{:S(2)}) copy-start(f32[2,1,128]{2,1,0:T(1,128)} %get-tuple-element.408) | copy-start | bytes 3076
  162.2 0.6 copy-start.38
  162.2 6.3 %copy-start.14 = (bf16[128,256]{1,0:T(8,128)(2,1)S(1)}, bf16[128,256]{1,0:T(8,128)(2,1)}, u32[]{:S(2)}) copy-start(bf16[128,256]{1,0:T(8,128)(2,1)} %param.31) | copy-start | bytes 196612
  163.5 14.8 %copy-start.20 = (f32[2,64,128]{2,1,0:T(8,128)S(1)}, f32[2,64,128]{2,1,0:T(8,128)}, u32[]{:S(2)}) copy-start(f32[2,64,128]{2,1,0:T(8,128)} %get-tuple-element.297) | copy-start | bytes 196612
  163.5 10.2 %all-to-all-start.5 = ((bf16[4,136,256]{2,1,0:T(8,128)(2,1)}), bf16[4,136,256]{2,1,0:T(8,128)(2,1)S(1)}, u32[]{:S(2)}, u32[]{:S(2)}) async-start(bf16[4,136,256]{2,1,0:T(8,128)(2,1)} %broadcast_in_dim.173), calls=%async_computation.5 | async-start | bytes 557056 | tf_op jit(solution)/shard_map/all_to_all | solution.py:36
  174.8 18.2 %all-to-all-start.6 = ((bf16[8,136,256]{2,1,0:T(8,128)(2,1)}), bf16[8,136,256]{2,1,0:T(8,128)(2,1)S(1)}, u32[]{:S(2)}, u32[]{:S(2)}) async-start(bf16[8,136,256]{2,1,0:T(8,128)(2,1)} %broadcast_in_dim.175), calls=%async_computation.6 | async-start | bytes 1114112 | tf_op jit(solution)/shard_map/all_to_all | solution.py:36
  178.4 5.0 %copy-start.15 = (bf16[2,1,128,256]{3,2,1,0:T(8,128)(2,1)S(1)}, bf16[2,1,128,256]{3,2,1,0:T(8,128)(2,1)}, u32[]{:S(2)}) copy-start(bf16[2,1,128,256]{3,2,1,0:T(8,128)(2,1)} %get-tuple-element.142) | copy-start | bytes 393220
  187.0 11.4 %copy-start.19 = (bf16[128,128]{1,0:T(8,128)(2,1)S(1)}, bf16[128,128]{1,0:T(8,128)(2,1)}, u32[]{:S(2)}) copy-start(bf16[128,128]{1,0:T(8,128)(2,1)} %param.30) | copy-start | bytes 98308
  187.0 11.4 %copy-start.29 = (bf16[128,128]{1,0:T(8,128)(2,1)S(1)}, bf16[128,128]{1,0:T(8,128)(2,1)}, u32[]{:S(2)}) copy-start(bf16[128,128]{1,0:T(8,128)(2,1)} %param.29) | copy-start | bytes 98308
  193.0 28.6 %all-to-all-start.3 = ((bf16[32,64,256]{2,1,0:T(8,128)(2,1)}), bf16[32,64,256]{2,1,0:T(8,128)(2,1)S(1)}, u32[]{:S(2)}, u32[]{:S(2)}) async-start(bf16[32,64,256]{2,1,0:T(8,128)(2,1)} %bitcast.28), calls=%async_computation.3 | async-start | bytes 2097152 | tf_op jit(solution)/shard_map/all_to_all | solution.py:262
  198.4 2.3 %copy-start.27 = (bf16[2,64,64]{2,1,0:T(8,128)(2,1)S(1)}, bf16[2,64,64]{2,1,0:T(8,128)(2,1)}, u32[]{:S(2)}) copy-start(bf16[2,64,64]{2,1,0:T(8,128)(2,1)} %get-tuple-element.288) | copy-start | bytes 49156

commit v2 on v1

--- a/solution.py
+++ b/solution.py
@@ -3,6 +3,7 @@
 from jax import lax
 from jax.sharding import Mesh
 from jax.sharding import PartitionSpec as P
+
 
 KEY_CHANNELS = 128
 DV = 256
@@ -30,6 +31,12 @@
     return total, factor
 
 
+def named_dot(left, right):
+    return lax.dot_general(
+        left, right, (((0,), (0,)), ((), ())), preferred_element_type=jnp.float32
+    ).astype(jnp.bfloat16)
+
+
 def to_all(array, axis):
     count = lax.axis_size(axis)
     copies = jnp.broadcast_to(array[None], (count, *array.shape))
@@ -64,7 +71,9 @@
         piece_part, block_sum = step_item
         return (jnp.exp(block_sum)[:, None] * carry_state + piece_part, carry_state)
 
-    end_state, starts = lax.scan(forward_step, entry_state, (inner_part, block_total))
+    end_state, starts = lax.scan(
+        forward_step, entry_state, (inner_part, block_total), unroll=True
+    )
     own_part = jnp.einsum("ntd,ntj->ndj", query_blk * jnp.exp(cumlog), grad_blk)
 
     def backward_step(carry_state, step_item):
@@ -72,7 +81,11 @@
         return (jnp.exp(block_sum)[:, None] * carry_state + piece_part, carry_state)
 
     start_cot, after_cot = lax.scan(
-        backward_step, jnp.zeros_like(entry_state), (own_part, block_total), reverse=True
+        backward_step,
+        jnp.zeros_like(entry_state),
+        (own_part, block_total),
+        reverse=True,
+        unroll=True,
     )
     span_total = jnp.sum(block_total, axis=0)
     later_log = span_total[None, :] - jnp.cumsum(block_total, axis=0)
@@ -114,7 +127,7 @@
     )
 
 
-def on_device(
+def on_device_body(
     resid,
     norm_gain,
     cotangent,
@@ -166,7 +179,15 @@
     sent = jnp.dot((hit_a | hit_b).astype(jnp.bfloat16), rows_two, preferred_element_type=jnp.float32)
     sent = (sent * scale).astype(jnp.bfloat16).reshape(sp_count, 2 * capacity, half)
     own = lax.all_to_all(sent, SP, 0, 0, tiled=True).reshape(2 * slots, half)
+    proj_near, _ = lax.optimization_barrier((out_proj, sent))
+    proj_near = lax.all_gather(proj_near, "x", axis=0, tiled=True)
     other = lax.ppermute(own, "c", [(0, 1), (1, 0)])
+    half_cols = out_proj.shape[1] // 2
+    copies_a = jnp.broadcast_to(
+        proj_near[None, :, :half_cols], (lax.axis_size("z"), proj_near.shape[0], half_cols)
+    )
+    copies_a, _ = lax.optimization_barrier((copies_a, own))
+    proj_a = lax.all_to_all(copies_a, "z", 0, 0, tiled=True).reshape(model_width, half_cols)
     rows_in = jnp.where(core == 0, own, other)
     rows_cot = jnp.where(core == 0, other, own)
 
@@ -208,28 +229,25 @@
     passed = lax.ppermute(onto(out_other).astype(jnp.bfloat16), "c", [(0, 1), (1, 0)])
     pair_sum = (onto(out_own) + passed.astype(jnp.float32)).astype(jnp.bfloat16)
     parts = pair_sum.reshape(slots, y_count, width).transpose(1, 0, 2)
-    summed = sum_parts(lax.all_to_all(parts, "y", 0, 0, tiled=True)).astype(jnp.bfloat16)
+    swapped = lax.all_to_all(parts, "y", 0, 0, tiled=True)
+    summed = sum_parts(swapped).astype(jnp.bfloat16)
+    proj_b, _ = lax.optimization_barrier((proj_near[:, half_cols:], parts))
+    proj_b = lax.all_gather(proj_b, "z", axis=0, tiled=True)
+    out_proj_all = jnp.concatenate([proj_a, proj_b], axis=1)
 
     def beside(values):
         return jnp.concatenate([values, jnp.roll(values, 1, axis=0)], axis=1)
 
-    grad_in_w = lax.dot_general(
+    grad_in_w = named_dot(
         rows_in,
         jnp.concatenate([beside(grad_gate_act), beside(grad_up_act)], axis=1),
-        (((0,), (0,)), ((), ())),
-        preferred_element_type=jnp.float32,
-    ).astype(jnp.bfloat16)
+    )
     grad_gate_w = jnp.concatenate([grad_in_w[:, :width], grad_in_w[:, width : 2 * width]], axis=0)
     grad_up_w = jnp.concatenate(
         [grad_in_w[:, 2 * width : 3 * width], grad_in_w[:, 3 * width :]], axis=0
     )
-    grad_out_w = lax.dot_general(
-        beside(hidden), rows_cot, (((0,), (0,)), ((), ())), preferred_element_type=jnp.float32
-    ).astype(jnp.bfloat16)
+    grad_out_w = named_dot(beside(hidden), rows_cot)
     grad_down_w = jnp.concatenate([grad_out_w[:width], grad_out_w[width:]], axis=1)
-
-    out_proj_here, own_tied = lax.optimization_barrier((out_proj, rows_in))
-    out_proj_all = to_all(out_proj_here, SP).reshape(model_width, -1)
 
     returned = lax.all_to_all(
         summed.reshape(experts, capacity, -1), SP, split_axis=0, concat_axis=0, tiled=True
@@ -258,43 +276,45 @@
     share = lax.dot_general(
         grad_resid, mixed, (((0,), (0,)), ((), ())), preferred_element_type=jnp.float32
     ).astype(jnp.bfloat16)
-    grad_out_proj = sum_parts(
-        lax.all_to_all(
-            share.reshape(sp_count, model_width // sp_count, -1), SP, 0, 0, tiled=True
-        )
-    )
-    head_count = query.shape[1] // KEY_CHANNELS
     query_scale = KEY_CHANNELS ** (-0.5)
-
-    def heads_first(values, head_depth):
-        return values.reshape(tokens_here, head_count, head_depth).transpose(1, 0, 2)
-
-    query_rows = heads_first(query, KEY_CHANNELS).astype(jnp.float32) * query_scale
-    key_rows = heads_first(key, KEY_CHANNELS).astype(jnp.float32)
-    value_rows = heads_first(value, DV).astype(jnp.float32)
-    grad_rows = heads_first(grad_mixed, DV).astype(jnp.float32)
-    decay_rows = heads_first(log_decay, KEY_CHANNELS)
-    kept_terms, summary = jax.vmap(span_forward)(
-        query_rows, key_rows, value_rows, grad_rows, decay_rows, span_state[0]
-    )
-    own_decay, own_state = summary[0][0], summary[1][0]
+    query_rows = query.astype(jnp.float32) * query_scale
+    key_rows = key.astype(jnp.float32)
+    value_rows = value.astype(jnp.float32)
+    grad_rows = grad_mixed.astype(jnp.float32)
+    kept_terms, summary = span_forward(
+        query_rows, key_rows, value_rows, grad_rows, log_decay, span_state[0, 0]
+    )
+    own_decay, own_state = summary
     near_states, near_decays = split_decay(to_all(with_decay(own_state, own_decay), "x"))
     near_sum, near_factor = later_sum(near_states, near_decays, lax.axis_index("x"))
     group_sum, group_factor = later_sum(near_states, near_decays, -1)
-    far_states, far_decays = split_decay(to_all(with_decay(group_sum, group_factor), "z"))
+    far_filled = to_all(with_decay(group_sum, group_factor), "z")
+    far_states, far_decays = split_decay(far_filled)
+    z_count, x_count = lax.axis_size("z"), lax.axis_size("x")
+    share_rows = model_width // sp_count
+    share_x = share.reshape(z_count, x_count, share_rows, -1).transpose(1, 0, 2, 3)
+    place = lax.axis_index("x")
+
+    def for_place(k):
+        return lax.dynamic_index_in_dim(share_x, jnp.bitwise_and(place + k, x_count - 1), 0, keepdims=False)
+
+    share_sum = for_place(0).astype(jnp.float32)
+    for k in range(1, 4):
+        passed = lax.ppermute(
+            for_place(k), "x", [(i, (i + k) % 4) for i in range(4)]
+        )
+        share_sum = share_sum + passed.astype(jnp.float32)
+    share_z = share_sum.astype(jnp.bfloat16)
+    share_z = lax.all_to_all(share_z, "z", 0, 0, tiled=True)
+    grad_out_proj = sum_parts(share_z)
     far_sum, _ = later_sum(far_states, far_decays, lax.axis_index("z"))
     exit_cot = near_sum + near_factor[:, None] * far_sum
-    head_grads = jax.vmap(span_backward)(
-        query_rows, key_rows, value_rows, grad_rows, kept_terms, exit_cot[None]
-    )
-
-    def tokens_first(values):
-        return values.transpose(1, 0, 2).reshape(tokens_here, -1)
-
-    grad_query = (tokens_first(head_grads[0]) * query_scale).astype(jnp.bfloat16)
-    grad_key = tokens_first(head_grads[1]).astype(jnp.bfloat16)
-    grad_value = tokens_first(head_grads[2]).astype(jnp.bfloat16)
-    grad_log_decay = tokens_first(head_grads[3])
+    grad_query, grad_key, grad_value, grad_log_decay = span_backward(
+        query_rows, key_rows, value_rows, grad_rows, kept_terms, exit_cot
+    )
+    grad_query = (grad_query * query_scale).astype(jnp.bfloat16)
+    grad_key = grad_key.astype(jnp.bfloat16)
+    grad_value = grad_value.astype(jnp.bfloat16)
     return (
         grad_gate_w[None],
         grad_up_w[None],
@@ -337,5 +357,5 @@
         P(SP, TP),
     )
     return jax.shard_map(
-        on_device, mesh=finer, in_specs=in_specs, out_specs=out_specs, check_vma=False
-    )
+        on_device_body, mesh=finer, in_specs=in_specs, out_specs=out_specs, check_vma=False
+    )

time: 224 us -> 256 us (1.14)
  the two profiles are of different devices: /device:TPU:2 before, /device:TPU:10 now
where the time goes in v2:
time: 256 us; the launch traced here: 254 us
  waiting for transfers between devices  83.4 us (33%)
  starting transfers between devices  61.7 us (24%)
  blocking collectives  57.4 us (22%)
  other arithmetic  25.8 us (10%)
  matrix products  13.9 us (5%)
  local copies, waits for them, and re-layouts  10.7 us (4%)
    all_to_all x1, waiting for transfers between devices, on_device_body(): own = lax.all_to_all(sent, SP, 0, 0, tiled=True).reshape(2 * slots, half)  35.1 us
    all_gather x1, blocking collectives, on_device_body(): proj_b = lax.all_gather(proj_b, 'z', axis=0, tiled=True)  26.6 us
    all_gather x1, blocking collectives, on_device_body(): lax.all_gather(lax.dot_general(slot_tokens, flat_rows, (((0,), (0,)), (()...  17.9 us
    all_to_all x1, waiting for transfers between devices, on_device_body(): swapped = lax.all_to_all(parts, 'y', 0, 0, tiled=True)  17.3 us
    all_to_all x1, starting transfers between devices, on_device_body(): own = lax.all_to_all(sent, SP, 0, 0, tiled=True).reshape(2 * slots, half)  13.7 us
    all_gather x1, blocking collectives, on_device_body(): proj_near = lax.all_gather(proj_near, 'x', axis=0, tiled=True)  12.9 us
    all_to_all x1, waiting for transfers between devices, on_device_body(): share_z = lax.all_to_all(share_z, 'z', 0, 0, tiled=True)  11.9 us
    ppermute x3, starting transfers between devices, on_device_body(): lax.ppermute(for_place(k), 'x', [(i, (i + k) % 4) for i in range(4)])  10.4 us
  transfers between devices with their start and end apart: 12, of which 8 were waited for; matrix products, arithmetic and copies ran while one was open for 10% of the time, Pallas kernels for 0%

profile of v2, /device:TPU:10, one launch (start us, length us, event | category | flops | bytes accessed | tf_op | source)
XLA Modules:
  0.0 254.4 jit_solution(16292109527799598761)
XLA Ops:
  0.6 0.8 copy.67
  1.8 0.6 reduce-window.6
  2.9 0.7 multiply_add_fusion.4
  3.6 0.8 slice_bitcast_fusion.12
  4.4 1.2 fusion.18
  5.9 1.3 fusion.47
  7.3 1.8 multiply_convert_fusion
  9.1 13.7 %all-to-all-start = ((bf16[32,24,1024]{2,1,0:T(8,128)(2,1)}), bf16[32,24,1024]{2,1,0:T(8,128)(2,1)}, u32[]{:S(2)}, u32[]{:S(2)}) async-start(bf16[32,24,1024]{2,1,0:T(8,128)(2,1)} %bitcast.10), calls=%async_computation | async-start | bytes 3145728 | tf_op jit(solution)/shard_map/all_to_all | solution.py:181
  23.0 0.6 fusion.142
  23.5 0.6 iota_multiply_fusion
  24.5 0.5 slice_bitcast_fusion.14
  25.0 0.6 broadcast_multiply_fusion
  25.5 0.6 fusion.147
  26.2 35.1 %all-to-all-done = bf16[32,24,1024]{2,1,0:T(8,128)(2,1)} async-done(((bf16[32,24,1024]{2,1,0:T(8,128)(2,1)}), bf16[32,24,1024]{2,1,0:T(8,128)(2,1)}, u32[]{:S(2)}, u32[]{:S(2)}) %all-to-all-start) | async-done | bytes 1572896 | tf_op jit(solution)/shard_map/all_to_all | solution.py:181
  61.3 1.9 collective-permute-start
  63.2 12.9 %all_gather.10 = bf16[256,256]{1,0:T(8,128)(2,1)S(1)} all-gather(bf16[64,256]{1,0:T(8,128)(2,1)S(1)} %copy-done.14), channel_id=1, replica_groups=mesh['z'=8,'x'=4,'y'=8,'c'=2] {'x'}, dimensions={0}, use_global_device_ids=true | all-gather | bytes 163840 | tf_op jit(solution)/shard_map/all_gather | solution.py:183
  76.2 0.6 fusion.165
  77.3 3.7 %fusion = (bf16[2,64,64]{2,1,0:T(8,128)(2,1)S(1)}, f32[2,64,128,64]{2,3,1,0:T(8,128)}) fusion(f32[2,128,64]{1,2,0:T(8,128)S(1)} %get-tuple-element.64, f32[2,128,64]{1,2,0:T(8,128)S(1)} %bitcast.343, f32[2,64,128]{2,1,0:T(8,128)S(1)} %reduce_window_sum.50, pred[64,64]{1,0:T(8,128)(4,1)S(1)} %iota_compare_fusion.10), kind=kLoop, calls=%fused_computation.1 | loop fusion | flops 5234688 | bytes 4411392 | tf_op jit(solution)/shard_map/ntd,nsd,ntsd->nts/dot_general | solution.py:106
  81.0 0.6 fusion.44
  81.7 2.4 fusion.19
  84.2 0.6 copy-done.19
  86.1 0.4 convolution_convert_fusion.2
  86.5 1.9 collective-permute-start.1
  88.4 0.5 convert_bitcast_fusion.12
  88.9 0.9 broadcast_in_dim.159
  89.8 0.7 convolution_convert_fusion.3
  90.6 0.4 fusion.30
  91.1 1.1 copy.97
  92.1 7.5 %all-to-all-start.1 = ((bf16[8,384,128]{2,1,0:T(8,128)(2,1)}), bf16[8,384,128]{2,1,0:T(8,128)(2,1)S(1)}, u32[]{:S(2)}, u32[]{:S(2)}) async-start(bf16[8,384,128]{2,1,0:T(8,128)(2,1)} %bitcast.328), calls=%async_computation.1 | async-start | bytes 1572864 | tf_op jit(solution)/shard_map/all_to_all | solution.py:232
  99.7 0.8 maximum_bitcast_fusion.2
  100.5 2.4 convolution_convert_fusion.1
  103.1 0.8 maximum_bitcast_fusion.1
  104.0 0.8 maximum_bitcast_fusion
  104.8 17.3 %all-to-all-done.1 = bf16[8,384,128]{2,1,0:T(8,128)(2,1)S(1)} async-done(((bf16[8,384,128]{2,1,0:T(8,128)(2,1)}), bf16[8,384,128]{2,1,0:T(8,128)(2,1)S(1)}, u32[]{:S(2)}, u32[]{:S(2)}) %all-to-all-start.1) | async-done | bytes 786464 | tf_op jit(solution)/shard_map/all_to_all | solution.py:232
  122.3 0.7 reshape.636
  123.0 5.2 %all-to-all-start.2 = ((bf16[32,12,128]{2,1,0:T(8,128)(2,1)}), bf16[32,12,128]{2,1,0:T(8,128)(2,1)S(1)}, u32[]{:S(2)}, u32[]{:S(2)}) async-start(bf16[32,12,128]{2,1,0:T(8,128)(2,1)} %reshape.636), calls=%async_computation.2 | async-start | bytes 262144 | tf_op jit(solution)/shard_map/all_to_all | solution.py:252
  128.2 26.6 %all_gather.11 = bf16[2048,128]{1,0:T(8,128)(2,1)S(1)} all-gather(bf16[256,128]{1,0:T(8,128)(2,1)S(1)} %copy-done.9), channel_id=1, replica_groups=mesh['z'=8,'x'=4,'y'=8,'c'=2] {'z'}, dimensions={0}, use_global_device_ids=true | all-gather | bytes 589824 | tf_op jit(solution)/shard_map/all_gather | solution.py:235
  154.8 5.5 %all-to-all-start.4 = ((bf16[8,256,128]{2,1,0:T(8,128)(2,1)}), bf16[8,256,128]{2,1,0:T(8,128)(2,1)}, u32[]{:S(2)}, u32[]{:S(2)}) async-start(bf16[8,256,128]{2,1,0:T(8,128)(2,1)} %broadcast_in_dim.159), calls=%async_computation.4 | async-start | bytes 1048576 | tf_op jit(solution)/shard_map/all_to_all | solution.py:190
  160.6 17.9 %all_gather.9 = bf16[128,2048]{1,0:T(8,128)(2,1)S(1)} all-gather(bf16[128,128]{1,0:T(8,128)(2,1)S(1)} %convolution_convert_fusion.5), channel_id=1, replica_groups=mesh['z'=8,'x'=4,'y'=8,'c'=2] {'y','c'}, dimensions={1}, use_global_device_ids=true | all-gather | bytes 557056 | tf_op jit(solution)/shard_map/all_gather | solution.py:260
  178.9 0.4 fusion.17
  179.3 1.4 convolution_convert_fusion.4
  181.1 0.7 broadcast_in_dim.163
  181.8 4.8 %all-to-all-start.5 = ((bf16[4,136,256]{2,1,0:T(8,128)(2,1)}), bf16[4,136,256]{2,1,0:T(8,128)(2,1)S(1)}, u32[]{:S(2)}, u32[]{:S(2)}) async-start(bf16[4,136,256]{2,1,0:T(8,128)(2,1)} %broadcast_in_dim.163), calls=%async_computation.5 | async-start | bytes 557056 | tf_op jit(solution)/shard_map/all_to_all | solution.py:43
  186.6 0.5 convolution_convert_fusion
  187.3 0.8 dynamic-slice_bitcast_fusion.2
  188.1 3.4 %collective-permute-start.2 = (bf16[8,64,256]{2,1,0:T(8,128)(2,1)}, bf16[8,64,256]{2,1,0:T(8,128)(2,1)S(1)}, u32[]{:S(2)}, u32[]{:S(2)}) collective-permute-start(bf16[8,64,256]{2,1,0:T(8,128)(2,1)} %get-tuple-element.34), channel_id=1, source_target_pairs={{0,16},{16,32},{32,48},{48,0},{1,17},{17,33},{33,49},{49,1},{2,18}... | collective-permute-start | bytes 786440 | tf_op jit(solution)/shard_map/ppermute | solution.py:303
  191.5 2.5 collective-permute-start.3
  194.0 4.5 %collective-permute-start.4 = (bf16[8,64,256]{2,1,0:T(8,128)(2,1)S(1)}, bf16[8,64,256]{2,1,0:T(8,128)(2,1)}, u32[]{:S(2)}, u32[]{:S(2)}) collective-permute-start(bf16[8,64,256]{2,1,0:T(8,128)(2,1)S(1)} %get-tuple-element.35), channel_id=1, source_target_pairs={{0,48},{16,0},{32,16},{48,32},{1,49},{17,1},{33,17},{49,33},{2,50}... | collective-permute-start | bytes 786440 | tf_op jit(solution)/shard_map/ppermute | solution.py:303
  198.6 0.8 collective-permute-done.2
  199.4 4.8 %collective-permute-done.3 = bf16[8,64,256]{2,1,0:T(8,128)(2,1)} collective-permute-done((bf16[8,64,256]{2,1,0:T(8,128)(2,1)S(1)}, bf16[8,64,256]{2,1,0:T(8,128)(2,1)}, u32[]{:S(2)}, u32[]{:S(2)}) %collective-permute-start.3) | collective-permute-done | bytes 262176 | tf_op jit(solution)/shard_map/ppermute | solution.py:303
  204.2 4.1 %collective-permute-done.4 = bf16[8,64,256]{2,1,0:T(8,128)(2,1)} collective-permute-done((bf16[8,64,256]{2,1,0:T(8,128)(2,1)S(1)}, bf16[8,64,256]{2,1,0:T(8,128)(2,1)}, u32[]{:S(2)}, u32[]{:S(2)}) %collective-permute-start.4) | collective-permute-done | bytes 262176 | tf_op jit(solution)/shard_map/ppermute | solution.py:303
  208.4 1.9 fusion.56
  210.2 7.2 %all-to-all-start.3 = ((bf16[8,64,256]{2,1,0:T(8,128)(2,1)}), bf16[8,64,256]{2,1,0:T(8,128)(2,1)S(1)}, u32[]{:S(2)}, u32[]{:S(2)}) async-start(bf16[8,64,256]{2,1,0:T(8,128)(2,1)} %fusion.56), calls=%async_computation.3 | async-start | bytes 524288 | tf_op jit(solution)/shard_map/all_to_all | solution.py:308
  217.6 11.9 %all-to-all-done.3 = bf16[8,64,256]{2,1,0:T(8,128)(2,1)S(1)} async-done(((bf16[8,64,256]{2,1,0:T(8,128)(2,1)}), bf16[8,64,256]{2,1,0:T(8,128)(2,1)S(1)}, u32[]{:S(2)}, u32[]{:S(2)}) %all-to-all-start.3) | async-done | bytes 262176 | tf_op jit(solution)/shard_map/all_to_all | solution.py:308
  229.5 0.9 broadcast_in_dim.164
  230.4 3.5 %all-to-all-start.6 = ((bf16[8,136,256]{2,1,0:T(8,128)(2,1)}), bf16[8,136,256]{2,1,0:T(8,128)(2,1)S(1)}, u32[]{:S(2)}, u32[]{:S(2)}) async-start(bf16[8,136,256]{2,1,0:T(8,128)(2,1)} %broadcast_in_dim.164), calls=%async_computation.6 | async-start | bytes 1114112 | tf_op jit(solution)/shard_map/all_to_all | solution.py:43
  233.9 4.9 %fusion.1 = f32[2,64,128]{2,1,0:T(8,128)S(1)} fusion(f32[2,64,128,64]{2,3,1,0:T(8,128)} %get-tuple-element.56, f32[2,64,128]{2,1,0:T(8,128)S(1)} %get-tuple-element.65, f32[2,64,64]{2,1,0:T(8,128)S(1)} %copy.72), kind=kLoop, calls=%fused_computation.3 | loop fusion | flops 3129344 | bytes 4358144 | tf_op jit(solution)/shard_map/nts,nsd,ntsd->ntd/dot_general | solution.py:109
  239.0 2.0 multiply_reduce_fusion
  241.0 0.7 convert_reduce_fusion
  241.7 9.2 %all-to-all-done.6 = bf16[8,136,256]{2,1,0:T(8,128)(2,1)S(1)} async-done(((bf16[8,136,256]{2,1,0:T(8,128)(2,1)}), bf16[8,136,256]{2,1,0:T(8,128)(2,1)S(1)}, u32[]{:S(2)}, u32[]{:S(2)}) %all-to-all-start.6) | async-done | bytes 557088 | tf_op jit(solution)/shard_map/all_to_all | solution.py:43
  251.5 0.9 multiply_subtract_fusion
  252.5 0.4 fusion.86
  252.9 0.6 broadcast_add_fusion
  253.6 0.8 fusion.8
  (129 shorter events, 6.1 us)
Async XLA Ops:
  0.6 186.0 %copy-start = (bf16[128,256]{1,0:T(8,128)(2,1)S(1)}, bf16[128,256]{1,0:T(8,128)(2,1)}, u32[]{:S(2)}) copy-start(bf16[128,256]{1,0:T(8,128)(2,1)} %param.24) | copy-start | bytes 196612
  5.6 1.7 copy-start.17
  9.0 13.8 %copy-start.13 = (f32[128,128]{1,0:T(8,128)S(1)}, f32[128,128]{1,0:T(8,128)}, u32[]{:S(2)}) copy-start(f32[128,128]{1,0:T(8,128)} %param.28) | copy-start | bytes 196612
  9.0 15.1 %copy-start.2 = (bf16[1,2048,128]{2,1,0:T(8,128)(2,1)S(1)}, bf16[1,2048,128]{2,1,0:T(8,128)(2,1)}, u32[]{:S(2)}) copy-start(bf16[1,2048,128]{2,1,0:T(8,128)(2,1)} %param.21) | copy-start | bytes 1572868
  9.0 15.1 %copy-start.3 = (bf16[1,2048,128]{2,1,0:T(8,128)(2,1)S(1)}, bf16[1,2048,128]{2,1,0:T(8,128)(2,1)}, u32[]{:S(2)}) copy-start(bf16[1,2048,128]{2,1,0:T(8,128)(2,1)} %param.20) | copy-start | bytes 1572868
  9.1 52.2 %all-to-all-start = ((bf16[32,24,1024]{2,1,0:T(8,128)(2,1)}), bf16[32,24,1024]{2,1,0:T(8,128)(2,1)}, u32[]{:S(2)}, u32[]{:S(2)}) async-start(bf16[32,24,1024]{2,1,0:T(8,128)(2,1)} %bitcast.10), calls=%async_computation | async-start | bytes 3145728 | tf_op jit(solution)/shard_map/all_to_all | solution.py:181
  22.7 3.4 %copy-start.10 = (bf16[128,128]{1,0:T(8,128)(2,1)S(1)}, bf16[128,128]{1,0:T(8,128)(2,1)}, u32[]{:S(2)}) copy-start(bf16[128,128]{1,0:T(8,128)(2,1)} %param.25) | copy-start | bytes 98308
  22.7 3.4 %copy-start.8 = (bf16[128,128]{1,0:T(8,128)(2,1)S(1)}, bf16[128,128]{1,0:T(8,128)(2,1)}, u32[]{:S(2)}) copy-start(bf16[128,128]{1,0:T(8,128)(2,1)} %param.26) | copy-start | bytes 98308
  22.7 40.5 %copy-start.14 = (bf16[64,256]{1,0:T(8,128)(2,1)S(1)}, bf16[64,256]{1,0:T(8,128)(2,1)}, u32[]{:S(2)}) copy-start(bf16[64,256]{1,0:T(8,128)(2,1)} %param.23) | copy-start | bytes 98308
  22.7 54.0 %copy-start.6 = (bf16[128,256]{1,0:T(8,128)(2,1)S(1)}, bf16[128,256]{1,0:T(8,128)(2,1)}, u32[]{:S(2)}) copy-start(bf16[128,256]{1,0:T(8,128)(2,1)} %param.27) | copy-start | bytes 196612
  22.9 54.1 %copy-start.21 = (f32[128]{0:T(128)}, f32[128]{0:T(128)S(1)}, u32[]{:S(2)}) copy-start(f32[128]{0:T(128)S(1)} %get-tuple-element.62) | copy-start | bytes 1540
  24.1 52.9 %copy-start.5 = (f32[1,1,128,256]{3,2,1,0:T(8,128)S(1)}, f32[1,1,128,256]{3,2,1,0:T(8,128)}, u32[]{:S(2)}) copy-start(f32[1,1,128,256]{3,2,1,0:T(8,128)} %param.29) | copy-start | bytes 393220
  24.2 53.0 %copy-start.7 = (bf16[1,128,2048]{2,1,0:T(8,128)(2,1)S(1)}, bf16[1,128,2048]{2,1,0:T(8,128)(2,1)}, u32[]{:S(2)}) copy-start(bf16[1,128,2048]{2,1,0:T(8,128)(2,1)} %param.22) | copy-start | bytes 1572868
  26.1 51.1 %copy-start.15 = (f32[128]{0:T(128)}, f32[128]{0:T(128)S(1)}, u32[]{:S(2)}) copy-start(f32[128]{0:T(128)S(1)} %get-tuple-element.58) | copy-start | bytes 1540
  61.3 19.7 %collective-permute-start = (bf16[768,1024]{1,0:T(8,128)(2,1)}, bf16[768,1024]{1,0:T(8,128)(2,1)S(1)}, u32[]{:S(2)}, u32[]{:S(2)}) collective-permute-start(bf16[768,1024]{1,0:T(8,128)(2,1)} %bitcast.11), channel_id=1, source_target_pairs={{0,1},{1,0},{2,3},{3,2},{4,5},{5,4},{6,7},{7,6},{8,9},{9,8},{10,11... | collective-permute-start | bytes 4718600 | tf_op jit(solution)/shard_map/ppermute | solution.py:184
  81.0 8.8 %copy-start.28 = (bf16[768,1024]{1,0:T(8,128)(2,1)}, bf16[768,1024]{1,0:T(8,128)(2,1)S(1)}, u32[]{:S(2)}) copy-start(bf16[768,1024]{1,0:T(8,128)(2,1)S(1)} %collective-permute-done) | copy-start | bytes 4718596
  84.1 0.7 copy-start.19
  85.0 0.7 copy-start.23
  85.3 3.1 %copy-start.22 = (f32[128]{0:T(128)S(1)}, f32[128]{0:T(128)}, u32[]{:S(2)}) copy-start(f32[128]{0:T(128)} %copy-done.21) | copy-start | bytes 1540
  86.5 4.2 %collective-permute-start.1 = (bf16[384,1024]{1,0:T(8,128)(2,1)S(1)}, bf16[384,1024]{1,0:T(8,128)(2,1)S(1)}, u32[]{:S(2)}, u32[]{:S(2)}) collective-permute-start(bf16[384,1024]{1,0:T(8,128)(2,1)S(1)} %convolution_convert_fusion.2), channel_id=1, source_target_pairs={{0,1},{1,0},{2,3},{3,2},{4,5},{5,4},{6,7},{7,6},{8,9},{9,8},{10,11... | collective-permute-start | bytes 2359304 | tf_op jit(solution)/shard_map/ppermute | solution.py:229
  92.1 30.0 %all-to-all-start.1 = ((bf16[8,384,128]{2,1,0:T(8,128)(2,1)}), bf16[8,384,128]{2,1,0:T(8,128)(2,1)S(1)}, u32[]{:S(2)}, u32[]{:S(2)}) async-start(bf16[8,384,128]{2,1,0:T(8,128)(2,1)} %bitcast.328), calls=%async_computation.1 | async-start | bytes 1572864 | tf_op jit(solution)/shard_map/all_to_all | solution.py:232
  103.1 25.0 %copy-start.9 = (bf16[256,128]{1,0:T(8,128)(2,1)S(1)}, bf16[256,128]{1,0:T(8,128)(2,1)}, u32[]{:S(2)}) copy-start(bf16[256,128]{1,0:T(8,128)(2,1)} %get-tuple-element.13) | copy-start | bytes 196612
  104.8 55.5 %copy-start.26 = (s32[128]{0:T(128)S(1)}, s32[128]{0:T(128)}, u32[]{:S(2)}) copy-start(s32[128]{0:T(128)} %get-tuple-element.78) | copy-start | bytes 1540
  104.8 55.5 %copy-start.27 = (s32[128]{0:T(128)S(1)}, s32[128]{0:T(128)}, u32[]{:S(2)}) copy-start(s32[128]{0:T(128)} %get-tuple-element.79) | copy-start | bytes 1540
  122.3 56.3 %copy-start.1 = (bf16[128,2048]{1,0:T(8,128)(2,1)S(1)}, bf16[128,2048]{1,0:T(8,128)(2,1)}, u32[]{:S(2)}) copy-start(bf16[128,2048]{1,0:T(8,128)(2,1)} %param.15) | copy-start | bytes 1572868
  122.3 56.3 %copy-start.12 = (f32[2048]{0:T(1024)S(1)}, f32[2048]{0:T(1024)}, u32[]{:S(2)}) copy-start(f32[2048]{0:T(1024)} %param.16) | copy-start | bytes 24580
  122.3 56.2 %copy-start.18 = (f32[128]{0:T(128)S(1)}, f32[128]{0:T(128)}, u32[]{:S(2)}) copy-start(f32[128]{0:T(128)} %copy-done.17) | copy-start | bytes 1540
  123.0 31.8 %all-to-all-start.2 = ((bf16[32,12,128]{2,1,0:T(8,128)(2,1)}), bf16[32,12,128]{2,1,0:T(8,128)(2,1)S(1)}, u32[]{:S(2)}, u32[]{:S(2)}) async-start(bf16[32,12,128]{2,1,0:T(8,128)(2,1)} %reshape.636), calls=%async_computation.2 | async-start | bytes 262144 | tf_op jit(solution)/shard_map/all_to_all | solution.py:252
  154.8 24.1 %copy-start.4 = (bf16[128,2048]{1,0:T(8,128)(2,1)S(1)}, bf16[128,2048]{1,0:T(8,128)(2,1)}, u32[]{:S(2)}) copy-start(bf16[128,2048]{1,0:T(8,128)(2,1)} %param.17) | copy-start | bytes 1572868
  154.8 24.6 %all-to-all-start.4 = ((bf16[8,256,128]{2,1,0:T(8,128)(2,1)}), bf16[8,256,128]{2,1,0:T(8,128)(2,1)}, u32[]{:S(2)}, u32[]{:S(2)}) async-start(bf16[8,256,128]{2,1,0:T(8,128)(2,1)} %broadcast_in_dim.159), calls=%async_computation.4 | async-start | bytes 1048576 | tf_op jit(solution)/shard_map/all_to_all | solution.py:190
  179.3 1.6 copy-start.16
  179.3 1.6 copy-start.24
  179.3 1.7 copy-start.25
  181.8 16.8 %all-to-all-start.5 = ((bf16[4,136,256]{2,1,0:T(8,128)(2,1)}), bf16[4,136,256]{2,1,0:T(8,128)(2,1)S(1)}, u32[]{:S(2)}, u32[]{:S(2)}) async-start(bf16[4,136,256]{2,1,0:T(8,128)(2,1)} %broadcast_in_dim.163), calls=%async_computation.5 | async-start | bytes 557056 | tf_op jit(solution)/shard_map/all_to_all | solution.py:43
  188.1 11.3 %collective-permute-start.2 = (bf16[8,64,256]{2,1,0:T(8,128)(2,1)}, bf16[8,64,256]{2,1,0:T(8,128)(2,1)S(1)}, u32[]{:S(2)}, u32[]{:S(2)}) collective-permute-start(bf16[8,64,256]{2,1,0:T(8,128)(2,1)} %get-tuple-element.34), channel_id=1, source_target_pairs={{0,16},{16,32},{32,48},{48,0},{1,17},{17,33},{33,49},{49,1},{2,18}... | collective-permute-start | bytes 786440 | tf_op jit(solution)/shard_map/ppermute | solution.py:303
  191.5 12.7 %collective-permute-start.3 = (bf16[8,64,256]{2,1,0:T(8,128)(2,1)S(1)}, bf16[8,64,256]{2,1,0:T(8,128)(2,1)}, u32[]{:S(2)}, u32[]{:S(2)}) collective-permute-start(bf16[8,64,256]{2,1,0:T(8,128)(2,1)S(1)} %get-tuple-element.36), channel_id=1, source_target_pairs={{0,32},{16,48},{32,0},{48,16},{1,33},{17,49},{33,1},{49,17},{2,34}... | collective-permute-start | bytes 786440 | tf_op jit(solution)/shard_map/ppermute | solution.py:303
  194.0 14.3 %collective-permute-start.4 = (bf16[8,64,256]{2,1,0:T(8,128)(2,1)S(1)}, bf16[8,64,256]{2,1,0:T(8,128)(2,1)}, u32[]{:S(2)}, u32[]{:S(2)}) collective-permute-start(bf16[8,64,256]{2,1,0:T(8,128)(2,1)S(1)} %get-tuple-element.35), channel_id=1, source_target_pairs={{0,48},{16,0},{32,16},{48,32},{1,49},{17,1},{33,17},{49,33},{2,50}... | collective-permute-start | bytes 786440 | tf_op jit(solution)/shard_map/ppermute | solution.py:303
  210.2 19.3 %all-to-all-start.3 = ((bf16[8,64,256]{2,1,0:T(8,128)(2,1)}), bf16[8,64,256]{2,1,0:T(8,128)(2,1)S(1)}, u32[]{:S(2)}, u32[]{:S(2)}) async-start(bf16[8,64,256]{2,1,0:T(8,128)(2,1)} %fusion.56), calls=%async_computation.3 | async-start | bytes 524288 | tf_op jit(solution)/shard_map/all_to_all | solution.py:308
  230.4 20.5 %all-to-all-start.6 = ((bf16[8,136,256]{2,1,0:T(8,128)(2,1)}), bf16[8,136,256]{2,1,0:T(8,128)(2,1)S(1)}, u32[]{:S(2)}, u32[]{:S(2)}) async-start(bf16[8,136,256]{2,1,0:T(8,128)(2,1)} %broadcast_in_dim.164), calls=%async_computation.6 | async-start | bytes 1114112 | tf_op jit(solution)/shard_map/all_to_all | solution.py:43
  239.0 12.5 %copy-start.11 = (bf16[128,128]{1,0:T(8,128)(2,1)S(1)}, bf16[128,128]{1,0:T(8,128)(2,1)}, u32[]{:S(2)}) copy-start(bf16[128,128]{1,0:T(8,128)(2,1)} %param.25) | copy-start | bytes 98308
  241.0 11.6 %copy-start.20 = (f32[128]{0:T(128)S(1)}, f32[128]{0:T(128)}, u32[]{:S(2)}) copy-start(f32[128]{0:T(128)} %get-tuple-element.57) | copy-start | bytes 1540

commit v3 on v2

--- a/solution.py
+++ b/solution.py
@@ -182,12 +182,6 @@
     proj_near, _ = lax.optimization_barrier((out_proj, sent))
     proj_near = lax.all_gather(proj_near, "x", axis=0, tiled=True)
     other = lax.ppermute(own, "c", [(0, 1), (1, 0)])
-    half_cols = out_proj.shape[1] // 2
-    copies_a = jnp.broadcast_to(
-        proj_near[None, :, :half_cols], (lax.axis_size("z"), proj_near.shape[0], half_cols)
-    )
-    copies_a, _ = lax.optimization_barrier((copies_a, own))
-    proj_a = lax.all_to_all(copies_a, "z", 0, 0, tiled=True).reshape(model_width, half_cols)
     rows_in = jnp.where(core == 0, own, other)
     rows_cot = jnp.where(core == 0, other, own)
 
@@ -231,9 +225,18 @@
     parts = pair_sum.reshape(slots, y_count, width).transpose(1, 0, 2)
     swapped = lax.all_to_all(parts, "y", 0, 0, tiled=True)
     summed = sum_parts(swapped).astype(jnp.bfloat16)
-    proj_b, _ = lax.optimization_barrier((proj_near[:, half_cols:], parts))
-    proj_b = lax.all_gather(proj_b, "z", axis=0, tiled=True)
-    out_proj_all = jnp.concatenate([proj_a, proj_b], axis=1)
+    proj_tied, _ = lax.optimization_barrier((proj_near, parts))
+    z_place = lax.axis_index("z")
+    blocks = [(0, proj_near)]
+    for k in (1, 7, 2, 6, 3, 5, 4):
+        ring = [(i, (i + k) % 8) for i in range(8)]
+        blocks.append((k, lax.ppermute(proj_tied, "z", ring)))
+    out_proj_all = jnp.zeros((model_width, out_proj.shape[1]), out_proj.dtype)
+    for k, block in blocks:
+        at = jnp.bitwise_and(z_place + (8 - k), 7) * block.shape[0]
+        out_proj_all = lax.dynamic_update_slice(
+            out_proj_all, block, (at.astype(jnp.uint32), jnp.uint32(0))
+        )
 
     def beside(values):
         return jnp.concatenate([values, jnp.roll(values, 1, axis=0)], axis=1)
@@ -296,7 +299,8 @@
     place = lax.axis_index("x")
 
     def for_place(k):
-        return lax.dynamic_index_in_dim(share_x, jnp.bitwise_and(place + k, x_count - 1), 0, keepdims=False)
+        at = jnp.bitwise_and(place + k, x_count - 1).astype(jnp.uint32)
+        return lax.dynamic_index_in_dim(share_x, at, 0, keepdims=False)
 
     share_sum = for_place(0).astype(jnp.float32)
     for k in range(1, 4):

time: 256 us -> 255 us (level)
  the two profiles are of different devices: /device:TPU:10 before, /device:TPU:2 now
where the time goes in v3:
time: 255 us; the launch traced here: 254 us
  starting transfers between devices  85.4 us (33%)
  waiting for transfers between devices  67.9 us (27%)
  blocking collectives  31.9 us (13%)
  other arithmetic  27.9 us (11%)
  local copies, waits for them, and re-layouts  23.7 us (9%)
  matrix products  15.2 us (6%)
    all_to_all x1, waiting for transfers between devices, on_device_body(): own = lax.all_to_all(sent, SP, 0, 0, tiled=True).reshape(2 * slots, half)  35.6 us
    ppermute x7, starting transfers between devices, on_device_body(): blocks.append((k, lax.ppermute(proj_tied, 'z', ring)))  26.9 us
    all_gather x1, blocking collectives, on_device_body(): lax.all_gather(lax.dot_general(slot_tokens, flat_rows, (((0,), (0,)), (()...  18.8 us
    all_to_all x1, starting transfers between devices, on_device_body(): own = lax.all_to_all(sent, SP, 0, 0, tiled=True).reshape(2 * slots, half)  13.6 us
    all_gather x1, blocking collectives, on_device_body(): proj_near = lax.all_gather(proj_near, 'x', axis=0, tiled=True)  13.1 us
    dynamic_update_slice x8, local copies, waits for them, and re-layouts, on_device_body(): lax.dynamic_update_slice(out_proj_all, block, (at.astype(jnp.uint32), jnp...  12.3 us
    all_to_all x1, waiting for transfers between devices, on_device_body(): share_z = lax.all_to_all(share_z, 'z', 0, 0, tiled=True)  11.9 us
    ppermute x3, starting transfers between devices, on_device_body(): lax.ppermute(for_place(k), 'x', [(i, (i + k) % 4) for i in range(4)])  10.4 us
  transfers between devices with their start and end apart: 18, of which 7 were waited for; matrix products, arithmetic and copies ran while one was open for 16% of the time, Pallas kernels for 0%

profile of v3, /device:TPU:2, one launch (start us, length us, event | category | flops | bytes accessed | tf_op | source)
XLA Modules:
  0.0 253.6 jit_solution(11671087525276839985)
XLA Ops:
  0.6 0.8 copy.67
  2.9 0.7 multiply_add_fusion.4
  3.6 0.8 slice_bitcast_fusion.12
  4.4 1.2 fusion.18
  5.9 1.3 fusion.44
  7.3 1.8 multiply_convert_fusion
  9.1 13.6 %all-to-all-start = ((bf16[32,24,1024]{2,1,0:T(8,128)(2,1)}), bf16[32,24,1024]{2,1,0:T(8,128)(2,1)}, u32[]{:S(2)}, u32[]{:S(2)}) async-start(bf16[32,24,1024]{2,1,0:T(8,128)(2,1)} %bitcast.10), calls=%async_computation | async-start | bytes 3145728 | tf_op jit(solution)/shard_map/all_to_all | solution.py:181
  25.7 35.6 %all-to-all-done = bf16[32,24,1024]{2,1,0:T(8,128)(2,1)} async-done(((bf16[32,24,1024]{2,1,0:T(8,128)(2,1)}), bf16[32,24,1024]{2,1,0:T(8,128)(2,1)}, u32[]{:S(2)}, u32[]{:S(2)}) %all-to-all-start) | async-done | bytes 1572896 | tf_op jit(solution)/shard_map/all_to_all | solution.py:181
  61.3 1.9 collective-permute-start
  64.4 0.7 multiply_add_fusion.3
  65.3 1.5 collective-permute-done
  67.9 2.4 fusion.19
  70.4 0.9 select_convert_fusion
  72.0 1.4 convolution_convert_fusion.2
  73.3 2.2 collective-permute-start.1
  75.5 13.1 %all_gather.7 = bf16[256,256]{1,0:T(8,128)(2,1)S(1)} all-gather(bf16[64,256]{1,0:T(8,128)(2,1)S(1)} %copy-done.20), channel_id=1, replica_groups=mesh['z'=8,'x'=4,'y'=8,'c'=2] {'x'}, dimensions={0}, use_global_device_ids=true | all-gather | bytes 163840 | tf_op jit(solution)/shard_map/all_gather | solution.py:183
  88.7 1.2 dynamic_update_slice.24
  89.9 3.8 %fusion = (bf16[2,64,64]{2,1,0:T(8,128)(2,1)S(1)}, f32[2,64,128,64]{2,3,1,0:T(8,128)}) fusion(f32[2,128,64]{1,2,0:T(8,128)S(1)} %copy-done.9, f32[2,128,64]{1,2,0:T(8,128)S(1)} %bitcast.343, f32[2,64,128]{2,1,0:T(8,128)S(1)} %reduce_window_sum.50, pred[64,64]{1,0:T(8,128)(4,1)S(1)} %iota_compare_fusion.10), kind=kLoop, calls=%fused_computation.1 | loop fusion | flops 5234688 | bytes 4411392 | tf_op jit(solution)/shard_map/ntd,nsd,ntsd->nts/dot_general | solution.py:106
  94.4 0.7 slice.363
  95.1 1.5 convolution_convert_fusion.3
  96.9 1.1 copy.97
  98.1 7.2 %all-to-all-start.1 = ((bf16[8,384,128]{2,1,0:T(8,128)(2,1)}), bf16[8,384,128]{2,1,0:T(8,128)(2,1)S(1)}, u32[]{:S(2)}, u32[]{:S(2)}) async-start(bf16[8,384,128]{2,1,0:T(8,128)(2,1)} %bitcast.328), calls=%async_computation.1 | async-start | bytes 1572864 | tf_op jit(solution)/shard_map/all_to_all | solution.py:226
  105.3 1.2 fusion.158
  106.5 0.8 maximum_bitcast_fusion.2
  107.3 2.4 convolution_convert_fusion.1
  110.0 2.5 collective-permute-start.5
  112.5 4.6 %collective-permute-start.6 = (bf16[256,256]{1,0:T(8,128)(2,1)S(1)}, bf16[256,256]{1,0:T(8,128)(2,1)}, u32[]{:S(2)}, u32[]{:S(2)}) collective-permute-start(bf16[256,256]{1,0:T(8,128)(2,1)S(1)} %all_gather.7), channel_id=1, source_target_pairs={{0,448},{64,0},{128,64},{192,128},{256,192},{320,256},{384,320},{4... | collective-permute-start | bytes 393224 | tf_op jit(solution)/shard_map/ppermute | solution.py:233
  117.0 0.8 maximum_bitcast_fusion.1
  117.9 1.9 collective-permute-start.7
  119.8 6.0 %collective-permute-start.8 = (bf16[256,256]{1,0:T(8,128)(2,1)S(1)}, bf16[256,256]{1,0:T(8,128)(2,1)}, u32[]{:S(2)}, u32[]{:S(2)}) collective-permute-start(bf16[256,256]{1,0:T(8,128)(2,1)S(1)} %all_gather.7), channel_id=1, source_target_pairs={{0,384},{64,448},{128,0},{192,64},{256,128},{320,192},{384,256},{4... | collective-permute-start | bytes 393224 | tf_op jit(solution)/shard_map/ppermute | solution.py:233
  125.8 1.9 collective-permute-start.9
  128.5 9.1 %all-to-all-start.2 = ((bf16[32,12,128]{2,1,0:T(8,128)(2,1)}), bf16[32,12,128]{2,1,0:T(8,128)(2,1)S(1)}, u32[]{:S(2)}, u32[]{:S(2)}) async-start(bf16[32,12,128]{2,1,0:T(8,128)(2,1)} %reshape.632), calls=%async_computation.2 | async-start | bytes 262144 | tf_op jit(solution)/shard_map/all_to_all | solution.py:255
  137.7 6.4 %collective-permute-start.10 = (bf16[256,256]{1,0:T(8,128)(2,1)S(1)}, bf16[256,256]{1,0:T(8,128)(2,1)}, u32[]{:S(2)}, u32[]{:S(2)}) collective-permute-start(bf16[256,256]{1,0:T(8,128)(2,1)S(1)} %all_gather.7), channel_id=1, source_target_pairs={{0,320},{64,384},{128,448},{192,0},{256,64},{320,128},{384,192},{4... | collective-permute-start | bytes 393224 | tf_op jit(solution)/shard_map/ppermute | solution.py:233
  144.1 3.5 %collective-permute-start.11 = (bf16[256,256]{1,0:T(8,128)(2,1)S(1)}, bf16[256,256]{1,0:T(8,128)(2,1)S(1)}, u32[]{:S(2)}, u32[]{:S(2)}) collective-permute-start(bf16[256,256]{1,0:T(8,128)(2,1)S(1)} %all_gather.7), channel_id=1, source_target_pairs={{0,256},{64,320},{128,384},{192,448},{256,0},{320,64},{384,128},{4... | collective-permute-start | bytes 393224 | tf_op jit(solution)/shard_map/ppermute | solution.py:233
  147.7 0.8 maximum_bitcast_fusion
  148.5 1.6 dynamic_update_slice.25
  150.1 1.8 dynamic_update_slice.26
  151.9 1.2 dynamic_update_slice.27
  153.1 1.8 dynamic_update_slice.28
  154.9 1.8 dynamic_update_slice.29
  156.8 1.8 dynamic_update_slice.30
  158.6 1.2 dynamic_update_slice.31
  159.8 0.9 convolution_convert_fusion.5
  160.7 18.8 %all_gather.6 = bf16[128,2048]{1,0:T(8,128)(2,1)S(1)} all-gather(bf16[128,128]{1,0:T(8,128)(2,1)S(1)} %convolution_convert_fusion.5), channel_id=1, replica_groups=mesh['z'=8,'x'=4,'y'=8,'c'=2] {'y','c'}, dimensions={1}, use_global_device_ids=true | all-gather | bytes 557056 | tf_op jit(solution)/shard_map/all_gather | solution.py:263
  179.8 1.1 fusion.17
  181.7 0.7 broadcast_in_dim.160
  182.4 4.8 %all-to-all-start.4 = ((bf16[4,136,256]{2,1,0:T(8,128)(2,1)}), bf16[4,136,256]{2,1,0:T(8,128)(2,1)S(1)}, u32[]{:S(2)}, u32[]{:S(2)}) async-start(bf16[4,136,256]{2,1,0:T(8,128)(2,1)} %broadcast_in_dim.160), calls=%async_computation.4 | async-start | bytes 557056 | tf_op jit(solution)/shard_map/all_to_all | solution.py:43
  188.0 0.8 dynamic-slice_bitcast_fusion.2
  188.7 3.4 %collective-permute-start.2 = (bf16[8,64,256]{2,1,0:T(8,128)(2,1)}, bf16[8,64,256]{2,1,0:T(8,128)(2,1)S(1)}, u32[]{:S(2)}, u32[]{:S(2)}) collective-permute-start(bf16[8,64,256]{2,1,0:T(8,128)(2,1)} %get-tuple-element.32), channel_id=1, source_target_pairs={{0,16},{16,32},{32,48},{48,0},{1,17},{17,33},{33,49},{49,1},{2,18}... | collective-permute-start | bytes 786440 | tf_op jit(solution)/shard_map/ppermute | solution.py:307
  192.1 2.5 collective-permute-start.3
  194.6 4.5 %collective-permute-start.4 = (bf16[8,64,256]{2,1,0:T(8,128)(2,1)S(1)}, bf16[8,64,256]{2,1,0:T(8,128)(2,1)}, u32[]{:S(2)}, u32[]{:S(2)}) collective-permute-start(bf16[8,64,256]{2,1,0:T(8,128)(2,1)S(1)} %get-tuple-element.33), channel_id=1, source_target_pairs={{0,48},{16,0},{32,16},{48,32},{1,49},{17,1},{33,17},{49,33},{2,50}... | collective-permute-start | bytes 786440 | tf_op jit(solution)/shard_map/ppermute | solution.py:307
  199.2 0.8 collective-permute-done.2
  200.0 4.8 %collective-permute-done.3 = bf16[8,64,256]{2,1,0:T(8,128)(2,1)} collective-permute-done((bf16[8,64,256]{2,1,0:T(8,128)(2,1)S(1)}, bf16[8,64,256]{2,1,0:T(8,128)(2,1)}, u32[]{:S(2)}, u32[]{:S(2)}) %collective-permute-start.3) | collective-permute-done | bytes 262176 | tf_op jit(solution)/shard_map/ppermute | solution.py:307
  204.8 4.1 %collective-permute-done.4 = bf16[8,64,256]{2,1,0:T(8,128)(2,1)} collective-permute-done((bf16[8,64,256]{2,1,0:T(8,128)(2,1)S(1)}, bf16[8,64,256]{2,1,0:T(8,128)(2,1)}, u32[]{:S(2)}, u32[]{:S(2)}) %collective-permute-start.4) | collective-permute-done | bytes 262176 | tf_op jit(solution)/shard_map/ppermute | solution.py:307
  209.0 1.9 fusion.53
  210.8 5.8 %all-to-all-start.3 = ((bf16[8,64,256]{2,1,0:T(8,128)(2,1)}), bf16[8,64,256]{2,1,0:T(8,128)(2,1)S(1)}, u32[]{:S(2)}, u32[]{:S(2)}) async-start(bf16[8,64,256]{2,1,0:T(8,128)(2,1)} %fusion.53), calls=%async_computation.3 | async-start | bytes 524288 | tf_op jit(solution)/shard_map/all_to_all | solution.py:312
  216.8 11.9 %all-to-all-done.3 = bf16[8,64,256]{2,1,0:T(8,128)(2,1)S(1)} async-done(((bf16[8,64,256]{2,1,0:T(8,128)(2,1)}), bf16[8,64,256]{2,1,0:T(8,128)(2,1)S(1)}, u32[]{:S(2)}, u32[]{:S(2)}) %all-to-all-start.3) | async-done | bytes 262176 | tf_op jit(solution)/shard_map/all_to_all | solution.py:312
  228.7 0.8 broadcast_in_dim.161
  229.5 3.5 %all-to-all-start.5 = ((bf16[8,136,256]{2,1,0:T(8,128)(2,1)}), bf16[8,136,256]{2,1,0:T(8,128)(2,1)S(1)}, u32[]{:S(2)}, u32[]{:S(2)}) async-start(bf16[8,136,256]{2,1,0:T(8,128)(2,1)} %broadcast_in_dim.161), calls=%async_computation.5 | async-start | bytes 1114112 | tf_op jit(solution)/shard_map/all_to_all | solution.py:43
  233.1 5.0 %fusion.1 = f32[2,64,128]{2,1,0:T(8,128)S(1)} fusion(f32[2,64,128,64]{2,3,1,0:T(8,128)} %get-tuple-element.52, f32[2,64,128]{2,1,0:T(8,128)S(1)} %get-tuple-element.61, f32[2,64,64]{2,1,0:T(8,128)S(1)} %copy.72), kind=kLoop, calls=%fused_computation.3 | loop fusion | flops 3129344 | bytes 4358144 | tf_op jit(solution)/shard_map/nts,nsd,ntsd->ntd/dot_general | solution.py:109
  238.3 2.0 multiply_reduce_fusion
  240.9 9.2 %all-to-all-done.5 = bf16[8,136,256]{2,1,0:T(8,128)(2,1)S(1)} async-done(((bf16[8,136,256]{2,1,0:T(8,128)(2,1)}), bf16[8,136,256]{2,1,0:T(8,128)(2,1)S(1)}, u32[]{:S(2)}, u32[]{:S(2)}) %all-to-all-start.5) | async-done | bytes 557088 | tf_op jit(solution)/shard_map/all_to_all | solution.py:43
  250.7 0.9 multiply_subtract_fusion
  252.8 0.8 fusion.8
  (157 shorter events, 14.5 us)
Async XLA Ops:
  0.6 186.6 %copy-start = (bf16[128,256]{1,0:T(8,128)(2,1)S(1)}, bf16[128,256]{1,0:T(8,128)(2,1)}, u32[]{:S(2)}) copy-start(bf16[128,256]{1,0:T(8,128)(2,1)} %param.24) | copy-start | bytes 196612
  5.6 1.7 copy-start.26
  9.0 13.7 %copy-start.19 = (f32[128,128]{1,0:T(8,128)S(1)}, f32[128,128]{1,0:T(8,128)}, u32[]{:S(2)}) copy-start(f32[128,128]{1,0:T(8,128)} %param.28) | copy-start | bytes 196612
  9.0 54.2 %copy-start.2 = (bf16[1,2048,128]{2,1,0:T(8,128)(2,1)S(1)}, bf16[1,2048,128]{2,1,0:T(8,128)(2,1)}, u32[]{:S(2)}) copy-start(bf16[1,2048,128]{2,1,0:T(8,128)(2,1)} %param.21) | copy-start | bytes 1572868
  9.1 54.2 %copy-start.3 = (bf16[1,2048,128]{2,1,0:T(8,128)(2,1)S(1)}, bf16[1,2048,128]{2,1,0:T(8,128)(2,1)}, u32[]{:S(2)}) copy-start(bf16[1,2048,128]{2,1,0:T(8,128)(2,1)} %param.20) | copy-start | bytes 1572868
  9.1 52.2 %all-to-all-start = ((bf16[32,24,1024]{2,1,0:T(8,128)(2,1)}), bf16[32,24,1024]{2,1,0:T(8,128)(2,1)}, u32[]{:S(2)}, u32[]{:S(2)}) async-start(bf16[32,24,1024]{2,1,0:T(8,128)(2,1)} %bitcast.10), calls=%async_computation | async-start | bytes 3145728 | tf_op jit(solution)/shard_map/all_to_all | solution.py:181
  22.7 40.8 %copy-start.16 = (bf16[128,128]{1,0:T(8,128)(2,1)S(1)}, bf16[128,128]{1,0:T(8,128)(2,1)}, u32[]{:S(2)}) copy-start(bf16[128,128]{1,0:T(8,128)(2,1)} %param.25) | copy-start | bytes 98308
  22.7 40.8 %copy-start.8 = (bf16[128,128]{1,0:T(8,128)(2,1)S(1)}, bf16[128,128]{1,0:T(8,128)(2,1)}, u32[]{:S(2)}) copy-start(bf16[128,128]{1,0:T(8,128)(2,1)} %param.26) | copy-start | bytes 98308
  22.7 41.5 %copy-start.6 = (bf16[128,256]{1,0:T(8,128)(2,1)S(1)}, bf16[128,256]{1,0:T(8,128)(2,1)}, u32[]{:S(2)}) copy-start(bf16[128,256]{1,0:T(8,128)(2,1)} %param.27) | copy-start | bytes 196612
  22.7 41.7 %copy-start.5 = (f32[1,1,128,256]{3,2,1,0:T(8,128)S(1)}, f32[1,1,128,256]{3,2,1,0:T(8,128)}, u32[]{:S(2)}) copy-start(f32[1,1,128,256]{3,2,1,0:T(8,128)} %param.29) | copy-start | bytes 393220
  22.9 42.3 %copy-start.21 = (f32[2,1,128]{2,1,0:T(1,128)}, f32[2,1,128]{2,1,0:T(1,128)S(1)}, u32[]{:S(2)}) copy-start(f32[2,1,128]{2,1,0:T(1,128)S(1)} %get-tuple-element.59) | copy-start | bytes 3076
  22.9 42.2 %copy-start.7 = (bf16[1,128,2048]{2,1,0:T(8,128)(2,1)S(1)}, bf16[1,128,2048]{2,1,0:T(8,128)(2,1)}, u32[]{:S(2)}) copy-start(bf16[1,128,2048]{2,1,0:T(8,128)(2,1)} %param.22) | copy-start | bytes 1572868
  25.7 39.5 %copy-start.24 = (f32[128]{0:T(128)}, f32[128]{0:T(128)S(1)}, u32[]{:S(2)}) copy-start(f32[128]{0:T(128)S(1)} %get-tuple-element.54) | copy-start | bytes 1540
  61.3 5.5 %collective-permute-start = (bf16[768,1024]{1,0:T(8,128)(2,1)}, bf16[768,1024]{1,0:T(8,128)(2,1)S(1)}, u32[]{:S(2)}, u32[]{:S(2)}) collective-permute-start(bf16[768,1024]{1,0:T(8,128)(2,1)} %bitcast.11), channel_id=1, source_target_pairs={{0,1},{1,0},{2,3},{3,2},{4,5},{5,4},{6,7},{7,6},{8,9},{9,8},{10,11... | collective-permute-start | bytes 4718600 | tf_op jit(solution)/shard_map/ppermute | solution.py:184
  66.8 1.1 copy-start.31
  71.6 17.1 %copy-start.12 = (bf16[768,128]{1,0:T(8,128)(2,1)}, bf16[768,128]{1,0:T(8,128)(2,1)S(1)}, u32[]{:S(2)}) copy-start(bf16[768,128]{1,0:T(8,128)(2,1)S(1)} %get-tuple-element.26) | copy-start | bytes 589828
  71.6 17.1 %copy-start.14 = (bf16[768,128]{1,0:T(8,128)(2,1)}, bf16[768,128]{1,0:T(8,128)(2,1)S(1)}, u32[]{:S(2)}) copy-start(bf16[768,128]{1,0:T(8,128)(2,1)S(1)} %get-tuple-element.27) | copy-start | bytes 589828
  71.6 3.9 %copy-start.20 = (bf16[64,256]{1,0:T(8,128)(2,1)S(1)}, bf16[64,256]{1,0:T(8,128)(2,1)}, u32[]{:S(2)}) copy-start(bf16[64,256]{1,0:T(8,128)(2,1)} %param.23) | copy-start | bytes 98308
  72.0 17.9 %copy-start.9 = (f32[2,128,64]{1,2,0:T(8,128)S(1)}, f32[2,128,64]{1,2,0:T(8,128)}, u32[]{:S(2)}) copy-start(f32[2,128,64]{1,2,0:T(8,128)} %get-tuple-element.60) | copy-start | bytes 196612
  73.3 23.2 %collective-permute-start.1 = (bf16[384,1024]{1,0:T(8,128)(2,1)}, bf16[384,1024]{1,0:T(8,128)(2,1)S(1)}, u32[]{:S(2)}, u32[]{:S(2)}) collective-permute-start(bf16[384,1024]{1,0:T(8,128)(2,1)} %convolution_convert_fusion.2), channel_id=1, source_target_pairs={{0,1},{1,0},{2,3},{3,2},{4,5},{5,4},{6,7},{7,6},{8,9},{9,8},{10,11... | collective-permute-start | bytes 2359304 | tf_op jit(solution)/shard_map/ppermute | solution.py:223
  89.9 5.2 %copy-start.11 = (bf16[768,128]{1,0:T(8,128)(2,1)S(1)}, bf16[768,128]{1,0:T(8,128)(2,1)}, u32[]{:S(2)}) copy-start(bf16[768,128]{1,0:T(8,128)(2,1)} %get-tuple-element.24) | copy-start | bytes 589828
  89.9 5.2 %copy-start.32 = (bf16[768,1024]{1,0:T(8,128)(2,1)S(1)}, bf16[768,1024]{1,0:T(8,128)(2,1)}, u32[]{:S(2)}) copy-start(bf16[768,1024]{1,0:T(8,128)(2,1)} %copy-done.31) | copy-start | bytes 4718596
  98.1 9.3 %copy-start.13 = (bf16[768,128]{1,0:T(8,128)(2,1)S(1)}, bf16[768,128]{1,0:T(8,128)(2,1)}, u32[]{:S(2)}) copy-start(bf16[768,128]{1,0:T(8,128)(2,1)} %copy-done.12) | copy-start | bytes 589828
  98.1 29.7 %all-to-all-start.1 = ((bf16[8,384,128]{2,1,0:T(8,128)(2,1)}), bf16[8,384,128]{2,1,0:T(8,128)(2,1)S(1)}, u32[]{:S(2)}, u32[]{:S(2)}) async-start(bf16[8,384,128]{2,1,0:T(8,128)(2,1)} %bitcast.328), calls=%async_computation.1 | async-start | bytes 1572864 | tf_op jit(solution)/shard_map/all_to_all | solution.py:226
  105.3 2.0 copy-start.15
  105.3 2.0 copy-start.33
  110.0 27.7 %collective-permute-start.5 = (bf16[256,256]{1,0:T(8,128)(2,1)S(1)}, bf16[256,256]{1,0:T(8,128)(2,1)}, u32[]{:S(2)}, u32[]{:S(2)}) collective-permute-start(bf16[256,256]{1,0:T(8,128)(2,1)S(1)} %all_gather.7), channel_id=1, source_target_pairs={{0,64},{64,128},{128,192},{192,256},{256,320},{320,384},{384,448},... | collective-permute-start | bytes 393224 | tf_op jit(solution)/shard_map/ppermute | solution.py:233
  112.5 31.6 %collective-permute-start.6 = (bf16[256,256]{1,0:T(8,128)(2,1)S(1)}, bf16[256,256]{1,0:T(8,128)(2,1)}, u32[]{:S(2)}, u32[]{:S(2)}) collective-permute-start(bf16[256,256]{1,0:T(8,128)(2,1)S(1)} %all_gather.7), channel_id=1, source_target_pairs={{0,448},{64,0},{128,64},{192,128},{256,192},{320,256},{384,320},{4... | collective-permute-start | bytes 393224 | tf_op jit(solution)/shard_map/ppermute | solution.py:233
  117.9 34.0 %collective-permute-start.7 = (bf16[256,256]{1,0:T(8,128)(2,1)S(1)}, bf16[256,256]{1,0:T(8,128)(2,1)S(1)}, u32[]{:S(2)}, u32[]{:S(2)}) collective-permute-start(bf16[256,256]{1,0:T(8,128)(2,1)S(1)} %all_gather.7), channel_id=1, source_target_pairs={{0,128},{64,192},{128,256},{192,320},{256,384},{320,448},{384,0},{... | collective-permute-start | bytes 393224 | tf_op jit(solution)/shard_map/ppermute | solution.py:233
  119.8 33.3 %collective-permute-start.8 = (bf16[256,256]{1,0:T(8,128)(2,1)S(1)}, bf16[256,256]{1,0:T(8,128)(2,1)}, u32[]{:S(2)}, u32[]{:S(2)}) collective-permute-start(bf16[256,256]{1,0:T(8,128)(2,1)S(1)} %all_gather.7), channel_id=1, source_target_pairs={{0,384},{64,448},{128,0},{192,64},{256,128},{320,192},{384,256},{4... | collective-permute-start | bytes 393224 | tf_op jit(solution)/shard_map/ppermute | solution.py:233
  125.8 29.1 %collective-permute-start.9 = (bf16[256,256]{1,0:T(8,128)(2,1)S(1)}, bf16[256,256]{1,0:T(8,128)(2,1)}, u32[]{:S(2)}, u32[]{:S(2)}) collective-permute-start(bf16[256,256]{1,0:T(8,128)(2,1)S(1)} %all_gather.7), channel_id=1, source_target_pairs={{0,192},{64,256},{128,320},{192,384},{256,448},{320,0},{384,64},{4... | collective-permute-start | bytes 393224 | tf_op jit(solution)/shard_map/ppermute | solution.py:233
  128.5 31.2 %all-to-all-start.2 = ((bf16[32,12,128]{2,1,0:T(8,128)(2,1)}), bf16[32,12,128]{2,1,0:T(8,128)(2,1)S(1)}, u32[]{:S(2)}, u32[]{:S(2)}) async-start(bf16[32,12,128]{2,1,0:T(8,128)(2,1)} %reshape.632), calls=%async_computation.2 | async-start | bytes 262144 | tf_op jit(solution)/shard_map/all_to_all | solution.py:255
  137.7 19.0 %collective-permute-start.10 = (bf16[256,256]{1,0:T(8,128)(2,1)S(1)}, bf16[256,256]{1,0:T(8,128)(2,1)}, u32[]{:S(2)}, u32[]{:S(2)}) collective-permute-start(bf16[256,256]{1,0:T(8,128)(2,1)S(1)} %all_gather.7), channel_id=1, source_target_pairs={{0,320},{64,384},{128,448},{192,0},{256,64},{320,128},{384,192},{4... | collective-permute-start | bytes 393224 | tf_op jit(solution)/shard_map/ppermute | solution.py:233
  144.1 14.4 %collective-permute-start.11 = (bf16[256,256]{1,0:T(8,128)(2,1)S(1)}, bf16[256,256]{1,0:T(8,128)(2,1)S(1)}, u32[]{:S(2)}, u32[]{:S(2)}) collective-permute-start(bf16[256,256]{1,0:T(8,128)(2,1)S(1)} %all_gather.7), channel_id=1, source_target_pairs={{0,256},{64,320},{128,384},{192,448},{256,0},{320,64},{384,128},{4... | collective-permute-start | bytes 393224 | tf_op jit(solution)/shard_map/ppermute | solution.py:233
  148.5 31.0 %copy-start.1 = (bf16[128,2048]{1,0:T(8,128)(2,1)S(1)}, bf16[128,2048]{1,0:T(8,128)(2,1)}, u32[]{:S(2)}) copy-start(bf16[128,2048]{1,0:T(8,128)(2,1)} %param.15) | copy-start | bytes 1572868
  148.5 31.0 %copy-start.18 = (f32[2048]{0:T(1024)S(1)}, f32[2048]{0:T(1024)}, u32[]{:S(2)}) copy-start(f32[2048]{0:T(1024)} %param.16) | copy-start | bytes 24580
  148.5 31.0 %copy-start.27 = (f32[128]{0:T(128)S(1)}, f32[128]{0:T(128)}, u32[]{:S(2)}) copy-start(f32[128]{0:T(128)} %copy-done.26) | copy-start | bytes 1540
  153.1 26.7 %copy-start.4 = (bf16[128,2048]{1,0:T(8,128)(2,1)S(1)}, bf16[128,2048]{1,0:T(8,128)(2,1)}, u32[]{:S(2)}) copy-start(bf16[128,2048]{1,0:T(8,128)(2,1)} %param.17) | copy-start | bytes 1572868
  180.9 0.7 copy-start.25
  180.9 0.7 copy-start.30
  180.9 0.8 copy-start.29
  182.4 16.7 %all-to-all-start.4 = ((bf16[4,136,256]{2,1,0:T(8,128)(2,1)}), bf16[4,136,256]{2,1,0:T(8,128)(2,1)S(1)}, u32[]{:S(2)}, u32[]{:S(2)}) async-start(bf16[4,136,256]{2,1,0:T(8,128)(2,1)} %broadcast_in_dim.160), calls=%async_computation.4 | async-start | bytes 557056 | tf_op jit(solution)/shard_map/all_to_all | solution.py:43
  188.7 11.3 %collective-permute-start.2 = (bf16[8,64,256]{2,1,0:T(8,128)(2,1)}, bf16[8,64,256]{2,1,0:T(8,128)(2,1)S(1)}, u32[]{:S(2)}, u32[]{:S(2)}) collective-permute-start(bf16[8,64,256]{2,1,0:T(8,128)(2,1)} %get-tuple-element.32), channel_id=1, source_target_pairs={{0,16},{16,32},{32,48},{48,0},{1,17},{17,33},{33,49},{49,1},{2,18}... | collective-permute-start | bytes 786440 | tf_op jit(solution)/shard_map/ppermute | solution.py:307
  192.1 12.7 %collective-permute-start.3 = (bf16[8,64,256]{2,1,0:T(8,128)(2,1)S(1)}, bf16[8,64,256]{2,1,0:T(8,128)(2,1)}, u32[]{:S(2)}, u32[]{:S(2)}) collective-permute-start(bf16[8,64,256]{2,1,0:T(8,128)(2,1)S(1)} %get-tuple-element.34), channel_id=1, source_target_pairs={{0,32},{16,48},{32,0},{48,16},{1,33},{17,49},{33,1},{49,17},{2,34}... | collective-permute-start | bytes 786440 | tf_op jit(solution)/shard_map/ppermute | solution.py:307
  194.6 14.3 %collective-permute-start.4 = (bf16[8,64,256]{2,1,0:T(8,128)(2,1)S(1)}, bf16[8,64,256]{2,1,0:T(8,128)(2,1)}, u32[]{:S(2)}, u32[]{:S(2)}) collective-permute-start(bf16[8,64,256]{2,1,0:T(8,128)(2,1)S(1)} %get-tuple-element.33), channel_id=1, source_target_pairs={{0,48},{16,0},{32,16},{48,32},{1,49},{17,1},{33,17},{49,33},{2,50}... | collective-permute-start | bytes 786440 | tf_op jit(solution)/shard_map/ppermute | solution.py:307
  210.8 17.8 %all-to-all-start.3 = ((bf16[8,64,256]{2,1,0:T(8,128)(2,1)}), bf16[8,64,256]{2,1,0:T(8,128)(2,1)S(1)}, u32[]{:S(2)}, u32[]{:S(2)}) async-start(bf16[8,64,256]{2,1,0:T(8,128)(2,1)} %fusion.53), calls=%async_computation.3 | async-start | bytes 524288 | tf_op jit(solution)/shard_map/all_to_all | solution.py:312
  229.5 20.5 %all-to-all-start.5 = ((bf16[8,136,256]{2,1,0:T(8,128)(2,1)}), bf16[8,136,256]{2,1,0:T(8,128)(2,1)S(1)}, u32[]{:S(2)}, u32[]{:S(2)}) async-start(bf16[8,136,256]{2,1,0:T(8,128)(2,1)} %broadcast_in_dim.161), calls=%async_computation.5 | async-start | bytes 1114112 | tf_op jit(solution)/shard_map/all_to_all | solution.py:43
  233.1 5.0 %copy-start.10 = (bf16[1,128,256]{2,1,0:T(8,128)(2,1)S(1)}, bf16[1,128,256]{2,1,0:T(8,128)(2,1)}, u32[]{:S(2)}) copy-start(bf16[1,128,256]{2,1,0:T(8,128)(2,1)} %multiply_add_fusion.3) | copy-start | bytes 196612
  238.2 12.2 %copy-start.22 = (f32[2,1,128]{2,1,0:T(1,128)S(1)}, f32[2,1,128]{2,1,0:T(1,128)}, u32[]{:S(2)}) copy-start(f32[2,1,128]{2,1,0:T(1,128)} %copy-done.21) | copy-start | bytes 3076
  238.2 12.2 %copy-start.23 = (f32[2,128]{1,0:T(2,128)S(1)}, f32[2,128]{1,0:T(2,128)}, u32[]{:S(2)}) copy-start(f32[2,128]{1,0:T(2,128)} %subtract_exponential_fusion.1) | copy-start | bytes 3076
  238.2 12.4 %copy-start.17 = (bf16[128,128]{1,0:T(8,128)(2,1)S(1)}, bf16[128,128]{1,0:T(8,128)(2,1)}, u32[]{:S(2)}) copy-start(bf16[128,128]{1,0:T(8,128)(2,1)} %param.25) | copy-start | bytes 98308
  240.2 11.5 %copy-start.28 = (f32[128]{0:T(128)S(1)}, f32[128]{0:T(128)}, u32[]{:S(2)}) copy-start(f32[128]{0:T(128)} %get-tuple-element.53) | copy-start | bytes 1540

commit v4 on v3

--- a/solution.py
+++ b/solution.py
@@ -1,13 +1,15 @@
 import jax
 import jax.numpy as jnp
 from jax import lax
+from jax.experimental import pallas as pl
+from jax.experimental.pallas import tpu as pltpu
 from jax.sharding import Mesh
 from jax.sharding import PartitionSpec as P
 
 
 KEY_CHANNELS = 128
 DV = 256
-TOP = 2
+CAPACITY = 12
 BLOCK = 64
 SP = ("z", "x")
 TP = ("y", "c")
@@ -124,6 +126,127 @@
         grad_key.reshape(length, key_width),
         grad_value.reshape(length, value_rows.shape[1]),
         grad_log,
+    )
+
+
+def dispatch_rows_kernel(core_ref, ids_ref, weight_ref, resid_ref, cot_ref, gain_ref, sent_ref, slot_ref, rows_ref):
+    tokens, model_width = resid_ref.shape
+    half = model_width // 2
+    experts = sent_ref.shape[0] // (2 * CAPACITY)
+
+    square = (tokens, tokens)
+    row_at = lax.broadcasted_iota(jnp.int32, square, 0)
+    col_at = lax.broadcasted_iota(jnp.int32, square, 1)
+    along = [ids_ref[k : k + 1, :].astype(jnp.float32) for k in range(2)]
+
+    @pl.when(core_ref[0] == 0)
+    def _():
+        for at in range(0, tokens, 32):
+            r = resid_ref[at : at + 32, :].astype(jnp.float32)
+            inverse_rms = lax.rsqrt(jnp.mean(r * r, axis=1, keepdims=True) + epsilon)
+            normed = (r * inverse_rms * gain_ref[...]).astype(jnp.bfloat16)
+            for k in range(2):
+                for h in range(2):
+                    low = (2 * k + h) * tokens + at
+                    rows_ref[low : low + 32, :] = normed[:, h * half : (h + 1) * half]
+
+    @pl.when(core_ref[0] != 0)
+    def _():
+        weights = []
+        for k in range(2):
+            spread = jnp.broadcast_to(weight_ref[k : k + 1, :], square)
+            weights.append(
+                jnp.sum(jnp.where(row_at == col_at, spread, 0.0), axis=1, keepdims=True)
+            )
+        for at in range(0, tokens, 32):
+            c = cot_ref[at : at + 32, :].astype(jnp.float32)
+            for k in range(2):
+                sent = (c * weights[k][at : at + 32, :]).astype(jnp.bfloat16)
+                for h in range(2):
+                    low = (2 * k + h) * tokens + at
+                    rows_ref[low : low + 32, :] = sent[:, h * half : (h + 1) * half]
+
+    expert_at = lax.broadcasted_iota(jnp.int32, (experts, tokens), 0).astype(jnp.float32)
+    named = [(expert_at == a).astype(jnp.float32) for a in along]
+    earlier = (row_at < col_at).astype(jnp.bfloat16)
+    before = jnp.dot(
+        (named[0] + named[1]).astype(jnp.bfloat16), earlier, preferred_element_type=jnp.float32
+    )
+    slots = [
+        (a * CAPACITY + jnp.sum(n * before, axis=0, keepdims=True)).astype(jnp.int32)
+        for a, n in zip(along, named)
+    ]
+    slot_ref[...] = jnp.concatenate(slots + [jnp.zeros((6, tokens), jnp.int32)], axis=0)
+    step = 256
+    for at in range(0, sent_ref.shape[0], step):
+        packed = lax.broadcasted_iota(jnp.int32, (step, tokens), 0) + at
+        hits = [
+            jnp.where(packed == 2 * slot + h, 1.0, 0.0).astype(jnp.bfloat16)
+            for slot in slots
+            for h in range(2)
+        ]
+        sent_ref[at : at + step, :] = jnp.dot(
+            jnp.concatenate(hits, axis=1), rows_ref[...], preferred_element_type=jnp.float32
+        ).astype(jnp.bfloat16)
+
+
+def dispatch_rows(core, ids, weight, resid, cotangent, gain, experts):
+    tokens, model_width = resid.shape
+    half = model_width // 2
+    vmem = pl.BlockSpec(memory_space=pltpu.VMEM)
+    return pl.pallas_call(
+        dispatch_rows_kernel,
+        out_shape=(
+            jax.ShapeDtypeStruct((2 * experts * CAPACITY, half), jnp.bfloat16),
+            jax.ShapeDtypeStruct((8, tokens), jnp.int32),
+        ),
+        in_specs=[pl.BlockSpec(memory_space=pltpu.SMEM)] + [vmem] * 5,
+        out_specs=(vmem, vmem),
+        scratch_shapes=[pltpu.VMEM((4 * tokens, half), jnp.bfloat16)],
+        name="dispatch_rows",
+    )(core.astype(jnp.int32).reshape(1), ids.T, weight.T, resid, cotangent, gain.reshape(1, -1))
+
+
+def resid_mixed_kernel(place_ref, normed_ref, cot_ref, resid_ref, gain_ref, *refs):
+    blocks, (out_ref, mixed_ref) = refs[:8], refs[8:]
+    tokens = resid_ref.shape[0]
+    for at in range(0, tokens, 32):
+        rows = slice(at, at + 32)
+        r = resid_ref[rows, :].astype(jnp.float32)
+        inverse_rms = lax.rsqrt(jnp.mean(r * r, axis=1, keepdims=True) + epsilon)
+        unit = r * inverse_rms
+        scaled = normed_ref[rows, :].astype(jnp.float32) * gain_ref[...]
+        mean = jnp.mean(scaled * unit, axis=1, keepdims=True)
+        grad = cot_ref[rows, :].astype(jnp.float32) + inverse_rms * (scaled - unit * mean)
+        out_ref[rows, :] = grad.astype(jnp.bfloat16)
+    depth = blocks[0].shape[0]
+    total = jnp.zeros(mixed_ref.shape, jnp.float32)
+    for k in range(8):
+        at = pl.multiple_of(jnp.bitwise_and(place_ref[0] + (8 - k), 7) * depth, depth)
+        total = total + jnp.dot(
+            out_ref[:, pl.ds(at, depth)], blocks[k][...], preferred_element_type=jnp.float32
+        )
+    mixed_ref[...] = total.astype(jnp.bfloat16)
+
+
+def resid_mixed(place, grad_normed, cotangent, resid, gain, blocks):
+    vmem = pl.BlockSpec(memory_space=pltpu.VMEM)
+    return pl.pallas_call(
+        resid_mixed_kernel,
+        out_shape=(
+            jax.ShapeDtypeStruct(resid.shape, jnp.bfloat16),
+            jax.ShapeDtypeStruct((resid.shape[0], blocks[0].shape[1]), jnp.bfloat16),
+        ),
+        in_specs=[pl.BlockSpec(memory_space=pltpu.SMEM)] + [vmem] * 12,
+        out_specs=(vmem, vmem),
+        name="resid_mixed",
+    )(
+        place.astype(jnp.int32).reshape(1),
+        grad_normed,
+        cotangent,
+        resid,
+        gain.reshape(1, -1),
+        *blocks,
     )
 
 
@@ -150,34 +273,14 @@
     sp_count = lax.axis_size(SP)
     y_count = lax.axis_size("y")
     experts = sp_count * expert_gate.shape[0]
-    capacity = 3 * tokens_here // experts
+    capacity = CAPACITY
     slots = experts * capacity
     core = lax.axis_index("c")
-    resid_f = resid.astype(jnp.float32)
-    inverse_rms = lax.rsqrt(jnp.mean(resid_f * resid_f, axis=1, keepdims=True) + epsilon)
-    unit_rows = resid_f * inverse_rms
-    normed = (unit_rows * norm_gain).astype(jnp.bfloat16)
-    pair_expert = route_ids.reshape(-1)
-    onehot = (pair_expert[:, None] == jnp.arange(experts, dtype=jnp.int32)[None, :]).astype(
-        jnp.int32
-    )
-    slot_rank = jnp.sum((jnp.cumsum(onehot, axis=0) - onehot) * onehot, axis=1)
-    slot_of = (pair_expert * capacity + slot_rank).reshape(tokens_here, TOP)
-    slot_a, slot_b = slot_of[:, 0], slot_of[:, 1]
-    packed = lax.broadcasted_iota(jnp.int32, (2 * slots, 2 * tokens_here), 0)
-    aim_a = jnp.concatenate([2 * slot_a, 2 * slot_a + 1])[None, :]
-    aim_b = jnp.concatenate([2 * slot_b, 2 * slot_b + 1])[None, :]
-    hit_a, hit_b = packed == aim_a, packed == aim_b
-    weight_a = jnp.concatenate([route_weight[:, 0]] * 2)[None, :]
-    weight_b = jnp.concatenate([route_weight[:, 1]] * 2)[None, :]
-    slot_weight = jnp.sum(
-        jnp.where(hit_a, weight_a, 0.0) + jnp.where(hit_b, weight_b, 0.0), axis=1, keepdims=True
-    )
-    scale = jnp.where(core == 0, 1.0, slot_weight)
-    chosen = jnp.where(core == 0, normed, cotangent)
-    rows_two = jnp.concatenate([chosen[:, :half], chosen[:, half:]], axis=0)
-    sent = jnp.dot((hit_a | hit_b).astype(jnp.bfloat16), rows_two, preferred_element_type=jnp.float32)
-    sent = (sent * scale).astype(jnp.bfloat16).reshape(sp_count, 2 * capacity, half)
+    sent, slot_rows = dispatch_rows(
+        core, route_ids, route_weight, resid, cotangent, norm_gain, experts
+    )
+    slot_a, slot_b = slot_rows[0], slot_rows[1]
+    sent = sent.reshape(sp_count, 2 * capacity, half)
     own = lax.all_to_all(sent, SP, 0, 0, tiled=True).reshape(2 * slots, half)
     proj_near, _ = lax.optimization_barrier((out_proj, sent))
     proj_near = lax.all_gather(proj_near, "x", axis=0, tiled=True)
@@ -227,23 +330,15 @@
     summed = sum_parts(swapped).astype(jnp.bfloat16)
     proj_tied, _ = lax.optimization_barrier((proj_near, parts))
     z_place = lax.axis_index("z")
-    blocks = [(0, proj_near)]
-    for k in (1, 7, 2, 6, 3, 5, 4):
-        ring = [(i, (i + k) % 8) for i in range(8)]
-        blocks.append((k, lax.ppermute(proj_tied, "z", ring)))
-    out_proj_all = jnp.zeros((model_width, out_proj.shape[1]), out_proj.dtype)
-    for k, block in blocks:
-        at = jnp.bitwise_and(z_place + (8 - k), 7) * block.shape[0]
-        out_proj_all = lax.dynamic_update_slice(
-            out_proj_all, block, (at.astype(jnp.uint32), jnp.uint32(0))
-        )
+    blocks = [proj_near] + [None] * 7
+    for k in range(1, 8):
+        blocks[k] = lax.ppermute(proj_tied, "z", [(i, (i + k) % 8) for i in range(8)])
 
     def beside(values):
         return jnp.concatenate([values, jnp.roll(values, 1, axis=0)], axis=1)
 
     grad_in_w = named_dot(
-        rows_in,
-        jnp.concatenate([beside(grad_gate_act), beside(grad_up_act)], axis=1),
+        rows_in, jnp.concatenate([beside(grad_gate_act), beside(grad_up_act)], axis=1)
     )
     grad_gate_w = jnp.concatenate([grad_in_w[:, :width], grad_in_w[:, width : 2 * width]], axis=0)
     grad_up_w = jnp.concatenate(
@@ -267,14 +362,9 @@
         ("y", "c"),
         axis=1,
         tiled=True,
-    ).astype(jnp.float32)
-    scaled = grad_normed * norm_gain
-    grad_resid = cotangent.astype(jnp.float32) + inverse_rms * (
-        scaled - unit_rows * jnp.mean(scaled * unit_rows, axis=1, keepdims=True)
-    )
-    grad_resid = grad_resid.astype(jnp.bfloat16)
-    grad_mixed = jnp.dot(grad_resid, out_proj_all, preferred_element_type=jnp.float32).astype(
-        jnp.bfloat16
+    )
+    grad_resid, grad_mixed = resid_mixed(
+        z_place, grad_normed, cotangent, resid, norm_gain, blocks
     )
     share = lax.dot_general(
         grad_resid, mixed, (((0,), (0,)), ((), ())), preferred_element_type=jnp.float32
@@ -288,7 +378,8 @@
         query_rows, key_rows, value_rows, grad_rows, log_decay, span_state[0, 0]
     )
     own_decay, own_state = summary
-    near_states, near_decays = split_decay(to_all(with_decay(own_state, own_decay), "x"))
+    near_filled = to_all(with_decay(own_state, own_decay), "x")
+    near_states, near_decays = split_decay(near_filled)
     near_sum, near_factor = later_sum(near_states, near_decays, lax.axis_index("x"))
     group_sum, group_factor = later_sum(near_states, near_decays, -1)
     far_filled = to_all(with_decay(group_sum, group_factor), "z")

time: 255 us -> 251 us (0.984)
  the two profiles are of different devices: /device:TPU:2 before, /device:TPU:1 now
where the time goes in v4:
time: 251 us; the launch traced here: 250 us
  waiting for transfers between devices  87.2 us (35%)
  starting transfers between devices  82.6 us (33%)
  blocking collectives  30.3 us (12%)
  other arithmetic  20.8 us (8%)
  matrix products  14.4 us (6%)
  Pallas kernels  7.01 us (3%)
  local copies, waits for them, and re-layouts  6.23 us (2%)
    all_to_all x1, waiting for transfers between devices, on_device_body(): own = lax.all_to_all(sent, SP, 0, 0, tiled=True).reshape(2 * slots, half)  36.5 us
    ppermute x7, starting transfers between devices, on_device_body(): lax.ppermute(proj_tied, 'z', [(i, (i + k) % 8) for i in range(8)])  28 us
    all_gather x1, blocking collectives, on_device_body(): lax.all_gather(lax.dot_general(slot_tokens, flat_rows, (((0,), (0,)), (()...  20.3 us
    all_to_all x1, waiting for transfers between devices, on_device_body(): swapped = lax.all_to_all(parts, 'y', 0, 0, tiled=True)  17.3 us
    all_to_all x1, starting transfers between devices, on_device_body(): own = lax.all_to_all(sent, SP, 0, 0, tiled=True).reshape(2 * slots, half)  14 us
    all_to_all x1, waiting for transfers between devices, on_device_body(): share_z = lax.all_to_all(share_z, 'z', 0, 0, tiled=True)  11.6 us
    ppermute x3, waiting for transfers between devices, on_device_body(): lax.ppermute(for_place(k), 'x', [(i, (i + k) % 4) for i in range(4)])  11.1 us
    all_to_all x2, waiting for transfers between devices, to_all(): return lax.all_to_all(copies, axis, 0, 0, tiled=True)  10.7 us
  transfers between devices with their start and end apart: 18, of which 6 were waited for; matrix products, arithmetic and copies ran while one was open for 10% of the time, Pallas kernels for 0%

profile of v4, /device:TPU:1, one launch (start us, length us, event | category | flops | bytes accessed | tf_op | source)
XLA Modules:
  0.0 250.2 jit_solution(778502234707832908)
XLA Ops:
  0.7 3.8 %dispatch_rows.1 = (bf16[768,1024]{1,0:T(8,128)(2,1)}, s32[8,128]{1,0:T(8,128)}) custom-call(s32[1]{0:T(128)} %bitcast.5.core_ref, s32[2,128]{1,0:T(2,128)} %bitcast.340, f32[2,128]{1,0:T(2,128)} %bitcast.341, bf16[128,2048]{1,0:T(8,128)(2,1)} %resid_ref.3, bf16[128,2048]{1,0:T(8,128)(2,1)} %cot_ref.3, f32[1,2048]{1,0:T(1,128)} %bitcast.332), custom_call_target="tpu_custom_call" | custom-call | tf_op jit(solution)/shard_map/dispatch_rows/pallas_call | solution.py:197
  4.5 14.0 %all-to-all-start = ((bf16[32,24,1024]{2,1,0:T(8,128)(2,1)}), bf16[32,24,1024]{2,1,0:T(8,128)(2,1)}, u32[]{:S(2)}, u32[]{:S(2)}) async-start(bf16[32,24,1024]{2,1,0:T(8,128)(2,1)} %bitcast.310), calls=%async_computation | async-start | bytes 3145728 | tf_op jit(solution)/shard_map/all_to_all | solution.py:284
  18.8 0.5 subtract_exponential_fusion.1
  19.3 0.5 fusion.122
  19.8 36.5 %all-to-all-done = bf16[32,24,1024]{2,1,0:T(8,128)(2,1)} async-done(((bf16[32,24,1024]{2,1,0:T(8,128)(2,1)}), bf16[32,24,1024]{2,1,0:T(8,128)(2,1)}, u32[]{:S(2)}, u32[]{:S(2)}) %all-to-all-start) | async-done | bytes 1572896 | tf_op jit(solution)/shard_map/all_to_all | solution.py:284
  56.4 4.1 %collective-permute-start = (bf16[768,1024]{1,0:T(8,128)(2,1)}, bf16[768,1024]{1,0:T(8,128)(2,1)}, u32[]{:S(2)}, u32[]{:S(2)}) collective-permute-start(bf16[768,1024]{1,0:T(8,128)(2,1)} %bitcast.10), channel_id=1, source_target_pairs={{0,1},{1,0},{2,3},{3,2},{4,5},{5,4},{6,7},{7,6},{8,9},{9,8},{10,11... | collective-permute-start | bytes 4718600 | tf_op jit(solution)/shard_map/ppermute | solution.py:287
  60.5 10.0 %all_gather.7.refs_0_ = bf16[256,256]{1,0:T(8,128)(2,1)S(1)} all-gather(bf16[64,256]{1,0:T(8,128)(2,1)S(1)} %copy-done.23), channel_id=1, replica_groups=mesh['z'=8,'x'=4,'y'=8,'c'=2] {'x'}, dimensions={0}, use_global_device_ids=true | all-gather | bytes 163840 | tf_op jit(solution)/shard_map/all_gather | solution.py:286
  70.5 0.3 broadcast_select_fusion.6
  70.8 0.8 slice_bitcast_fusion.12
  72.0 2.4 fusion.9
  74.5 2.0 fusion.29
  76.8 0.3 select_convert_fusion.2
  77.1 0.4 fusion.4
  77.5 0.4 convolution_convert_fusion.2
  77.9 4.7 %collective-permute-start.1 = (bf16[384,1024]{1,0:T(8,128)(2,1)S(1)}, bf16[384,1024]{1,0:T(8,128)(2,1)S(1)}, u32[]{:S(2)}, u32[]{:S(2)}) collective-permute-start(bf16[384,1024]{1,0:T(8,128)(2,1)S(1)} %convolution_convert_fusion.2), channel_id=1, source_target_pairs={{0,1},{1,0},{2,3},{3,2},{4,5},{5,4},{6,7},{7,6},{8,9},{9,8},{10,11... | collective-permute-start | bytes 2359304 | tf_op jit(solution)/shard_map/ppermute | solution.py:326
  82.6 0.7 multiply_add_fusion.3
  83.3 3.7 %fusion = (bf16[2,64,64]{2,1,0:T(8,128)(2,1)S(1)}, f32[2,64,128,64]{2,3,1,0:T(8,128)}) fusion(f32[2,128,64]{1,2,0:T(8,128)S(1)} %get-tuple-element.66, f32[2,128,64]{1,2,0:T(8,128)S(1)} %bitcast.316, f32[2,64,128]{2,1,0:T(8,128)S(1)} %reduce_window_sum.33, pred[64,64]{1,0:T(8,128)(4,1)S(1)} %iota_compare_fusion.8), kind=kLoop, calls=%fused_computation.1 | loop fusion | flops 5234688 | bytes 4411392 | tf_op jit(solution)/shard_map/ntd,nsd,ntsd->nts/dot_general | solution.py:108
  87.1 0.4 fusion.17
  87.5 1.1 copy.61
  88.6 6.8 %all-to-all-start.1 = ((bf16[8,384,128]{2,1,0:T(8,128)(2,1)}), bf16[8,384,128]{2,1,0:T(8,128)(2,1)S(1)}, u32[]{:S(2)}, u32[]{:S(2)}) async-start(bf16[8,384,128]{2,1,0:T(8,128)(2,1)} %bitcast.300), calls=%async_computation.1 | async-start | bytes 1572864 | tf_op jit(solution)/shard_map/all_to_all | solution.py:329
  95.4 2.4 convolution_convert_fusion.1
  98.1 0.8 maximum_bitcast_fusion
  98.9 0.8 maximum_bitcast_fusion.1
  99.7 2.0 convolution_convert_fusion.3
  101.8 17.3 %all-to-all-done.1 = bf16[8,384,128]{2,1,0:T(8,128)(2,1)S(1)} async-done(((bf16[8,384,128]{2,1,0:T(8,128)(2,1)}), bf16[8,384,128]{2,1,0:T(8,128)(2,1)S(1)}, u32[]{:S(2)}, u32[]{:S(2)}) %all-to-all-start.1) | async-done | bytes 786464 | tf_op jit(solution)/shard_map/all_to_all | solution.py:329
  119.2 0.7 reshape.601
  119.8 4.3 %all-to-all-start.2 = ((bf16[32,12,128]{2,1,0:T(8,128)(2,1)}), bf16[32,12,128]{2,1,0:T(8,128)(2,1)S(1)}, u32[]{:S(2)}, u32[]{:S(2)}) async-start(bf16[32,12,128]{2,1,0:T(8,128)(2,1)} %reshape.601), calls=%async_computation.2 | async-start | bytes 262144 | tf_op jit(solution)/shard_map/all_to_all | solution.py:350
  124.1 0.8 maximum_bitcast_fusion.2
  125.0 3.1 %collective-permute-start.2 = (bf16[256,256]{1,0:T(8,128)(2,1)S(1)}, bf16[256,256]{1,0:T(8,128)(2,1)S(1)}, u32[]{:S(2)}, u32[]{:S(2)}) collective-permute-start(bf16[256,256]{1,0:T(8,128)(2,1)S(1)} %all_gather.7.refs_0_), channel_id=1, source_target_pairs={{0,64},{64,128},{128,192},{192,256},{256,320},{320,384},{384,448},... | collective-permute-start | bytes 393224 | tf_op jit(solution)/shard_map/ppermute | solution.py:335
  128.1 4.0 %collective-permute-start.3 = (bf16[256,256]{1,0:T(8,128)(2,1)S(1)}, bf16[256,256]{1,0:T(8,128)(2,1)S(1)}, u32[]{:S(2)}, u32[]{:S(2)}) collective-permute-start(bf16[256,256]{1,0:T(8,128)(2,1)S(1)} %all_gather.7.refs_0_), channel_id=1, source_target_pairs={{0,128},{64,192},{128,256},{192,320},{256,384},{320,448},{384,0},{... | collective-permute-start | bytes 393224 | tf_op jit(solution)/shard_map/ppermute | solution.py:335
  132.1 4.3 %collective-permute-start.4 = (bf16[256,256]{1,0:T(8,128)(2,1)S(1)}, bf16[256,256]{1,0:T(8,128)(2,1)S(1)}, u32[]{:S(2)}, u32[]{:S(2)}) collective-permute-start(bf16[256,256]{1,0:T(8,128)(2,1)S(1)} %all_gather.7.refs_0_), channel_id=1, source_target_pairs={{0,192},{64,256},{128,320},{192,384},{256,448},{320,0},{384,64},{4... | collective-permute-start | bytes 393224 | tf_op jit(solution)/shard_map/ppermute | solution.py:335
  136.5 3.9 %collective-permute-start.5 = (bf16[256,256]{1,0:T(8,128)(2,1)S(1)}, bf16[256,256]{1,0:T(8,128)(2,1)S(1)}, u32[]{:S(2)}, u32[]{:S(2)}) collective-permute-start(bf16[256,256]{1,0:T(8,128)(2,1)S(1)} %all_gather.7.refs_0_), channel_id=1, source_target_pairs={{0,256},{64,320},{128,384},{192,448},{256,0},{320,64},{384,128},{4... | collective-permute-start | bytes 393224 | tf_op jit(solution)/shard_map/ppermute | solution.py:335
  140.4 4.4 %collective-permute-start.6 = (bf16[256,256]{1,0:T(8,128)(2,1)S(1)}, bf16[256,256]{1,0:T(8,128)(2,1)S(1)}, u32[]{:S(2)}, u32[]{:S(2)}) collective-permute-start(bf16[256,256]{1,0:T(8,128)(2,1)S(1)} %all_gather.7.refs_0_), channel_id=1, source_target_pairs={{0,320},{64,384},{128,448},{192,0},{256,64},{320,128},{384,192},{4... | collective-permute-start | bytes 393224 | tf_op jit(solution)/shard_map/ppermute | solution.py:335
  144.8 0.3 convolution_convert_fusion.4
  145.1 5.1 %collective-permute-start.7 = (bf16[256,256]{1,0:T(8,128)(2,1)S(1)}, bf16[256,256]{1,0:T(8,128)(2,1)S(1)}, u32[]{:S(2)}, u32[]{:S(2)}) collective-permute-start(bf16[256,256]{1,0:T(8,128)(2,1)S(1)} %all_gather.7.refs_0_), channel_id=1, source_target_pairs={{0,384},{64,448},{128,0},{192,64},{256,128},{320,192},{384,256},{4... | collective-permute-start | bytes 393224 | tf_op jit(solution)/shard_map/ppermute | solution.py:335
  150.3 3.1 %collective-permute-start.8 = (bf16[256,256]{1,0:T(8,128)(2,1)S(1)}, bf16[256,256]{1,0:T(8,128)(2,1)S(1)}, u32[]{:S(2)}, u32[]{:S(2)}) collective-permute-start(bf16[256,256]{1,0:T(8,128)(2,1)S(1)} %all_gather.7.refs_0_), channel_id=1, source_target_pairs={{0,448},{64,0},{128,64},{192,128},{256,192},{320,256},{384,320},{4... | collective-permute-start | bytes 393224 | tf_op jit(solution)/shard_map/ppermute | solution.py:335
  153.4 20.3 %all_gather.6.normed_ref = bf16[128,2048]{1,0:T(8,128)(2,1)} all-gather(bf16[128,128]{1,0:T(8,128)(2,1)S(1)} %convolution_convert_fusion.4), channel_id=1, replica_groups=mesh['z'=8,'x'=4,'y'=8,'c'=2] {'y','c'}, dimensions={1}, use_global_device_ids=true | all-gather | bytes 557056 | tf_op jit(solution)/shard_map/all_gather | solution.py:358
  173.8 0.6 copy-done.13
  174.5 3.2 %resid_mixed.1 = (bf16[128,2048]{1,0:T(8,128)(2,1)}, bf16[128,256]{1,0:T(8,128)(2,1)}) custom-call(s32[1]{0:T(128)} %bitcast.19.place_ref, bf16[128,2048]{1,0:T(8,128)(2,1)} %all_gather.6.normed_ref, bf16[128,2048]{1,0:T(8,128)(2,1)} %cot_ref.3, bf16[128,2048]{1,0:T(8,128)(2,1)} %resid_ref.3, f32[1,2048]{1,0:T(1,128)} %bitcast.333, ...), custom_call_target="tpu_custom_call" | custom-call | tf_op jit(solution)/shard_map/resid_mixed/pallas_call | solution.py:234
  177.7 1.1 fusion.108
  179.0 0.7 broadcast_in_dim.120
  179.7 4.0 %all-to-all-start.4 = ((bf16[4,136,256]{2,1,0:T(8,128)(2,1)}), bf16[4,136,256]{2,1,0:T(8,128)(2,1)S(1)}, u32[]{:S(2)}, u32[]{:S(2)}) async-start(bf16[4,136,256]{2,1,0:T(8,128)(2,1)} %broadcast_in_dim.120), calls=%async_computation.4 | async-start | bytes 557056 | tf_op jit(solution)/shard_map/all_to_all | solution.py:45
  183.7 0.5 convolution_convert_fusion
  184.2 4.8 %collective-permute-start.11 = (bf16[8,64,256]{2,1,0:T(8,128)(2,1)S(1)}, bf16[8,64,256]{2,1,0:T(8,128)(2,1)S(1)}, u32[]{:S(2)}, u32[]{:S(2)}) collective-permute-start(bf16[8,64,256]{2,1,0:T(8,128)(2,1)S(1)} %get-tuple-element.41), channel_id=1, source_target_pairs={{0,48},{16,0},{32,16},{48,32},{1,49},{17,1},{33,17},{49,33},{2,50}... | collective-permute-start | bytes 786440 | tf_op jit(solution)/shard_map/ppermute | solution.py:398
  189.0 2.5 collective-permute-start.10
  191.5 2.5 collective-permute-start.9
  194.0 0.6 broadcast_select_fusion.25
  194.6 0.6 broadcast_select_fusion.23
  195.2 4.1 %collective-permute-done.10 = bf16[8,64,256]{2,1,0:T(8,128)(2,1)S(1)} collective-permute-done((bf16[8,64,256]{2,1,0:T(8,128)(2,1)S(1)}, bf16[8,64,256]{2,1,0:T(8,128)(2,1)S(1)}, u32[]{:S(2)}, u32[]{:S(2)}) %collective-permute-start.10) | collective-permute-done | bytes 262176 | tf_op jit(solution)/shard_map/ppermute | solution.py:398
  199.3 7.0 %collective-permute-done.9 = bf16[8,64,256]{2,1,0:T(8,128)(2,1)} collective-permute-done((bf16[8,64,256]{2,1,0:T(8,128)(2,1)S(1)}, bf16[8,64,256]{2,1,0:T(8,128)(2,1)}, u32[]{:S(2)}, u32[]{:S(2)}) %collective-permute-start.9) | collective-permute-done | bytes 262176 | tf_op jit(solution)/shard_map/ppermute | solution.py:398
  206.3 1.8 fusion.37
  208.2 3.5 %all-to-all-start.3 = ((bf16[8,64,256]{2,1,0:T(8,128)(2,1)}), bf16[8,64,256]{2,1,0:T(8,128)(2,1)S(1)}, u32[]{:S(2)}, u32[]{:S(2)}) async-start(bf16[8,64,256]{2,1,0:T(8,128)(2,1)} %fusion.37), calls=%async_computation.3 | async-start | bytes 524288 | tf_op jit(solution)/shard_map/all_to_all | solution.py:403
  211.9 11.6 %all-to-all-done.3 = bf16[8,64,256]{2,1,0:T(8,128)(2,1)S(1)} async-done(((bf16[8,64,256]{2,1,0:T(8,128)(2,1)}), bf16[8,64,256]{2,1,0:T(8,128)(2,1)S(1)}, u32[]{:S(2)}, u32[]{:S(2)}) %all-to-all-start.3) | async-done | bytes 262176 | tf_op jit(solution)/shard_map/all_to_all | solution.py:403
  223.5 0.9 broadcast_in_dim.121
  224.3 3.5 %all-to-all-start.5 = ((bf16[8,136,256]{2,1,0:T(8,128)(2,1)}), bf16[8,136,256]{2,1,0:T(8,128)(2,1)S(1)}, u32[]{:S(2)}, u32[]{:S(2)}) async-start(bf16[8,136,256]{2,1,0:T(8,128)(2,1)} %broadcast_in_dim.121), calls=%async_computation.5 | async-start | bytes 1114112 | tf_op jit(solution)/shard_map/all_to_all | solution.py:45
  228.1 2.0 multiply_reduce_fusion
  230.2 4.9 %fusion.1 = f32[2,64,128]{2,1,0:T(8,128)S(1)} fusion(f32[2,64,128,64]{2,3,1,0:T(8,128)} %get-tuple-element.58, f32[2,64,128]{2,1,0:T(8,128)S(1)} %get-tuple-element.67, f32[2,64,64]{2,1,0:T(8,128)S(1)} %copy.38), kind=kLoop, calls=%fused_computation.3 | loop fusion | flops 3129344 | bytes 4358144 | tf_op jit(solution)/shard_map/nts,nsd,ntsd->ntd/dot_general | solution.py:111
  235.1 0.7 convert_reduce_fusion
  235.8 10.7 %all-to-all-done.5 = bf16[8,136,256]{2,1,0:T(8,128)(2,1)S(1)} async-done(((bf16[8,136,256]{2,1,0:T(8,128)(2,1)}), bf16[8,136,256]{2,1,0:T(8,128)(2,1)S(1)}, u32[]{:S(2)}, u32[]{:S(2)}) %all-to-all-start.5) | async-done | bytes 557088 | tf_op jit(solution)/shard_map/all_to_all | solution.py:45
  246.6 0.3 fusion.59
  247.3 0.8 multiply_subtract_fusion
  248.4 0.8 fusion.5
  249.2 0.4 fusion.65
  249.6 0.6 broadcast_add_fusion
  (131 shorter events, 2.9 us)
Async XLA Ops:
  0.6 183.0 %copy-start = (bf16[128,256]{1,0:T(8,128)(2,1)S(1)}, bf16[128,256]{1,0:T(8,128)(2,1)}, u32[]{:S(2)}) copy-start(bf16[128,256]{1,0:T(8,128)(2,1)} %param.24) | copy-start | bytes 196612
  4.5 14.0 %copy-start.20 = (f32[128,128]{1,0:T(8,128)S(1)}, f32[128,128]{1,0:T(8,128)}, u32[]{:S(2)}) copy-start(f32[128,128]{1,0:T(8,128)} %param.28) | copy-start | bytes 196612
  4.5 56.0 %copy-start.23 = (bf16[64,256]{1,0:T(8,128)(2,1)S(1)}, bf16[64,256]{1,0:T(8,128)(2,1)}, u32[]{:S(2)}) copy-start(bf16[64,256]{1,0:T(8,128)(2,1)} %param.23) | copy-start | bytes 98308
  4.5 66.0 %copy-start.1 = (bf16[1,2048,128]{2,1,0:T(8,128)(2,1)S(1)}, bf16[1,2048,128]{2,1,0:T(8,128)(2,1)}, u32[]{:S(2)}) copy-start(bf16[1,2048,128]{2,1,0:T(8,128)(2,1)} %param.21) | copy-start | bytes 1572868
  4.5 66.0 %copy-start.2 = (bf16[1,2048,128]{2,1,0:T(8,128)(2,1)S(1)}, bf16[1,2048,128]{2,1,0:T(8,128)(2,1)}, u32[]{:S(2)}) copy-start(bf16[1,2048,128]{2,1,0:T(8,128)(2,1)} %param.20) | copy-start | bytes 1572868
  4.5 51.8 %all-to-all-start = ((bf16[32,24,1024]{2,1,0:T(8,128)(2,1)}), bf16[32,24,1024]{2,1,0:T(8,128)(2,1)}, u32[]{:S(2)}, u32[]{:S(2)}) async-start(bf16[32,24,1024]{2,1,0:T(8,128)(2,1)} %bitcast.310), calls=%async_computation | async-start | bytes 3145728 | tf_op jit(solution)/shard_map/all_to_all | solution.py:284
  18.5 53.1 %copy-start.18 = (bf16[128,128]{1,0:T(8,128)(2,1)S(1)}, bf16[128,128]{1,0:T(8,128)(2,1)}, u32[]{:S(2)}) copy-start(bf16[128,128]{1,0:T(8,128)(2,1)} %param.25) | copy-start | bytes 98308
  18.5 53.1 %copy-start.9 = (bf16[128,128]{1,0:T(8,128)(2,1)S(1)}, bf16[128,128]{1,0:T(8,128)(2,1)}, u32[]{:S(2)}) copy-start(bf16[128,128]{1,0:T(8,128)(2,1)} %param.26) | copy-start | bytes 98308
  18.5 53.1 %copy-start.5 = (bf16[128,256]{1,0:T(8,128)(2,1)S(1)}, bf16[128,256]{1,0:T(8,128)(2,1)}, u32[]{:S(2)}) copy-start(bf16[128,256]{1,0:T(8,128)(2,1)} %param.27) | copy-start | bytes 196612
  18.5 53.3 %copy-start.8 = (bf16[1,128,2048]{2,1,0:T(8,128)(2,1)S(1)}, bf16[1,128,2048]{2,1,0:T(8,128)(2,1)}, u32[]{:S(2)}) copy-start(bf16[1,128,2048]{2,1,0:T(8,128)(2,1)} %param.22) | copy-start | bytes 1572868
  18.7 53.2 %copy-start.24 = (f32[2,1,128]{2,1,0:T(1,128)}, f32[2,1,128]{2,1,0:T(1,128)S(1)}, u32[]{:S(2)}) copy-start(f32[2,1,128]{2,1,0:T(1,128)S(1)} %get-tuple-element.65) | copy-start | bytes 3076
  18.7 64.6 %copy-start.21 = (pred[64,64]{1,0:T(8,128)(4,1)}, pred[64,64]{1,0:T(8,128)(4,1)S(1)}, u32[]{:S(2)}) copy-start(pred[64,64]{1,0:T(8,128)(4,1)S(1)} %iota_compare_fusion.8) | copy-start | bytes 12292
  19.8 159.0 %copy-start.29 = (f32[128]{0:T(128)}, f32[128]{0:T(128)S(1)}, u32[]{:S(2)}) copy-start(f32[128]{0:T(128)S(1)} %get-tuple-element.60) | copy-start | bytes 1540
  56.4 15.6 %collective-permute-start = (bf16[768,1024]{1,0:T(8,128)(2,1)}, bf16[768,1024]{1,0:T(8,128)(2,1)}, u32[]{:S(2)}, u32[]{:S(2)}) collective-permute-start(bf16[768,1024]{1,0:T(8,128)(2,1)} %bitcast.10), channel_id=1, source_target_pairs={{0,1},{1,0},{2,3},{3,2},{4,5},{5,4},{6,7},{7,6},{8,9},{9,8},{10,11... | collective-permute-start | bytes 4718600 | tf_op jit(solution)/shard_map/ppermute | solution.py:287
  70.5 79.8 %copy-start.7 = (bf16[256,256]{1,0:T(8,128)(2,1)}, bf16[256,256]{1,0:T(8,128)(2,1)S(1)}, u32[]{:S(2)}) copy-start(bf16[256,256]{1,0:T(8,128)(2,1)S(1)} %all_gather.7.refs_0_) | copy-start | bytes 393220
  77.1 5.5 %copy-start.3 = (f32[1,1,128,256]{3,2,1,0:T(8,128)S(1)}, f32[1,1,128,256]{3,2,1,0:T(8,128)}, u32[]{:S(2)}) copy-start(f32[1,1,128,256]{3,2,1,0:T(8,128)} %param.29) | copy-start | bytes 393220
  77.9 9.2 %collective-permute-start.1 = (bf16[384,1024]{1,0:T(8,128)(2,1)S(1)}, bf16[384,1024]{1,0:T(8,128)(2,1)S(1)}, u32[]{:S(2)}, u32[]{:S(2)}) collective-permute-start(bf16[384,1024]{1,0:T(8,128)(2,1)S(1)} %convolution_convert_fusion.2), channel_id=1, source_target_pairs={{0,1},{1,0},{2,3},{3,2},{4,5},{5,4},{6,7},{7,6},{8,9},{9,8},{10,11... | collective-permute-start | bytes 2359304 | tf_op jit(solution)/shard_map/ppermute | solution.py:326
  88.6 30.5 %all-to-all-start.1 = ((bf16[8,384,128]{2,1,0:T(8,128)(2,1)}), bf16[8,384,128]{2,1,0:T(8,128)(2,1)S(1)}, u32[]{:S(2)}, u32[]{:S(2)}) async-start(bf16[8,384,128]{2,1,0:T(8,128)(2,1)} %bitcast.300), calls=%async_computation.1 | async-start | bytes 1572864 | tf_op jit(solution)/shard_map/all_to_all | solution.py:329
  119.8 24.9 %all-to-all-start.2 = ((bf16[32,12,128]{2,1,0:T(8,128)(2,1)}), bf16[32,12,128]{2,1,0:T(8,128)(2,1)S(1)}, u32[]{:S(2)}, u32[]{:S(2)}) async-start(bf16[32,12,128]{2,1,0:T(8,128)(2,1)} %reshape.601), calls=%async_computation.2 | async-start | bytes 262144 | tf_op jit(solution)/shard_map/all_to_all | solution.py:350
  125.0 20.1 %collective-permute-start.2 = (bf16[256,256]{1,0:T(8,128)(2,1)S(1)}, bf16[256,256]{1,0:T(8,128)(2,1)S(1)}, u32[]{:S(2)}, u32[]{:S(2)}) collective-permute-start(bf16[256,256]{1,0:T(8,128)(2,1)S(1)} %all_gather.7.refs_0_), channel_id=1, source_target_pairs={{0,64},{64,128},{128,192},{192,256},{256,320},{320,384},{384,448},... | collective-permute-start | bytes 393224 | tf_op jit(solution)/shard_map/ppermute | solution.py:335
  128.1 22.2 %collective-permute-start.3 = (bf16[256,256]{1,0:T(8,128)(2,1)S(1)}, bf16[256,256]{1,0:T(8,128)(2,1)S(1)}, u32[]{:S(2)}, u32[]{:S(2)}) collective-permute-start(bf16[256,256]{1,0:T(8,128)(2,1)S(1)} %all_gather.7.refs_0_), channel_id=1, source_target_pairs={{0,128},{64,192},{128,256},{192,320},{256,384},{320,448},{384,0},{... | collective-permute-start | bytes 393224 | tf_op jit(solution)/shard_map/ppermute | solution.py:335
  132.1 41.6 %collective-permute-start.4 = (bf16[256,256]{1,0:T(8,128)(2,1)S(1)}, bf16[256,256]{1,0:T(8,128)(2,1)S(1)}, u32[]{:S(2)}, u32[]{:S(2)}) collective-permute-start(bf16[256,256]{1,0:T(8,128)(2,1)S(1)} %all_gather.7.refs_0_), channel_id=1, source_target_pairs={{0,192},{64,256},{128,320},{192,384},{256,448},{320,0},{384,64},{4... | collective-permute-start | bytes 393224 | tf_op jit(solution)/shard_map/ppermute | solution.py:335
  136.5 37.2 %collective-permute-start.5 = (bf16[256,256]{1,0:T(8,128)(2,1)S(1)}, bf16[256,256]{1,0:T(8,128)(2,1)S(1)}, u32[]{:S(2)}, u32[]{:S(2)}) collective-permute-start(bf16[256,256]{1,0:T(8,128)(2,1)S(1)} %all_gather.7.refs_0_), channel_id=1, source_target_pairs={{0,256},{64,320},{128,384},{192,448},{256,0},{320,64},{384,128},{4... | collective-permute-start | bytes 393224 | tf_op jit(solution)/shard_map/ppermute | solution.py:335
  140.4 33.3 %collective-permute-start.6 = (bf16[256,256]{1,0:T(8,128)(2,1)S(1)}, bf16[256,256]{1,0:T(8,128)(2,1)S(1)}, u32[]{:S(2)}, u32[]{:S(2)}) collective-permute-start(bf16[256,256]{1,0:T(8,128)(2,1)S(1)} %all_gather.7.refs_0_), channel_id=1, source_target_pairs={{0,320},{64,384},{128,448},{192,0},{256,64},{320,128},{384,192},{4... | collective-permute-start | bytes 393224 | tf_op jit(solution)/shard_map/ppermute | solution.py:335
  145.1 28.7 %copy-start.11 = (bf16[256,256]{1,0:T(8,128)(2,1)}, bf16[256,256]{1,0:T(8,128)(2,1)S(1)}, u32[]{:S(2)}) copy-start(bf16[256,256]{1,0:T(8,128)(2,1)S(1)} %collective-permute-done.2.refs_1_) | copy-start | bytes 393220
  145.1 28.6 %collective-permute-start.7 = (bf16[256,256]{1,0:T(8,128)(2,1)S(1)}, bf16[256,256]{1,0:T(8,128)(2,1)S(1)}, u32[]{:S(2)}, u32[]{:S(2)}) collective-permute-start(bf16[256,256]{1,0:T(8,128)(2,1)S(1)} %all_gather.7.refs_0_), channel_id=1, source_target_pairs={{0,384},{64,448},{128,0},{192,64},{256,128},{320,192},{384,256},{4... | collective-permute-start | bytes 393224 | tf_op jit(solution)/shard_map/ppermute | solution.py:335
  150.3 23.5 %copy-start.12 = (bf16[256,256]{1,0:T(8,128)(2,1)}, bf16[256,256]{1,0:T(8,128)(2,1)S(1)}, u32[]{:S(2)}) copy-start(bf16[256,256]{1,0:T(8,128)(2,1)S(1)} %collective-permute-done.3.refs_2_) | copy-start | bytes 393220
  150.3 23.4 %collective-permute-start.8 = (bf16[256,256]{1,0:T(8,128)(2,1)S(1)}, bf16[256,256]{1,0:T(8,128)(2,1)S(1)}, u32[]{:S(2)}, u32[]{:S(2)}) collective-permute-start(bf16[256,256]{1,0:T(8,128)(2,1)S(1)} %all_gather.7.refs_0_), channel_id=1, source_target_pairs={{0,448},{64,0},{128,64},{192,128},{256,192},{320,256},{384,320},{4... | collective-permute-start | bytes 393224 | tf_op jit(solution)/shard_map/ppermute | solution.py:335
  173.7 0.7 copy-start.13
  173.7 0.7 copy-start.14
  173.7 0.7 copy-start.15
  173.7 0.8 copy-start.16
  173.8 0.8 copy-start.17
  177.7 6.0 %copy-start.6 = (bf16[128,2048]{1,0:T(8,128)(2,1)S(1)}, bf16[128,2048]{1,0:T(8,128)(2,1)}, u32[]{:S(2)}) copy-start(bf16[128,2048]{1,0:T(8,128)(2,1)} %get-tuple-element.18) | copy-start | bytes 1572868
  179.7 14.3 %all-to-all-start.4 = ((bf16[4,136,256]{2,1,0:T(8,128)(2,1)}), bf16[4,136,256]{2,1,0:T(8,128)(2,1)S(1)}, u32[]{:S(2)}, u32[]{:S(2)}) async-start(bf16[4,136,256]{2,1,0:T(8,128)(2,1)} %broadcast_in_dim.120), calls=%async_computation.4 | async-start | bytes 557056 | tf_op jit(solution)/shard_map/all_to_all | solution.py:45
  184.2 11.0 %collective-permute-start.11 = (bf16[8,64,256]{2,1,0:T(8,128)(2,1)S(1)}, bf16[8,64,256]{2,1,0:T(8,128)(2,1)S(1)}, u32[]{:S(2)}, u32[]{:S(2)}) collective-permute-start(bf16[8,64,256]{2,1,0:T(8,128)(2,1)S(1)} %get-tuple-element.41), channel_id=1, source_target_pairs={{0,48},{16,0},{32,16},{48,32},{1,49},{17,1},{33,17},{49,33},{2,50}... | collective-permute-start | bytes 786440 | tf_op jit(solution)/shard_map/ppermute | solution.py:398
  189.0 10.3 %collective-permute-start.10 = (bf16[8,64,256]{2,1,0:T(8,128)(2,1)S(1)}, bf16[8,64,256]{2,1,0:T(8,128)(2,1)S(1)}, u32[]{:S(2)}, u32[]{:S(2)}) collective-permute-start(bf16[8,64,256]{2,1,0:T(8,128)(2,1)S(1)} %get-tuple-element.42), channel_id=1, source_target_pairs={{0,32},{16,48},{32,0},{48,16},{1,33},{17,49},{33,1},{49,17},{2,34}... | collective-permute-start | bytes 786440 | tf_op jit(solution)/shard_map/ppermute | solution.py:398
  191.5 14.9 %collective-permute-start.9 = (bf16[8,64,256]{2,1,0:T(8,128)(2,1)S(1)}, bf16[8,64,256]{2,1,0:T(8,128)(2,1)}, u32[]{:S(2)}, u32[]{:S(2)}) collective-permute-start(bf16[8,64,256]{2,1,0:T(8,128)(2,1)S(1)} %get-tuple-element.40), channel_id=1, source_target_pairs={{0,16},{16,32},{32,48},{48,0},{1,17},{17,33},{33,49},{49,1},{2,18}... | collective-permute-start | bytes 786440 | tf_op jit(solution)/shard_map/ppermute | solution.py:398
  194.0 5.3 %copy-start.26 = (f32[4,1,128]{2,1,0:T(1,128)}, f32[4,1,128]{2,1,0:T(1,128)S(1)}, u32[]{:S(2)}) copy-start(f32[4,1,128]{2,1,0:T(1,128)S(1)} %slice_convert_fusion.1) | copy-start | bytes 6148
  195.2 16.5 %copy-start.35 = (f32[128]{0:T(128)S(1)}, f32[128]{0:T(128)}, u32[]{:S(2)}) copy-start(f32[128]{0:T(128)} %get-tuple-element.78) | copy-start | bytes 1540
  195.2 16.5 %copy-start.36 = (f32[128]{0:T(128)S(1)}, f32[128]{0:T(128)}, u32[]{:S(2)}) copy-start(f32[128]{0:T(128)} %get-tuple-element.79) | copy-start | bytes 1540
  206.3 5.4 %copy-start.27 = (f32[4,1,128]{2,1,0:T(1,128)S(1)}, f32[4,1,128]{2,1,0:T(1,128)}, u32[]{:S(2)}) copy-start(f32[4,1,128]{2,1,0:T(1,128)} %copy-done.26) | copy-start | bytes 6148
  208.2 19.7 %copy-start.4 = (bf16[128,256]{1,0:T(8,128)(2,1)S(1)}, bf16[128,256]{1,0:T(8,128)(2,1)}, u32[]{:S(2)}) copy-start(bf16[128,256]{1,0:T(8,128)(2,1)} %get-tuple-element.19) | copy-start | bytes 196612
  208.2 20.0 %copy-start.22 = (pred[64,64]{1,0:T(8,128)(4,1)S(1)}, pred[64,64]{1,0:T(8,128)(4,1)}, u32[]{:S(2)}) copy-start(pred[64,64]{1,0:T(8,128)(4,1)} %copy-done.21) | copy-start | bytes 12292
  208.2 15.3 %all-to-all-start.3 = ((bf16[8,64,256]{2,1,0:T(8,128)(2,1)}), bf16[8,64,256]{2,1,0:T(8,128)(2,1)S(1)}, u32[]{:S(2)}, u32[]{:S(2)}) async-start(bf16[8,64,256]{2,1,0:T(8,128)(2,1)} %fusion.37), calls=%async_computation.3 | async-start | bytes 524288 | tf_op jit(solution)/shard_map/all_to_all | solution.py:403
  224.3 22.1 %all-to-all-start.5 = ((bf16[8,136,256]{2,1,0:T(8,128)(2,1)}), bf16[8,136,256]{2,1,0:T(8,128)(2,1)S(1)}, u32[]{:S(2)}, u32[]{:S(2)}) async-start(bf16[8,136,256]{2,1,0:T(8,128)(2,1)} %broadcast_in_dim.121), calls=%async_computation.5 | async-start | bytes 1114112 | tf_op jit(solution)/shard_map/all_to_all | solution.py:45
  230.1 16.4 %copy-start.31 = (f32[128]{0:T(128)S(1)}, f32[128]{0:T(128)}, u32[]{:S(2)}) copy-start(f32[128]{0:T(128)} %get-tuple-element.74) | copy-start | bytes 1540
  230.1 16.4 %copy-start.32 = (f32[128]{0:T(128)S(1)}, f32[128]{0:T(128)}, u32[]{:S(2)}) copy-start(f32[128]{0:T(128)} %get-tuple-element.75) | copy-start | bytes 1540
  230.1 16.4 %copy-start.33 = (f32[128]{0:T(128)S(1)}, f32[128]{0:T(128)}, u32[]{:S(2)}) copy-start(f32[128]{0:T(128)} %get-tuple-element.77) | copy-start | bytes 1540
  230.1 16.4 %copy-start.34 = (f32[128]{0:T(128)S(1)}, f32[128]{0:T(128)}, u32[]{:S(2)}) copy-start(f32[128]{0:T(128)} %get-tuple-element.20) | copy-start | bytes 1540
  230.1 16.7 %copy-start.25 = (f32[2,1,128]{2,1,0:T(1,128)S(1)}, f32[2,1,128]{2,1,0:T(1,128)}, u32[]{:S(2)}) copy-start(f32[2,1,128]{2,1,0:T(1,128)} %copy-done.24) | copy-start | bytes 3076
  230.2 16.7 %copy-start.28 = (f32[2,128]{1,0:T(2,128)S(1)}, f32[2,128]{1,0:T(2,128)}, u32[]{:S(2)}) copy-start(f32[2,128]{1,0:T(2,128)} %subtract_exponential_fusion.1) | copy-start | bytes 3076
  235.1 12.2 %copy-start.10 = (bf16[1,128,256]{2,1,0:T(8,128)(2,1)S(1)}, bf16[1,128,256]{2,1,0:T(8,128)(2,1)}, u32[]{:S(2)}) copy-start(bf16[1,128,256]{2,1,0:T(8,128)(2,1)} %multiply_add_fusion.3) | copy-start | bytes 196612
  235.1 12.2 %copy-start.19 = (bf16[128,128]{1,0:T(8,128)(2,1)S(1)}, bf16[128,128]{1,0:T(8,128)(2,1)}, u32[]{:S(2)}) copy-start(bf16[128,128]{1,0:T(8,128)(2,1)} %param.25) | copy-start | bytes 98308
  246.5 2.7 %copy-start.30 = (f32[128]{0:T(128)S(1)}, f32[128]{0:T(128)}, u32[]{:S(2)}) copy-start(f32[128]{0:T(128)} %copy-done.29) | copy-start | bytes 1540
  246.5 2.6 %copy-start.37 = (f32[128]{0:T(128)S(1)}, f32[128]{0:T(128)}, u32[]{:S(2)}) copy-start(f32[128]{0:T(128)} %get-tuple-element.59) | copy-start | bytes 1540

commit v5 on v4

--- a/solution.py
+++ b/solution.py
@@ -205,6 +205,26 @@
         scratch_shapes=[pltpu.VMEM((4 * tokens, half), jnp.bfloat16)],
         name="dispatch_rows",
     )(core.astype(jnp.int32).reshape(1), ids.T, weight.T, resid, cotangent, gain.reshape(1, -1))
+
+
+def pair_tiles_kernel(own_ref, passed_ref, out_ref):
+    width = out_ref.shape[2]
+    for k in range(out_ref.shape[0]):
+        cols = slice(k * width, (k + 1) * width)
+        total = own_ref[:, cols] + passed_ref[:, cols].astype(jnp.float32)
+        out_ref[k] = total.astype(jnp.bfloat16)
+
+
+def pair_tiles(own, passed, count):
+    rows, width = own.shape
+    vmem = pl.BlockSpec(memory_space=pltpu.VMEM)
+    return pl.pallas_call(
+        pair_tiles_kernel,
+        out_shape=jax.ShapeDtypeStruct((count, rows, width // count), jnp.bfloat16),
+        in_specs=[vmem, vmem],
+        out_specs=vmem,
+        name="pair_tiles",
+    )(own, passed)
 
 
 def resid_mixed_kernel(place_ref, normed_ref, cot_ref, resid_ref, gain_ref, *refs):
@@ -281,6 +301,8 @@
     )
     slot_a, slot_b = slot_rows[0], slot_rows[1]
     sent = sent.reshape(sp_count, 2 * capacity, half)
+    gate_w, up_w, down_w = expert_gate[0], expert_up[0], expert_down[0]
+    width = gate_w.shape[1]
     own = lax.all_to_all(sent, SP, 0, 0, tiled=True).reshape(2 * slots, half)
     proj_near, _ = lax.optimization_barrier((out_proj, sent))
     proj_near = lax.all_gather(proj_near, "x", axis=0, tiled=True)
@@ -288,16 +310,20 @@
     rows_in = jnp.where(core == 0, own, other)
     rows_cot = jnp.where(core == 0, other, own)
 
-    gate_w, up_w, down_w = expert_gate[0], expert_up[0], expert_down[0]
-    width = gate_w.shape[1]
     into_w = jnp.concatenate([gate_w[:half], gate_w[half:], up_w[:half], up_w[half:]], axis=1)
-    down_two = jnp.concatenate([down_w[:, :half], down_w[:, half:]], axis=0)
-    pre = jnp.dot(rows_in, into_w, preferred_element_type=jnp.float32)
+    down_t = jnp.transpose(down_w)
+    down_t = jnp.concatenate([down_t[:half], down_t[half:]], axis=1)
+    down_t = jnp.pad(down_t, ((0, 0), (0, 2 * width)))
+    own_w = jnp.where(core == 0, into_w, down_t)
+    other_w = jnp.where(core == 0, down_t, into_w)
+    own_w, other_w = lax.optimization_barrier((own_w, other_w))
+    own_pre = jnp.dot(own, own_w, preferred_element_type=jnp.float32)
+    own_pre = lax.optimization_barrier(own_pre)
+    other_pre = jnp.dot(other, other_w, preferred_element_type=jnp.float32)
+    pre = jnp.where(core == 0, own_pre, other_pre)
+    hid = jnp.where(core == 0, other_pre[:, : 2 * width], own_pre[:, : 2 * width])
     gate_pre = pre[:, :width] + jnp.roll(pre[:, width : 2 * width], -1, axis=0)
     up_pre = pre[:, 2 * width : 3 * width] + jnp.roll(pre[:, 3 * width :], -1, axis=0)
-    hid = lax.dot_general(
-        rows_cot, down_two, (((1,), (1,)), ((), ())), preferred_element_type=jnp.float32
-    )
     grad_hidden = hid[:, :width] + jnp.roll(hid[:, width:], -1, axis=0)
     gate_sig = jax.nn.sigmoid(gate_pre)
     first = (lax.broadcasted_iota(jnp.int32, (2 * slots, 1), 0) % 2) == 0
@@ -324,15 +350,18 @@
         )
 
     passed = lax.ppermute(onto(out_other).astype(jnp.bfloat16), "c", [(0, 1), (1, 0)])
-    pair_sum = (onto(out_own) + passed.astype(jnp.float32)).astype(jnp.bfloat16)
-    parts = pair_sum.reshape(slots, y_count, width).transpose(1, 0, 2)
+    own_parts = onto(out_own)
+    parts = pair_tiles(own_parts, passed, y_count)
     swapped = lax.all_to_all(parts, "y", 0, 0, tiled=True)
     summed = sum_parts(swapped).astype(jnp.bfloat16)
     proj_tied, _ = lax.optimization_barrier((proj_near, parts))
+    proj_early, _ = lax.optimization_barrier((proj_near, own))
+    proj_mid, _ = lax.optimization_barrier((proj_near, acts))
     z_place = lax.axis_index("z")
     blocks = [proj_near] + [None] * 7
     for k in range(1, 8):
-        blocks[k] = lax.ppermute(proj_tied, "z", [(i, (i + k) % 8) for i in range(8)])
+        sent_block = proj_early if k == 5 else proj_mid if k == 4 else proj_tied
+        blocks[k] = lax.ppermute(sent_block, "z", [(i, (i + k) % 8) for i in range(8)])
 
     def beside(values):
         return jnp.concatenate([values, jnp.roll(values, 1, axis=0)], axis=1)

time: 251 us -> 250 us (level)
  the two profiles are of different devices: /device:TPU:1 before, /device:TPU:2 now
where the time goes in v5:
time: 250 us; the launch traced here: 248 us
  starting transfers between devices  81 us (32%)
  waiting for transfers between devices  76.8 us (31%)
  blocking collectives  30.6 us (12%)
  other arithmetic  24.3 us (10%)
  matrix products  14.4 us (6%)
  local copies, waits for them, and re-layouts  9.97 us (4%)
  Pallas kernels  9.74 us (4%)
    all_to_all x1, waiting for transfers between devices, on_device_body(): own = lax.all_to_all(sent, SP, 0, 0, tiled=True).reshape(2 * slots, half)  34 us
    ppermute x7, starting transfers between devices, on_device_body(): lax.ppermute(sent_block, 'z', [(i, (i + k) % 8) for i in range(8)])  27.8 us
    all_gather x1, blocking collectives, on_device_body(): lax.all_gather(lax.dot_general(slot_tokens, flat_rows, (((0,), (0,)), (()...  17.6 us
    all_to_all x1, waiting for transfers between devices, on_device_body(): swapped = lax.all_to_all(parts, 'y', 0, 0, tiled=True)  15.2 us
    all_to_all x1, starting transfers between devices, on_device_body(): own = lax.all_to_all(sent, SP, 0, 0, tiled=True).reshape(2 * slots, half)  13.6 us
    all_gather x1, blocking collectives, on_device_body(): proj_near = lax.all_gather(proj_near, 'x', axis=0, tiled=True)  12.9 us
    all_to_all x1, waiting for transfers between devices, on_device_body(): share_z = lax.all_to_all(share_z, 'z', 0, 0, tiled=True)  10.5 us
    ppermute x3, starting transfers between devices, on_device_body(): lax.ppermute(for_place(k), 'x', [(i, (i + k) % 4) for i in range(4)])  9.82 us
  transfers between devices with their start and end apart: 18, of which 6 were waited for; matrix products, arithmetic and copies ran while one was open for 14% of the time, Pallas kernels for 1%

profile of v5, /device:TPU:2, one launch (start us, length us, event | category | flops | bytes accessed | tf_op | source)
XLA Modules:
  0.0 248.4 jit_solution(7388146255822487326)
XLA Ops:
  0.7 3.8 %dispatch_rows.1 = (bf16[768,1024]{1,0:T(8,128)(2,1)}, s32[8,128]{1,0:T(8,128)}) custom-call(s32[1]{0:T(128)} %bitcast.5.core_ref, s32[2,128]{1,0:T(2,128)} %bitcast.338, f32[2,128]{1,0:T(2,128)} %bitcast.339, bf16[128,2048]{1,0:T(8,128)(2,1)} %resid_ref.3, bf16[128,2048]{1,0:T(8,128)(2,1)} %cot_ref.3, f32[1,2048]{1,0:T(1,128)} %bitcast.330), custom_call_target="tpu_custom_call" | custom-call | tf_op jit(solution)/shard_map/dispatch_rows/pallas_call | solution.py:197
  4.5 13.6 %all-to-all-start = ((bf16[32,24,1024]{2,1,0:T(8,128)(2,1)}), bf16[32,24,1024]{2,1,0:T(8,128)(2,1)}, u32[]{:S(2)}, u32[]{:S(2)}) async-start(bf16[32,24,1024]{2,1,0:T(8,128)(2,1)} %bitcast.304), calls=%async_computation | async-start | bytes 3145728 | tf_op jit(solution)/shard_map/all_to_all | solution.py:306
  18.7 0.5 copy-done.1
  19.6 1.5 broadcast_select_fusion
  21.1 0.6 iota_multiply_fusion
  22.0 0.6 broadcast_multiply_fusion
  22.6 34.0 %all-to-all-done = bf16[32,24,1024]{2,1,0:T(8,128)(2,1)} async-done(((bf16[32,24,1024]{2,1,0:T(8,128)(2,1)}), bf16[32,24,1024]{2,1,0:T(8,128)(2,1)}, u32[]{:S(2)}, u32[]{:S(2)}) %all-to-all-start) | async-done | bytes 1572896 | tf_op jit(solution)/shard_map/all_to_all | solution.py:306
  56.6 1.9 collective-permute-start
  58.5 1.3 slice_bitcast_fusion.8
  59.8 0.6 convert_multiply_fusion.15
  60.5 0.7 convert_bitcast_fusion.10
  61.1 1.1 fusion.115
  62.2 1.6 multiply_add_fusion.3
  63.8 2.7 %fusion.139 = f32[768,512]{1,0:T(8,128)S(1)} fusion(bf16[768,1024]{1,0:T(8,128)(2,1)} %bitcast.10, bf16[1024,512]{0,1:T(8,128)(2,1)} %get-tuple-element.20), kind=kOutput, calls=%fused_computation.257 | convolution fusion | flops 805306368 | bytes 4194304 | tf_op jit(solution)/shard_map/dot_general | solution.py:320
  66.6 1.0 broadcast_select_fusion.2
  68.0 0.9 select_convert_fusion
  70.4 2.4 collective-permute-start.1
  72.9 12.9 %all_gather.7.refs_0_ = bf16[256,256]{1,0:T(8,128)(2,1)S(1)} all-gather(bf16[64,256]{1,0:T(8,128)(2,1)S(1)} %copy-done.31), channel_id=1, replica_groups=mesh['z'=8,'x'=4,'y'=8,'c'=2] {'x'}, dimensions={0}, use_global_device_ids=true | all-gather | bytes 163840 | tf_op jit(solution)/shard_map/all_gather | solution.py:308
  85.8 3.8 %fusion = (bf16[2,64,64]{2,1,0:T(8,128)(2,1)S(1)}, f32[2,64,128,64]{2,3,1,0:T(8,128)}) fusion(f32[2,128,64]{1,2,0:T(8,128)S(1)} %copy-done.16, f32[2,128,64]{1,2,0:T(8,128)S(1)} %bitcast.314, f32[2,64,128]{2,1,0:T(8,128)S(1)} %reduce_window_sum.33, pred[64,64]{1,0:T(8,128)(4,1)S(1)} %iota_compare_fusion.9), kind=kLoop, calls=%fused_computation.1 | loop fusion | flops 5234688 | bytes 4411392 | tf_op jit(solution)/shard_map/ntd,nsd,ntsd->nts/dot_general | solution.py:108
  89.6 2.4 collective-permute-start.6
  92.1 0.7 slice.344
  92.8 0.7 slice.346
  93.4 0.7 slice.352
  94.1 6.4 %collective-permute-start.5 = (bf16[256,256]{1,0:T(8,128)(2,1)S(1)}, bf16[256,256]{1,0:T(8,128)(2,1)}, u32[]{:S(2)}, u32[]{:S(2)}) collective-permute-start(bf16[256,256]{1,0:T(8,128)(2,1)S(1)} %all_gather.7.refs_0_), channel_id=1, source_target_pairs={{0,256},{64,320},{128,384},{192,448},{256,0},{320,64},{384,128},{4... | collective-permute-start | bytes 393224 | tf_op jit(solution)/shard_map/ppermute | solution.py:364
  100.6 1.6 fusion.140.own_ref
  102.2 0.9 copy-done.7
  103.1 2.7 %pair_tiles.1 = bf16[8,384,128]{2,1,0:T(8,128)(2,1)} custom-call(f32[384,1024]{1,0:T(8,128)} %fusion.140.own_ref, bf16[384,1024]{1,0:T(8,128)(2,1)} %copy-done.7), custom_call_target="tpu_custom_call" | custom-call | tf_op jit(solution)/shard_map/pair_tiles/pallas_call | solution.py:221
  105.9 7.2 %all-to-all-start.1 = ((bf16[8,384,128]{2,1,0:T(8,128)(2,1)}), bf16[8,384,128]{2,1,0:T(8,128)(2,1)S(1)}, u32[]{:S(2)}, u32[]{:S(2)}) async-start(bf16[8,384,128]{2,1,0:T(8,128)(2,1)} %pair_tiles.1), calls=%async_computation.1 | async-start | bytes 1572864 | tf_op jit(solution)/shard_map/all_to_all | solution.py:355
  113.1 0.6 fusion.14
  114.1 2.4 fusion.11
  116.8 1.0 maximum_bitcast_fusion
  117.8 15.2 %all-to-all-done.1 = bf16[8,384,128]{2,1,0:T(8,128)(2,1)S(1)} async-done(((bf16[8,384,128]{2,1,0:T(8,128)(2,1)}), bf16[8,384,128]{2,1,0:T(8,128)(2,1)S(1)}, u32[]{:S(2)}, u32[]{:S(2)}) %all-to-all-start.1) | async-done | bytes 786464 | tf_op jit(solution)/shard_map/all_to_all | solution.py:355
  133.1 0.7 reshape.597
  133.8 5.5 %all-to-all-start.2 = ((bf16[32,12,128]{2,1,0:T(8,128)(2,1)}), bf16[32,12,128]{2,1,0:T(8,128)(2,1)S(1)}, u32[]{:S(2)}, u32[]{:S(2)}) async-start(bf16[32,12,128]{2,1,0:T(8,128)(2,1)} %reshape.597), calls=%async_computation.2 | async-start | bytes 262144 | tf_op jit(solution)/shard_map/all_to_all | solution.py:379
  139.3 0.8 maximum_bitcast_fusion.2
  140.2 4.6 %collective-permute-start.8 = (bf16[256,256]{1,0:T(8,128)(2,1)S(1)}, bf16[256,256]{1,0:T(8,128)(2,1)S(1)}, u32[]{:S(2)}, u32[]{:S(2)}) collective-permute-start(bf16[256,256]{1,0:T(8,128)(2,1)S(1)} %all_gather.7.refs_0_), channel_id=1, source_target_pairs={{0,448},{64,0},{128,64},{192,128},{256,192},{320,256},{384,320},{4... | collective-permute-start | bytes 393224 | tf_op jit(solution)/shard_map/ppermute | solution.py:364
  144.8 4.2 %collective-permute-start.7 = (bf16[256,256]{1,0:T(8,128)(2,1)S(1)}, bf16[256,256]{1,0:T(8,128)(2,1)S(1)}, u32[]{:S(2)}, u32[]{:S(2)}) collective-permute-start(bf16[256,256]{1,0:T(8,128)(2,1)S(1)} %all_gather.7.refs_0_), channel_id=1, source_target_pairs={{0,384},{64,448},{128,0},{192,64},{256,128},{320,192},{384,256},{4... | collective-permute-start | bytes 393224 | tf_op jit(solution)/shard_map/ppermute | solution.py:364
  149.0 1.9 collective-permute-start.4
  151.3 4.8 %collective-permute-start.3 = (bf16[256,256]{1,0:T(8,128)(2,1)S(1)}, bf16[256,256]{1,0:T(8,128)(2,1)S(1)}, u32[]{:S(2)}, u32[]{:S(2)}) collective-permute-start(bf16[256,256]{1,0:T(8,128)(2,1)S(1)} %all_gather.7.refs_0_), channel_id=1, source_target_pairs={{0,128},{64,192},{128,256},{192,320},{256,384},{320,448},{384,0},{... | collective-permute-start | bytes 393224 | tf_op jit(solution)/shard_map/ppermute | solution.py:364
  156.1 3.4 %collective-permute-start.2 = (bf16[256,256]{1,0:T(8,128)(2,1)S(1)}, bf16[256,256]{1,0:T(8,128)(2,1)S(1)}, u32[]{:S(2)}, u32[]{:S(2)}) collective-permute-start(bf16[256,256]{1,0:T(8,128)(2,1)S(1)} %all_gather.7.refs_0_), channel_id=1, source_target_pairs={{0,64},{64,128},{128,192},{192,256},{256,320},{320,384},{384,448},... | collective-permute-start | bytes 393224 | tf_op jit(solution)/shard_map/ppermute | solution.py:364
  159.5 17.6 %all_gather.6.normed_ref = bf16[128,2048]{1,0:T(8,128)(2,1)} all-gather(bf16[128,128]{1,0:T(8,128)(2,1)S(1)} %convolution_convert_fusion.2), channel_id=1, replica_groups=mesh['z'=8,'x'=4,'y'=8,'c'=2] {'y','c'}, dimensions={1}, use_global_device_ids=true | all-gather | bytes 557056 | tf_op jit(solution)/shard_map/all_gather | solution.py:387
  177.3 0.6 copy-done.23
  178.0 3.2 %resid_mixed.1 = (bf16[128,2048]{1,0:T(8,128)(2,1)}, bf16[128,256]{1,0:T(8,128)(2,1)}) custom-call(s32[1]{0:T(128)} %bitcast.21.place_ref, bf16[128,2048]{1,0:T(8,128)(2,1)} %all_gather.6.normed_ref, bf16[128,2048]{1,0:T(8,128)(2,1)} %cot_ref.3, bf16[128,2048]{1,0:T(8,128)(2,1)} %resid_ref.3, f32[1,2048]{1,0:T(1,128)} %bitcast.331, ...), custom_call_target="tpu_custom_call" | custom-call | tf_op jit(solution)/shard_map/resid_mixed/pallas_call | solution.py:254
  181.2 1.1 fusion.110
  182.5 0.7 broadcast_in_dim.120
  183.2 4.8 %all-to-all-start.4 = ((bf16[4,136,256]{2,1,0:T(8,128)(2,1)}), bf16[4,136,256]{2,1,0:T(8,128)(2,1)S(1)}, u32[]{:S(2)}, u32[]{:S(2)}) async-start(bf16[4,136,256]{2,1,0:T(8,128)(2,1)} %broadcast_in_dim.120), calls=%async_computation.4 | async-start | bytes 557056 | tf_op jit(solution)/shard_map/all_to_all | solution.py:45
  188.0 0.5 convolution_convert_fusion
  188.6 3.4 %collective-permute-start.9 = (bf16[8,64,256]{2,1,0:T(8,128)(2,1)S(1)}, bf16[8,64,256]{2,1,0:T(8,128)(2,1)S(1)}, u32[]{:S(2)}, u32[]{:S(2)}) collective-permute-start(bf16[8,64,256]{2,1,0:T(8,128)(2,1)S(1)} %get-tuple-element.50), channel_id=1, source_target_pairs={{0,16},{16,32},{32,48},{48,0},{1,17},{17,33},{33,49},{49,1},{2,18}... | collective-permute-start | bytes 786440 | tf_op jit(solution)/shard_map/ppermute | solution.py:427
  191.9 2.5 collective-permute-start.11
  194.4 4.0 %collective-permute-start.10 = (bf16[8,64,256]{2,1,0:T(8,128)(2,1)S(1)}, bf16[8,64,256]{2,1,0:T(8,128)(2,1)}, u32[]{:S(2)}, u32[]{:S(2)}) collective-permute-start(bf16[8,64,256]{2,1,0:T(8,128)(2,1)S(1)} %get-tuple-element.52), channel_id=1, source_target_pairs={{0,32},{16,48},{32,0},{48,16},{1,33},{17,49},{33,1},{49,17},{2,34}... | collective-permute-start | bytes 786440 | tf_op jit(solution)/shard_map/ppermute | solution.py:427
  198.5 3.9 %collective-permute-done.11 = bf16[8,64,256]{2,1,0:T(8,128)(2,1)S(1)} collective-permute-done((bf16[8,64,256]{2,1,0:T(8,128)(2,1)S(1)}, bf16[8,64,256]{2,1,0:T(8,128)(2,1)S(1)}, u32[]{:S(2)}, u32[]{:S(2)}) %collective-permute-start.11) | collective-permute-done | bytes 262176 | tf_op jit(solution)/shard_map/ppermute | solution.py:427
  202.4 5.5 %collective-permute-done.10 = bf16[8,64,256]{2,1,0:T(8,128)(2,1)} collective-permute-done((bf16[8,64,256]{2,1,0:T(8,128)(2,1)S(1)}, bf16[8,64,256]{2,1,0:T(8,128)(2,1)}, u32[]{:S(2)}, u32[]{:S(2)}) %collective-permute-start.10) | collective-permute-done | bytes 262176 | tf_op jit(solution)/shard_map/ppermute | solution.py:427
  207.9 1.8 fusion.39
  209.7 4.2 %all-to-all-start.3 = ((bf16[8,64,256]{2,1,0:T(8,128)(2,1)}), bf16[8,64,256]{2,1,0:T(8,128)(2,1)S(1)}, u32[]{:S(2)}, u32[]{:S(2)}) async-start(bf16[8,64,256]{2,1,0:T(8,128)(2,1)} %fusion.39), calls=%async_computation.3 | async-start | bytes 524288 | tf_op jit(solution)/shard_map/all_to_all | solution.py:432
  214.0 10.5 %all-to-all-done.3 = bf16[8,64,256]{2,1,0:T(8,128)(2,1)S(1)} async-done(((bf16[8,64,256]{2,1,0:T(8,128)(2,1)}), bf16[8,64,256]{2,1,0:T(8,128)(2,1)S(1)}, u32[]{:S(2)}, u32[]{:S(2)}) %all-to-all-start.3) | async-done | bytes 262176 | tf_op jit(solution)/shard_map/all_to_all | solution.py:432
  224.5 0.9 broadcast_in_dim.121
  225.4 3.7 %all-to-all-start.5 = ((bf16[8,136,256]{2,1,0:T(8,128)(2,1)}), bf16[8,136,256]{2,1,0:T(8,128)(2,1)S(1)}, u32[]{:S(2)}, u32[]{:S(2)}) async-start(bf16[8,136,256]{2,1,0:T(8,128)(2,1)} %broadcast_in_dim.121), calls=%async_computation.5 | async-start | bytes 1114112 | tf_op jit(solution)/shard_map/all_to_all | solution.py:45
  229.3 2.0 multiply_reduce_fusion
  231.3 4.9 %fusion.1 = f32[2,64,128]{2,1,0:T(8,128)S(1)} fusion(f32[2,64,128,64]{2,3,1,0:T(8,128)} %get-tuple-element.68, f32[2,64,128]{2,1,0:T(8,128)S(1)} %copy-done.15, f32[2,64,64]{2,1,0:T(8,128)S(1)} %copy.48), kind=kLoop, calls=%fused_computation.3 | loop fusion | flops 3129344 | bytes 4358144 | tf_op jit(solution)/shard_map/nts,nsd,ntsd->ntd/dot_general | solution.py:111
  236.3 0.7 convert_reduce_fusion
  237.0 7.7 %all-to-all-done.5 = bf16[8,136,256]{2,1,0:T(8,128)(2,1)S(1)} async-done(((bf16[8,136,256]{2,1,0:T(8,128)(2,1)}), bf16[8,136,256]{2,1,0:T(8,128)(2,1)S(1)}, u32[]{:S(2)}, u32[]{:S(2)}) %all-to-all-start.5) | async-done | bytes 557088 | tf_op jit(solution)/shard_map/all_to_all | solution.py:45
  245.5 0.8 multiply_subtract_fusion
  246.5 0.8 fusion.19
  247.8 0.6 broadcast_add_fusion
  (137 shorter events, 6.2 us)
Async XLA Ops:
  0.6 187.4 %copy-start = (bf16[128,256]{1,0:T(8,128)(2,1)S(1)}, bf16[128,256]{1,0:T(8,128)(2,1)}, u32[]{:S(2)}) copy-start(bf16[128,256]{1,0:T(8,128)(2,1)} %param.24) | copy-start | bytes 196612
  4.5 13.7 %copy-start.30 = (f32[128,128]{1,0:T(8,128)S(1)}, f32[128,128]{1,0:T(8,128)}, u32[]{:S(2)}) copy-start(f32[128,128]{1,0:T(8,128)} %param.28) | copy-start | bytes 196612
  4.5 13.8 %copy-start.2 = (bf16[1,2048,128]{2,1,0:T(8,128)(2,1)S(1)}, bf16[1,2048,128]{2,1,0:T(8,128)(2,1)}, u32[]{:S(2)}) copy-start(bf16[1,2048,128]{2,1,0:T(8,128)(2,1)} %param.20) | copy-start | bytes 1572868
  4.5 52.1 %all-to-all-start = ((bf16[32,24,1024]{2,1,0:T(8,128)(2,1)}), bf16[32,24,1024]{2,1,0:T(8,128)(2,1)}, u32[]{:S(2)}, u32[]{:S(2)}) async-start(bf16[32,24,1024]{2,1,0:T(8,128)(2,1)} %bitcast.304), calls=%async_computation | async-start | bytes 3145728 | tf_op jit(solution)/shard_map/all_to_all | solution.py:306
  18.2 1.0 copy-start.1
  18.3 3.7 %copy-start.32 = (f32[128]{0:T(128)}, f32[128]{0:T(128)S(1)}, u32[]{:S(2)}) copy-start(f32[128]{0:T(128)S(1)} %get-tuple-element.74) | copy-start | bytes 1540
  18.4 1.2 copy-start.12
  21.1 38.7 %copy-start.28 = (bf16[128,128]{1,0:T(8,128)(2,1)S(1)}, bf16[128,128]{1,0:T(8,128)(2,1)}, u32[]{:S(2)}) copy-start(bf16[128,128]{1,0:T(8,128)(2,1)} %param.25) | copy-start | bytes 98308
  21.1 39.4 %copy-start.13 = (bf16[128,128]{1,0:T(8,128)(2,1)S(1)}, bf16[128,128]{1,0:T(8,128)(2,1)}, u32[]{:S(2)}) copy-start(bf16[128,128]{1,0:T(8,128)(2,1)} %param.26) | copy-start | bytes 98308
  56.6 10.0 %collective-permute-start = (bf16[768,1024]{1,0:T(8,128)(2,1)}, bf16[768,1024]{1,0:T(8,128)(2,1)S(1)}, u32[]{:S(2)}, u32[]{:S(2)}) collective-permute-start(bf16[768,1024]{1,0:T(8,128)(2,1)} %bitcast.10), channel_id=1, source_target_pairs={{0,1},{1,0},{2,3},{3,2},{4,5},{5,4},{6,7},{7,6},{8,9},{9,8},{10,11... | collective-permute-start | bytes 4718600 | tf_op jit(solution)/shard_map/ppermute | solution.py:309
  66.6 1.1 copy-start.3
  68.9 0.7 copy-start.34
  69.2 0.8 copy-start.19
  69.2 0.8 copy-start.21
  69.2 3.6 %copy-start.33 = (f32[128]{0:T(128)S(1)}, f32[128]{0:T(128)}, u32[]{:S(2)}) copy-start(f32[128]{0:T(128)} %copy-done.32) | copy-start | bytes 1540
  69.2 3.6 %copy-start.31 = (bf16[64,256]{1,0:T(8,128)(2,1)S(1)}, bf16[64,256]{1,0:T(8,128)(2,1)}, u32[]{:S(2)}) copy-start(bf16[64,256]{1,0:T(8,128)(2,1)} %param.23) | copy-start | bytes 98308
  69.2 16.6 %copy-start.8 = (f32[128,128]{1,0:T(8,128)S(1)}, f32[128,128]{1,0:T(8,128)}, u32[]{:S(2)}) copy-start(f32[128,128]{1,0:T(8,128)} %convert_multiply_fusion.15) | copy-start | bytes 196612
  69.3 16.6 %copy-start.16 = (f32[2,128,64]{1,2,0:T(8,128)S(1)}, f32[2,128,64]{1,2,0:T(8,128)}, u32[]{:S(2)}) copy-start(f32[2,128,64]{1,2,0:T(8,128)} %get-tuple-element.76) | copy-start | bytes 196612
  70.4 31.8 %collective-permute-start.1 = (bf16[384,1024]{1,0:T(8,128)(2,1)S(1)}, bf16[384,1024]{1,0:T(8,128)(2,1)S(1)}, u32[]{:S(2)}, u32[]{:S(2)}) collective-permute-start(bf16[384,1024]{1,0:T(8,128)(2,1)S(1)} %convolution_convert_fusion.1), channel_id=1, source_target_pairs={{0,1},{1,0},{2,3},{3,2},{4,5},{5,4},{6,7},{7,6},{8,9},{9,8},{10,11... | collective-permute-start | bytes 2359304 | tf_op jit(solution)/shard_map/ppermute | solution.py:352
  85.8 70.3 %copy-start.11 = (bf16[256,256]{1,0:T(8,128)(2,1)}, bf16[256,256]{1,0:T(8,128)(2,1)S(1)}, u32[]{:S(2)}) copy-start(bf16[256,256]{1,0:T(8,128)(2,1)S(1)} %all_gather.7.refs_0_) | copy-start | bytes 393220
  89.6 61.7 %collective-permute-start.6 = (bf16[256,256]{1,0:T(8,128)(2,1)S(1)}, bf16[256,256]{1,0:T(8,128)(2,1)}, u32[]{:S(2)}, u32[]{:S(2)}) collective-permute-start(bf16[256,256]{1,0:T(8,128)(2,1)S(1)} %all_gather.7.refs_0_), channel_id=1, source_target_pairs={{0,320},{64,384},{128,448},{192,0},{256,64},{320,128},{384,192},{4... | collective-permute-start | bytes 393224 | tf_op jit(solution)/shard_map/ppermute | solution.py:364
  94.1 62.0 %collective-permute-start.5 = (bf16[256,256]{1,0:T(8,128)(2,1)S(1)}, bf16[256,256]{1,0:T(8,128)(2,1)}, u32[]{:S(2)}, u32[]{:S(2)}) collective-permute-start(bf16[256,256]{1,0:T(8,128)(2,1)S(1)} %all_gather.7.refs_0_), channel_id=1, source_target_pairs={{0,256},{64,320},{128,384},{192,448},{256,0},{320,64},{384,128},{4... | collective-permute-start | bytes 393224 | tf_op jit(solution)/shard_map/ppermute | solution.py:364
  102.2 0.9 copy-start.7
  103.1 10.0 %copy-start.18 = (bf16[768,128]{1,0:T(8,128)(2,1)S(1)}, bf16[768,128]{1,0:T(8,128)(2,1)}, u32[]{:S(2)}) copy-start(bf16[768,128]{1,0:T(8,128)(2,1)} %get-tuple-element.40) | copy-start | bytes 589828
  105.9 7.3 %copy-start.4 = (bf16[768,1024]{1,0:T(8,128)(2,1)S(1)}, bf16[768,1024]{1,0:T(8,128)(2,1)}, u32[]{:S(2)}) copy-start(bf16[768,1024]{1,0:T(8,128)(2,1)} %copy-done.3) | copy-start | bytes 4718596
  105.9 27.1 %all-to-all-start.1 = ((bf16[8,384,128]{2,1,0:T(8,128)(2,1)}), bf16[8,384,128]{2,1,0:T(8,128)(2,1)S(1)}, u32[]{:S(2)}, u32[]{:S(2)}) async-start(bf16[8,384,128]{2,1,0:T(8,128)(2,1)} %pair_tiles.1), calls=%async_computation.1 | async-start | bytes 1572864 | tf_op jit(solution)/shard_map/all_to_all | solution.py:355
  113.1 0.9 copy-start.20
  113.1 1.0 copy-start.22
  117.8 33.2 %copy-start.36 = (s32[128]{0:T(128)S(1)}, s32[128]{0:T(128)}, u32[]{:S(2)}) copy-start(s32[128]{0:T(128)} %get-tuple-element.82) | copy-start | bytes 1540
  117.8 33.2 %copy-start.37 = (s32[128]{0:T(128)S(1)}, s32[128]{0:T(128)}, u32[]{:S(2)}) copy-start(s32[128]{0:T(128)} %get-tuple-element.83) | copy-start | bytes 1540
  133.8 17.2 %all-to-all-start.2 = ((bf16[32,12,128]{2,1,0:T(8,128)(2,1)}), bf16[32,12,128]{2,1,0:T(8,128)(2,1)S(1)}, u32[]{:S(2)}, u32[]{:S(2)}) async-start(bf16[32,12,128]{2,1,0:T(8,128)(2,1)} %reshape.597), calls=%async_computation.2 | async-start | bytes 262144 | tf_op jit(solution)/shard_map/all_to_all | solution.py:379
  140.2 37.0 %collective-permute-start.8 = (bf16[256,256]{1,0:T(8,128)(2,1)S(1)}, bf16[256,256]{1,0:T(8,128)(2,1)S(1)}, u32[]{:S(2)}, u32[]{:S(2)}) collective-permute-start(bf16[256,256]{1,0:T(8,128)(2,1)S(1)} %all_gather.7.refs_0_), channel_id=1, source_target_pairs={{0,448},{64,0},{128,64},{192,128},{256,192},{320,256},{384,320},{4... | collective-permute-start | bytes 393224 | tf_op jit(solution)/shard_map/ppermute | solution.py:364
  144.8 32.4 %collective-permute-start.7 = (bf16[256,256]{1,0:T(8,128)(2,1)S(1)}, bf16[256,256]{1,0:T(8,128)(2,1)S(1)}, u32[]{:S(2)}, u32[]{:S(2)}) collective-permute-start(bf16[256,256]{1,0:T(8,128)(2,1)S(1)} %all_gather.7.refs_0_), channel_id=1, source_target_pairs={{0,384},{64,448},{128,0},{192,64},{256,128},{320,192},{384,256},{4... | collective-permute-start | bytes 393224 | tf_op jit(solution)/shard_map/ppermute | solution.py:364
  149.0 28.2 %collective-permute-start.4 = (bf16[256,256]{1,0:T(8,128)(2,1)S(1)}, bf16[256,256]{1,0:T(8,128)(2,1)S(1)}, u32[]{:S(2)}, u32[]{:S(2)}) collective-permute-start(bf16[256,256]{1,0:T(8,128)(2,1)S(1)} %all_gather.7.refs_0_), channel_id=1, source_target_pairs={{0,192},{64,256},{128,320},{192,384},{256,448},{320,0},{384,64},{4... | collective-permute-start | bytes 393224 | tf_op jit(solution)/shard_map/ppermute | solution.py:364
  151.3 25.9 %collective-permute-start.3 = (bf16[256,256]{1,0:T(8,128)(2,1)S(1)}, bf16[256,256]{1,0:T(8,128)(2,1)S(1)}, u32[]{:S(2)}, u32[]{:S(2)}) collective-permute-start(bf16[256,256]{1,0:T(8,128)(2,1)S(1)} %all_gather.7.refs_0_), channel_id=1, source_target_pairs={{0,128},{64,192},{128,256},{192,320},{256,384},{320,448},{384,0},{... | collective-permute-start | bytes 393224 | tf_op jit(solution)/shard_map/ppermute | solution.py:364
  156.1 21.1 %collective-permute-start.2 = (bf16[256,256]{1,0:T(8,128)(2,1)S(1)}, bf16[256,256]{1,0:T(8,128)(2,1)S(1)}, u32[]{:S(2)}, u32[]{:S(2)}) collective-permute-start(bf16[256,256]{1,0:T(8,128)(2,1)S(1)} %all_gather.7.refs_0_), channel_id=1, source_target_pairs={{0,64},{64,128},{128,192},{192,256},{256,320},{320,384},{384,448},... | collective-permute-start | bytes 393224 | tf_op jit(solution)/shard_map/ppermute | solution.py:364
  177.2 5.2 %copy-start.35 = (f32[128]{0:T(128)S(1)}, f32[128]{0:T(128)}, u32[]{:S(2)}) copy-start(f32[128]{0:T(128)} %broadcast_multiply_fusion) | copy-start | bytes 1540
  177.2 0.7 copy-start.23
  177.2 0.7 copy-start.24
  177.2 0.7 copy-start.25
  177.2 0.8 copy-start.26
  177.3 0.8 copy-start.27
  181.2 6.8 %copy-start.10 = (bf16[128,2048]{1,0:T(8,128)(2,1)S(1)}, bf16[128,2048]{1,0:T(8,128)(2,1)}, u32[]{:S(2)}) copy-start(bf16[128,2048]{1,0:T(8,128)(2,1)} %get-tuple-element.26) | copy-start | bytes 1572868
  183.2 15.2 %all-to-all-start.4 = ((bf16[4,136,256]{2,1,0:T(8,128)(2,1)}), bf16[4,136,256]{2,1,0:T(8,128)(2,1)S(1)}, u32[]{:S(2)}, u32[]{:S(2)}) async-start(bf16[4,136,256]{2,1,0:T(8,128)(2,1)} %broadcast_in_dim.120), calls=%async_computation.4 | async-start | bytes 557056 | tf_op jit(solution)/shard_map/all_to_all | solution.py:45
  188.6 9.9 %collective-permute-start.9 = (bf16[8,64,256]{2,1,0:T(8,128)(2,1)S(1)}, bf16[8,64,256]{2,1,0:T(8,128)(2,1)S(1)}, u32[]{:S(2)}, u32[]{:S(2)}) collective-permute-start(bf16[8,64,256]{2,1,0:T(8,128)(2,1)S(1)} %get-tuple-element.50), channel_id=1, source_target_pairs={{0,16},{16,32},{32,48},{48,0},{1,17},{17,33},{33,49},{49,1},{2,18}... | collective-permute-start | bytes 786440 | tf_op jit(solution)/shard_map/ppermute | solution.py:427
  191.9 10.5 %collective-permute-start.11 = (bf16[8,64,256]{2,1,0:T(8,128)(2,1)S(1)}, bf16[8,64,256]{2,1,0:T(8,128)(2,1)S(1)}, u32[]{:S(2)}, u32[]{:S(2)}) collective-permute-start(bf16[8,64,256]{2,1,0:T(8,128)(2,1)S(1)} %get-tuple-element.51), channel_id=1, source_target_pairs={{0,48},{16,0},{32,16},{48,32},{1,49},{17,1},{33,17},{49,33},{2,50}... | collective-permute-start | bytes 786440 | tf_op jit(solution)/shard_map/ppermute | solution.py:427
  194.4 13.5 %collective-permute-start.10 = (bf16[8,64,256]{2,1,0:T(8,128)(2,1)S(1)}, bf16[8,64,256]{2,1,0:T(8,128)(2,1)}, u32[]{:S(2)}, u32[]{:S(2)}) collective-permute-start(bf16[8,64,256]{2,1,0:T(8,128)(2,1)S(1)} %get-tuple-element.52), channel_id=1, source_target_pairs={{0,32},{16,48},{32,0},{48,16},{1,33},{17,49},{33,1},{49,17},{2,34}... | collective-permute-start | bytes 786440 | tf_op jit(solution)/shard_map/ppermute | solution.py:427
  209.7 19.4 %copy-start.6 = (bf16[128,256]{1,0:T(8,128)(2,1)S(1)}, bf16[128,256]{1,0:T(8,128)(2,1)}, u32[]{:S(2)}) copy-start(bf16[128,256]{1,0:T(8,128)(2,1)} %get-tuple-element.27) | copy-start | bytes 196612
  209.7 19.4 %copy-start.9 = (bf16[128,256]{1,0:T(8,128)(2,1)S(1)}, bf16[128,256]{1,0:T(8,128)(2,1)}, u32[]{:S(2)}) copy-start(bf16[128,256]{1,0:T(8,128)(2,1)} %param.27) | copy-start | bytes 196612
  209.7 14.8 %all-to-all-start.3 = ((bf16[8,64,256]{2,1,0:T(8,128)(2,1)}), bf16[8,64,256]{2,1,0:T(8,128)(2,1)S(1)}, u32[]{:S(2)}, u32[]{:S(2)}) async-start(bf16[8,64,256]{2,1,0:T(8,128)(2,1)} %fusion.39), calls=%async_computation.3 | async-start | bytes 524288 | tf_op jit(solution)/shard_map/all_to_all | solution.py:432
  225.4 5.9 %copy-start.15 = (f32[2,64,128]{2,1,0:T(8,128)S(1)}, f32[2,64,128]{2,1,0:T(8,128)}, u32[]{:S(2)}) copy-start(f32[2,64,128]{2,1,0:T(8,128)} %get-tuple-element.77) | copy-start | bytes 196612
  225.4 19.3 %all-to-all-start.5 = ((bf16[8,136,256]{2,1,0:T(8,128)(2,1)}), bf16[8,136,256]{2,1,0:T(8,128)(2,1)S(1)}, u32[]{:S(2)}, u32[]{:S(2)}) async-start(bf16[8,136,256]{2,1,0:T(8,128)(2,1)} %broadcast_in_dim.121), calls=%async_computation.5 | async-start | bytes 1114112 | tf_op jit(solution)/shard_map/all_to_all | solution.py:45
  231.3 13.7 %copy-start.14 = (bf16[128,128]{1,0:T(8,128)(2,1)S(1)}, bf16[128,128]{1,0:T(8,128)(2,1)}, u32[]{:S(2)}) copy-start(bf16[128,128]{1,0:T(8,128)(2,1)} %param.26) | copy-start | bytes 98308
  236.3 9.2 %copy-start.5 = (f32[1,1,128,256]{3,2,1,0:T(8,128)S(1)}, f32[1,1,128,256]{3,2,1,0:T(8,128)}, u32[]{:S(2)}) copy-start(f32[1,1,128,256]{3,2,1,0:T(8,128)} %param.29) | copy-start | bytes 393220
  236.3 9.2 %copy-start.17 = (bf16[1,128,256]{2,1,0:T(8,128)(2,1)S(1)}, bf16[1,128,256]{2,1,0:T(8,128)(2,1)}, u32[]{:S(2)}) copy-start(bf16[1,128,256]{2,1,0:T(8,128)(2,1)} %multiply_add_fusion.3) | copy-start | bytes 196612
  236.3 9.2 %copy-start.29 = (bf16[128,128]{1,0:T(8,128)(2,1)S(1)}, bf16[128,128]{1,0:T(8,128)(2,1)}, u32[]{:S(2)}) copy-start(bf16[128,128]{1,0:T(8,128)(2,1)} %param.25) | copy-start | bytes 98308

commit v6 on v5

--- a/solution.py
+++ b/solution.py
@@ -76,22 +76,11 @@
     end_state, starts = lax.scan(
         forward_step, entry_state, (inner_part, block_total), unroll=True
     )
-    own_part = jnp.einsum("ntd,ntj->ndj", query_blk * jnp.exp(cumlog), grad_blk)
-
-    def backward_step(carry_state, step_item):
-        piece_part, block_sum = step_item
-        return (jnp.exp(block_sum)[:, None] * carry_state + piece_part, carry_state)
-
-    start_cot, after_cot = lax.scan(
-        backward_step,
-        jnp.zeros_like(entry_state),
-        (own_part, block_total),
-        reverse=True,
-        unroll=True,
-    )
+    second_part = jnp.einsum("td,tj->dj", query_blk[1] * jnp.exp(cumlog[1]), grad_blk[1])
+    after_cot = jnp.stack([second_part, jnp.zeros_like(second_part)])
     span_total = jnp.sum(block_total, axis=0)
     later_log = span_total[None, :] - jnp.cumsum(block_total, axis=0)
-    return ((cumlog, starts, after_cot, later_log, end_state), (jnp.exp(span_total), start_cot))
+    return (cumlog, starts, after_cot, later_log, end_state)
 
 
 def span_backward(query_rows, key_rows, value_rows, grad_rows, kept_terms, exit_cot):
@@ -207,28 +196,10 @@
     )(core.astype(jnp.int32).reshape(1), ids.T, weight.T, resid, cotangent, gain.reshape(1, -1))
 
 
-def pair_tiles_kernel(own_ref, passed_ref, out_ref):
-    width = out_ref.shape[2]
-    for k in range(out_ref.shape[0]):
-        cols = slice(k * width, (k + 1) * width)
-        total = own_ref[:, cols] + passed_ref[:, cols].astype(jnp.float32)
-        out_ref[k] = total.astype(jnp.bfloat16)
-
-
-def pair_tiles(own, passed, count):
-    rows, width = own.shape
-    vmem = pl.BlockSpec(memory_space=pltpu.VMEM)
-    return pl.pallas_call(
-        pair_tiles_kernel,
-        out_shape=jax.ShapeDtypeStruct((count, rows, width // count), jnp.bfloat16),
-        in_specs=[vmem, vmem],
-        out_specs=vmem,
-        name="pair_tiles",
-    )(own, passed)
-
-
-def resid_mixed_kernel(place_ref, normed_ref, cot_ref, resid_ref, gain_ref, *refs):
-    blocks, (out_ref, mixed_ref) = refs[:8], refs[8:]
+def resid_mixed_kernel(
+    place_ref, normed_ref, cot_ref, resid_ref, gain_ref, query_ref, decay_ref, *refs
+):
+    blocks, (out_ref, mixed_ref, near_ref) = refs[:8], refs[8:]
     tokens = resid_ref.shape[0]
     for at in range(0, tokens, 32):
         rows = slice(at, at + 32)
@@ -246,19 +217,28 @@
         total = total + jnp.dot(
             out_ref[:, pl.ds(at, depth)], blocks[k][...], preferred_element_type=jnp.float32
         )
-    mixed_ref[...] = total.astype(jnp.bfloat16)
-
-
-def resid_mixed(place, grad_normed, cotangent, resid, gain, blocks):
+    mixed = total.astype(jnp.bfloat16)
+    mixed_ref[...] = mixed
+    state = jnp.dot(query_ref[...], mixed, preferred_element_type=jnp.float32)
+    keys = state.shape[0]
+    for k in range(near_ref.shape[0]):
+        near_ref[k, :keys, :] = state.astype(jnp.bfloat16)
+        near_ref[k, keys:, :] = decay_ref[...].astype(jnp.bfloat16)
+
+
+def resid_mixed(place, grad_normed, cotangent, resid, gain, blocks, query_cols, decay_row, copies):
     vmem = pl.BlockSpec(memory_space=pltpu.VMEM)
     return pl.pallas_call(
         resid_mixed_kernel,
         out_shape=(
             jax.ShapeDtypeStruct(resid.shape, jnp.bfloat16),
             jax.ShapeDtypeStruct((resid.shape[0], blocks[0].shape[1]), jnp.bfloat16),
+            jax.ShapeDtypeStruct(
+                (copies, query_cols.shape[0] + decay_row.shape[0], blocks[0].shape[1]), jnp.bfloat16
+            ),
         ),
-        in_specs=[pl.BlockSpec(memory_space=pltpu.SMEM)] + [vmem] * 12,
-        out_specs=(vmem, vmem),
+        in_specs=[pl.BlockSpec(memory_space=pltpu.SMEM)] + [vmem] * 14,
+        out_specs=(vmem, vmem, vmem),
         name="resid_mixed",
     )(
         place.astype(jnp.int32).reshape(1),
@@ -266,6 +246,8 @@
         cotangent,
         resid,
         gain.reshape(1, -1),
+        query_cols,
+        decay_row,
         *blocks,
     )
 
@@ -350,17 +332,16 @@
         )
 
     passed = lax.ppermute(onto(out_other).astype(jnp.bfloat16), "c", [(0, 1), (1, 0)])
-    own_parts = onto(out_own)
-    parts = pair_tiles(own_parts, passed, y_count)
+    pair_sum = (onto(out_own) + passed.astype(jnp.float32)).astype(jnp.bfloat16)
+    parts = pair_sum.reshape(slots, y_count, width).transpose(1, 0, 2)
     swapped = lax.all_to_all(parts, "y", 0, 0, tiled=True)
     summed = sum_parts(swapped).astype(jnp.bfloat16)
     proj_tied, _ = lax.optimization_barrier((proj_near, parts))
     proj_early, _ = lax.optimization_barrier((proj_near, own))
-    proj_mid, _ = lax.optimization_barrier((proj_near, acts))
     z_place = lax.axis_index("z")
     blocks = [proj_near] + [None] * 7
     for k in range(1, 8):
-        sent_block = proj_early if k == 5 else proj_mid if k == 4 else proj_tied
+        sent_block = proj_near if k in (1, 7) else proj_early if k == 5 else proj_tied
         blocks[k] = lax.ppermute(sent_block, "z", [(i, (i + k) % 8) for i in range(8)])
 
     def beside(values):
@@ -392,22 +373,35 @@
         axis=1,
         tiled=True,
     )
-    grad_resid, grad_mixed = resid_mixed(
-        z_place, grad_normed, cotangent, resid, norm_gain, blocks
+    query_scale = KEY_CHANNELS ** (-0.5)
+    query_rows = query.astype(jnp.float32) * query_scale
+    span_log = jnp.cumsum(into_blocks(log_decay), axis=1)
+    span_log = jnp.concatenate([span_log[0], span_log[1] + span_log[0, -1:]], axis=0)
+    query_cols = jnp.transpose(query_rows * jnp.exp(span_log)).astype(jnp.bfloat16)
+    decay_row = jnp.pad(
+        jnp.exp(span_log[-1:]), ((0, 7), (0, out_proj.shape[1] - KEY_CHANNELS))
+    )
+    grad_resid, grad_mixed, near_sent = resid_mixed(
+        z_place,
+        grad_normed,
+        cotangent,
+        resid,
+        norm_gain,
+        blocks,
+        query_cols,
+        decay_row,
+        lax.axis_size("x"),
     )
     share = lax.dot_general(
         grad_resid, mixed, (((0,), (0,)), ((), ())), preferred_element_type=jnp.float32
     ).astype(jnp.bfloat16)
-    query_scale = KEY_CHANNELS ** (-0.5)
-    query_rows = query.astype(jnp.float32) * query_scale
     key_rows = key.astype(jnp.float32)
     value_rows = value.astype(jnp.float32)
     grad_rows = grad_mixed.astype(jnp.float32)
-    kept_terms, summary = span_forward(
+    kept_terms = span_forward(
         query_rows, key_rows, value_rows, grad_rows, log_decay, span_state[0, 0]
     )
-    own_decay, own_state = summary
-    near_filled = to_all(with_decay(own_state, own_decay), "x")
+    near_filled = lax.all_to_all(near_sent, "x", 0, 0, tiled=True)
     near_states, near_decays = split_decay(near_filled)
     near_sum, near_factor = later_sum(near_states, near_decays, lax.axis_index("x"))
     group_sum, group_factor = later_sum(near_states, near_decays, -1)

time: 250 us -> 230 us (0.920)
  waiting for transfers between devices: 76.8 us -> 56.7 us
  starting transfers between devices: 81 us -> 85.5 us
    all_to_all x1, waiting for transfers between devices: 34 us -> 10.7 us  [on_device_body(): own = lax.all_to_all(sent, SP, 0, 0, tiled=True).reshape(2 * slots, half)]
    all_to_all x0 -> x1, starting transfers between devices: none -> 4.8 us  [on_device_body(): near_filled = lax.all_to_all(near_sent, 'x', 0, 0, tiled=True)]
    all_to_all x2 -> x1, starting transfers between devices: 8.46 us -> 3.67 us  [to_all(): return lax.all_to_all(copies, axis, 0, 0, tiled=True)]
    all_to_all x1, starting transfers between devices: 5.54 us -> 8.67 us  [on_device_body(): lax.all_to_all(summed.reshape(experts, capacity, -1), SP, split_axis=0, c...]
    all_to_all x1, waiting for transfers between devices: 15.2 us -> 18.2 us  [on_device_body(): swapped = lax.all_to_all(parts, 'y', 0, 0, tiled=True)]
    pallas_call x1 -> x0, Pallas kernels: 2.73 us -> none  [pair_tiles(): pl.pallas_call(pair_tiles_kernel, out_shape=jax.ShapeDtypeStruct((count,...]
    all_to_all x2 -> x1, waiting for transfers between devices: 7.71 us -> 7.51 us  [to_all(): return lax.all_to_all(copies, axis, 0, 0, tiled=True)]
  transfers between devices with their start and end apart: 18 -> 18, of which waited for: 6 -> 6; matrix products, arithmetic and copies ran while one was open for 14% -> 17% of each run, Pallas kernels for 1% -> 0%
where the time goes in v6:
time: 230 us; the launch traced here: 228 us
  starting transfers between devices  85.5 us (37%)
  waiting for transfers between devices  56.7 us (25%)
  blocking collectives  31.3 us (14%)
  other arithmetic  22.5 us (10%)
  matrix products  12.1 us (5%)
  local copies, waits for them, and re-layouts  11.5 us (5%)
  Pallas kernels  7.29 us (3%)
    ppermute x7, starting transfers between devices, on_device_body(): lax.ppermute(sent_block, 'z', [(i, (i + k) % 8) for i in range(8)])  28.2 us
    all_to_all x1, waiting for transfers between devices, on_device_body(): swapped = lax.all_to_all(parts, 'y', 0, 0, tiled=True)  18.2 us
    all_gather x1, blocking collectives, on_device_body(): lax.all_gather(lax.dot_general(slot_tokens, flat_rows, (((0,), (0,)), (()...  17.5 us
    all_gather x1, blocking collectives, on_device_body(): proj_near = lax.all_gather(proj_near, 'x', axis=0, tiled=True)  13.7 us
    all_to_all x1, starting transfers between devices, on_device_body(): own = lax.all_to_all(sent, SP, 0, 0, tiled=True).reshape(2 * slots, half)  13.7 us
    all_to_all x1, waiting for transfers between devices, on_device_body(): share_z = lax.all_to_all(share_z, 'z', 0, 0, tiled=True)  10.8 us
    all_to_all x1, waiting for transfers between devices, on_device_body(): own = lax.all_to_all(sent, SP, 0, 0, tiled=True).reshape(2 * slots, half)  10.7 us
    ppermute x3, starting transfers between devices, on_device_body(): lax.ppermute(for_place(k), 'x', [(i, (i + k) % 4) for i in range(4)])  9.82 us
  transfers between devices with their start and end apart: 18, of which 6 were waited for; matrix products, arithmetic and copies ran while one was open for 17% of the time, Pallas kernels for 0%

profile of v6, /device:TPU:2, one launch (start us, length us, event | category | flops | bytes accessed | tf_op | source)
XLA Modules:
  0.0 228.5 jit_solution(18213985310920527494)
XLA Ops:
  0.7 3.8 %dispatch_rows.1 = (bf16[768,1024]{1,0:T(8,128)(2,1)}, s32[8,128]{1,0:T(8,128)}) custom-call(s32[1]{0:T(128)} %bitcast.5.core_ref, s32[2,128]{1,0:T(2,128)} %bitcast.352, f32[2,128]{1,0:T(2,128)} %bitcast.353, bf16[128,2048]{1,0:T(8,128)(2,1)} %resid_ref.3, bf16[128,2048]{1,0:T(8,128)(2,1)} %cot_ref.3, f32[1,2048]{1,0:T(1,128)} %bitcast.344), custom_call_target="tpu_custom_call" | custom-call | tf_op jit(solution)/shard_map/dispatch_rows/pallas_call | solution.py:186
  4.5 13.7 %all-to-all-start = ((bf16[32,24,1024]{2,1,0:T(8,128)(2,1)}), bf16[32,24,1024]{2,1,0:T(8,128)(2,1)}, u32[]{:S(2)}, u32[]{:S(2)}) async-start(bf16[32,24,1024]{2,1,0:T(8,128)(2,1)} %bitcast.320), calls=%async_computation | async-start | bytes 3145728 | tf_op jit(solution)/shard_map/all_to_all | solution.py:288
  18.2 13.7 %all_gather.7.refs_0_ = bf16[256,256]{1,0:T(8,128)(2,1)} all-gather(bf16[64,256]{1,0:T(8,128)(2,1)S(1)} %copy-done.27), channel_id=1, replica_groups=mesh['z'=8,'x'=4,'y'=8,'c'=2] {'x'}, dimensions={0}, use_global_device_ids=true | all-gather | bytes 163840 | tf_op jit(solution)/shard_map/all_gather | solution.py:290
  31.9 5.4 %collective-permute-start.8 = (bf16[256,256]{1,0:T(8,128)(2,1)}, bf16[256,256]{1,0:T(8,128)(2,1)}, u32[]{:S(2)}, u32[]{:S(2)}) collective-permute-start(bf16[256,256]{1,0:T(8,128)(2,1)} %all_gather.7.refs_0_), channel_id=1, source_target_pairs={{0,448},{64,0},{128,64},{192,128},{256,192},{320,256},{384,320},{4... | collective-permute-start | bytes 393224 | tf_op jit(solution)/shard_map/ppermute | solution.py:345
  37.3 1.9 collective-permute-start.2
  39.4 0.5 slice_reduce_fusion
  39.9 0.6 reduce_window_sum.35
  40.5 0.6 fusion.124
  41.1 0.6 pad.14.decay_ref
  41.7 0.6 convert_multiply_fusion.15
  42.3 0.7 copy.62.query_ref
  43.3 0.9 copy.84
  44.2 0.9 copy.85
  45.0 0.8 copy.86
  45.9 1.6 broadcast_select_fusion
  47.6 10.7 %all-to-all-done = bf16[32,24,1024]{2,1,0:T(8,128)(2,1)} async-done(((bf16[32,24,1024]{2,1,0:T(8,128)(2,1)}), bf16[32,24,1024]{2,1,0:T(8,128)(2,1)}, u32[]{:S(2)}, u32[]{:S(2)}) %all-to-all-start) | async-done | bytes 1572896 | tf_op jit(solution)/shard_map/all_to_all | solution.py:288
  58.3 1.9 collective-permute-start
  60.6 1.4 slice_bitcast_fusion.12
  61.9 0.6 convert_bitcast_fusion.10
  62.8 2.4 %fusion.139 = f32[768,512]{1,0:T(8,128)S(1)} fusion(bf16[768,1024]{1,0:T(8,128)(2,1)} %bitcast.10, bf16[1024,512]{0,1:T(8,128)(2,1)S(1)} %get-tuple-element.20), kind=kOutput, calls=%fused_computation.261 | convolution fusion | flops 805306368 | bytes 4194304 | tf_op jit(solution)/shard_map/dot_general | solution.py:302
  65.3 1.0 broadcast_select_fusion.2
  68.0 0.4 convolution_convert_fusion.1
  68.4 2.4 %collective-permute-start.1 = (bf16[384,1024]{1,0:T(8,128)(2,1)S(1)}, bf16[384,1024]{1,0:T(8,128)(2,1)S(1)}, u32[]{:S(2)}, u32[]{:S(2)}) collective-permute-start(bf16[384,1024]{1,0:T(8,128)(2,1)S(1)} %convolution_convert_fusion.1), channel_id=1, source_target_pairs={{0,1},{1,0},{2,3},{3,2},{4,5},{5,4},{6,7},{7,6},{8,9},{9,8},{10,11... | collective-permute-start | bytes 2359304 | tf_op jit(solution)/shard_map/ppermute | solution.py:334
  70.8 0.7 multiply_add_fusion.3
  71.6 3.8 %fusion = (bf16[2,64,64]{2,1,0:T(8,128)(2,1)S(1)}, f32[2,64,128,64]{2,3,1,0:T(8,128)}) fusion(f32[2,128,64]{1,2,0:T(8,128)S(1)} %get-tuple-element.74, f32[2,128,64]{1,2,0:T(8,128)S(1)} %bitcast.335, f32[2,64,128]{2,1,0:T(8,128)S(1)} %reduce_window_sum.34, pred[64,64]{1,0:T(8,128)(4,1)S(1)} %iota_compare_fusion.9), kind=kLoop, calls=%fused_computation.1 | loop fusion | flops 5234688 | bytes 4411392 | tf_op jit(solution)/shard_map/ntd,nsd,ntsd->nts/dot_general | solution.py:97
  75.3 3.0 %collective-permute-start.6 = (bf16[256,256]{1,0:T(8,128)(2,1)}, bf16[256,256]{1,0:T(8,128)(2,1)}, u32[]{:S(2)}, u32[]{:S(2)}) collective-permute-start(bf16[256,256]{1,0:T(8,128)(2,1)} %all_gather.7.refs_0_), channel_id=1, source_target_pairs={{0,320},{64,384},{128,448},{192,0},{256,64},{320,128},{384,192},{4... | collective-permute-start | bytes 393224 | tf_op jit(solution)/shard_map/ppermute | solution.py:345
  78.3 0.5 slice.366
  78.8 0.4 fusion.24
  79.2 1.1 copy.90
  80.3 7.2 %all-to-all-start.1 = ((bf16[8,384,128]{2,1,0:T(8,128)(2,1)}), bf16[8,384,128]{2,1,0:T(8,128)(2,1)S(1)}, u32[]{:S(2)}, u32[]{:S(2)}) async-start(bf16[8,384,128]{2,1,0:T(8,128)(2,1)} %bitcast.310), calls=%async_computation.1 | async-start | bytes 1572864 | tf_op jit(solution)/shard_map/all_to_all | solution.py:337
  87.6 0.6 fusion.14
  88.7 2.5 %fusion.11 = bf16[1024,512]{1,0:T(8,128)(2,1)S(1)} fusion(bf16[768,1024]{1,0:T(8,128)(2,1)} %bitcast.10, bf16[768,1024]{1,0:T(8,128)(2,1)S(1)} %copy-done.4, pred[]{:T(512)S(6)} %eq.48, bf16[767,128]{1,0:T(8,128)(2,1)S(1)} %bitcast.341, bf16[1,128]{1,0:T(2,128)(2,1)S(1)} %slice.360, bf16[768,128]{1,0:T(8,128)(2,1)S(1)} %copy-done.19, ...), kind=kOutput, calls=%fused_computation.18 | convolution fusion | flops 811335680 | bytes 4980737 | tf_op jit(solution)/shard_map/dot_general | solution.py:37
  91.3 1.0 maximum_bitcast_fusion
  92.4 18.2 %all-to-all-done.1 = bf16[8,384,128]{2,1,0:T(8,128)(2,1)S(1)} async-done(((bf16[8,384,128]{2,1,0:T(8,128)(2,1)}), bf16[8,384,128]{2,1,0:T(8,128)(2,1)S(1)}, u32[]{:S(2)}, u32[]{:S(2)}) %all-to-all-start.1) | async-done | bytes 786464 | tf_op jit(solution)/shard_map/all_to_all | solution.py:337
  110.7 0.7 reshape.572
  111.4 8.7 %all-to-all-start.2 = ((bf16[32,12,128]{2,1,0:T(8,128)(2,1)}), bf16[32,12,128]{2,1,0:T(8,128)(2,1)S(1)}, u32[]{:S(2)}, u32[]{:S(2)}) async-start(bf16[32,12,128]{2,1,0:T(8,128)(2,1)} %reshape.572), calls=%async_computation.2 | async-start | bytes 262144 | tf_op jit(solution)/shard_map/all_to_all | solution.py:360
  120.1 0.8 maximum_bitcast_fusion.2
  120.9 5.5 %collective-permute-start.7 = (bf16[256,256]{1,0:T(8,128)(2,1)}, bf16[256,256]{1,0:T(8,128)(2,1)S(1)}, u32[]{:S(2)}, u32[]{:S(2)}) collective-permute-start(bf16[256,256]{1,0:T(8,128)(2,1)} %all_gather.7.refs_0_), channel_id=1, source_target_pairs={{0,384},{64,448},{128,0},{192,64},{256,128},{320,192},{384,256},{4... | collective-permute-start | bytes 393224 | tf_op jit(solution)/shard_map/ppermute | solution.py:345
  126.4 4.2 %collective-permute-start.5 = (bf16[256,256]{1,0:T(8,128)(2,1)}, bf16[256,256]{1,0:T(8,128)(2,1)S(1)}, u32[]{:S(2)}, u32[]{:S(2)}) collective-permute-start(bf16[256,256]{1,0:T(8,128)(2,1)} %all_gather.7.refs_0_), channel_id=1, source_target_pairs={{0,256},{64,320},{128,384},{192,448},{256,0},{320,64},{384,128},{4... | collective-permute-start | bytes 393224 | tf_op jit(solution)/shard_map/ppermute | solution.py:345
  131.0 4.3 %collective-permute-start.4 = (bf16[256,256]{1,0:T(8,128)(2,1)}, bf16[256,256]{1,0:T(8,128)(2,1)S(1)}, u32[]{:S(2)}, u32[]{:S(2)}) collective-permute-start(bf16[256,256]{1,0:T(8,128)(2,1)} %all_gather.7.refs_0_), channel_id=1, source_target_pairs={{0,192},{64,256},{128,320},{192,384},{256,448},{320,0},{384,64},{4... | collective-permute-start | bytes 393224 | tf_op jit(solution)/shard_map/ppermute | solution.py:345
  135.3 3.9 %collective-permute-start.3 = (bf16[256,256]{1,0:T(8,128)(2,1)}, bf16[256,256]{1,0:T(8,128)(2,1)S(1)}, u32[]{:S(2)}, u32[]{:S(2)}) collective-permute-start(bf16[256,256]{1,0:T(8,128)(2,1)} %all_gather.7.refs_0_), channel_id=1, source_target_pairs={{0,128},{64,192},{128,256},{192,320},{256,384},{320,448},{384,0},{... | collective-permute-start | bytes 393224 | tf_op jit(solution)/shard_map/ppermute | solution.py:345
  139.2 17.5 %all_gather.6.normed_ref = bf16[128,2048]{1,0:T(8,128)(2,1)} all-gather(bf16[128,128]{1,0:T(8,128)(2,1)S(1)} %convolution_convert_fusion.2), channel_id=1, replica_groups=mesh['z'=8,'x'=4,'y'=8,'c'=2] {'y','c'}, dimensions={1}, use_global_device_ids=true | all-gather | bytes 557056 | tf_op jit(solution)/shard_map/all_gather | solution.py:368
  156.8 0.6 copy-done.20
  157.6 3.5 %resid_mixed.1 = (bf16[128,2048]{1,0:T(8,128)(2,1)}, bf16[128,256]{1,0:T(8,128)(2,1)}, bf16[4,136,256]{2,1,0:T(8,128)(2,1)}) custom-call(s32[1]{0:T(128)} %bitcast.21.place_ref, bf16[128,2048]{1,0:T(8,128)(2,1)} %all_gather.6.normed_ref, bf16[128,2048]{1,0:T(8,128)(2,1)} %cot_ref.3, bf16[128,2048]{1,0:T(8,128)(2,1)} %resid_ref.3, f32[1,2048]{1,0:T(1,128)} %bitcast.345, ...), custom_call_target="tpu_custom_call" | custom-call | tf_op jit(solution)/shard_map/resid_mixed/pallas_call | solution.py:231
  161.0 4.8 %all-to-all-start.4 = ((bf16[4,136,256]{2,1,0:T(8,128)(2,1)}), bf16[4,136,256]{2,1,0:T(8,128)(2,1)S(1)}, u32[]{:S(2)}, u32[]{:S(2)}) async-start(bf16[4,136,256]{2,1,0:T(8,128)(2,1)} %get-tuple-element.27), calls=%async_computation.4 | async-start | bytes 557056 | tf_op jit(solution)/shard_map/all_to_all | solution.py:404
  165.8 1.5 convolution_convert_fusion
  167.4 3.4 %collective-permute-start.9 = (bf16[8,64,256]{2,1,0:T(8,128)(2,1)S(1)}, bf16[8,64,256]{2,1,0:T(8,128)(2,1)S(1)}, u32[]{:S(2)}, u32[]{:S(2)}) collective-permute-start(bf16[8,64,256]{2,1,0:T(8,128)(2,1)S(1)} %get-tuple-element.48), channel_id=1, source_target_pairs={{0,16},{16,32},{32,48},{48,0},{1,17},{17,33},{33,49},{49,1},{2,18}... | collective-permute-start | bytes 786440 | tf_op jit(solution)/shard_map/ppermute | solution.py:421
  170.8 2.5 %collective-permute-start.11 = (bf16[8,64,256]{2,1,0:T(8,128)(2,1)S(1)}, bf16[8,64,256]{2,1,0:T(8,128)(2,1)S(1)}, u32[]{:S(2)}, u32[]{:S(2)}) collective-permute-start(bf16[8,64,256]{2,1,0:T(8,128)(2,1)S(1)} %get-tuple-element.49), channel_id=1, source_target_pairs={{0,48},{16,0},{32,16},{48,32},{1,49},{17,1},{33,17},{49,33},{2,50}... | collective-permute-start | bytes 786440 | tf_op jit(solution)/shard_map/ppermute | solution.py:421
  173.3 4.0 %collective-permute-start.10 = (bf16[8,64,256]{2,1,0:T(8,128)(2,1)S(1)}, bf16[8,64,256]{2,1,0:T(8,128)(2,1)}, u32[]{:S(2)}, u32[]{:S(2)}) collective-permute-start(bf16[8,64,256]{2,1,0:T(8,128)(2,1)S(1)} %get-tuple-element.50), channel_id=1, source_target_pairs={{0,32},{16,48},{32,0},{48,16},{1,33},{17,49},{33,1},{49,17},{2,34}... | collective-permute-start | bytes 786440 | tf_op jit(solution)/shard_map/ppermute | solution.py:421
  177.3 3.9 %collective-permute-done.11 = bf16[8,64,256]{2,1,0:T(8,128)(2,1)S(1)} collective-permute-done((bf16[8,64,256]{2,1,0:T(8,128)(2,1)S(1)}, bf16[8,64,256]{2,1,0:T(8,128)(2,1)S(1)}, u32[]{:S(2)}, u32[]{:S(2)}) %collective-permute-start.11) | collective-permute-done | bytes 262176 | tf_op jit(solution)/shard_map/ppermute | solution.py:421
  181.3 5.5 %collective-permute-done.10 = bf16[8,64,256]{2,1,0:T(8,128)(2,1)} collective-permute-done((bf16[8,64,256]{2,1,0:T(8,128)(2,1)S(1)}, bf16[8,64,256]{2,1,0:T(8,128)(2,1)}, u32[]{:S(2)}, u32[]{:S(2)}) %collective-permute-start.10) | collective-permute-done | bytes 262176 | tf_op jit(solution)/shard_map/ppermute | solution.py:421
  186.7 1.8 fusion.40
  188.5 5.1 %all-to-all-start.3 = ((bf16[8,64,256]{2,1,0:T(8,128)(2,1)}), bf16[8,64,256]{2,1,0:T(8,128)(2,1)S(1)}, u32[]{:S(2)}, u32[]{:S(2)}) async-start(bf16[8,64,256]{2,1,0:T(8,128)(2,1)} %fusion.40), calls=%async_computation.3 | async-start | bytes 524288 | tf_op jit(solution)/shard_map/all_to_all | solution.py:426
  193.8 10.8 %all-to-all-done.3 = bf16[8,64,256]{2,1,0:T(8,128)(2,1)S(1)} async-done(((bf16[8,64,256]{2,1,0:T(8,128)(2,1)}), bf16[8,64,256]{2,1,0:T(8,128)(2,1)S(1)}, u32[]{:S(2)}, u32[]{:S(2)}) %all-to-all-start.3) | async-done | bytes 262176 | tf_op jit(solution)/shard_map/all_to_all | solution.py:426
  204.6 0.9 broadcast_in_dim.109
  205.5 3.7 %all-to-all-start.5 = ((bf16[8,136,256]{2,1,0:T(8,128)(2,1)}), bf16[8,136,256]{2,1,0:T(8,128)(2,1)S(1)}, u32[]{:S(2)}, u32[]{:S(2)}) async-start(bf16[8,136,256]{2,1,0:T(8,128)(2,1)} %broadcast_in_dim.109), calls=%async_computation.5 | async-start | bytes 1114112 | tf_op jit(solution)/shard_map/all_to_all | solution.py:45
  209.6 2.0 multiply_reduce_fusion
  211.6 4.9 %fusion.1 = f32[2,64,128]{2,1,0:T(8,128)S(1)} fusion(f32[2,64,128,64]{2,3,1,0:T(8,128)} %get-tuple-element.66, f32[2,64,128]{2,1,0:T(8,128)S(1)} %copy-done.12, f32[2,64,64]{2,1,0:T(8,128)S(1)} %copy.63), kind=kLoop, calls=%fused_computation.3 | loop fusion | flops 3129344 | bytes 4358144 | tf_op jit(solution)/shard_map/nts,nsd,ntsd->ntd/dot_general | solution.py:100
  216.6 0.7 convert_reduce_fusion
  217.2 7.5 %all-to-all-done.5 = bf16[8,136,256]{2,1,0:T(8,128)(2,1)S(1)} async-done(((bf16[8,136,256]{2,1,0:T(8,128)(2,1)}), bf16[8,136,256]{2,1,0:T(8,128)(2,1)S(1)}, u32[]{:S(2)}, u32[]{:S(2)}) %all-to-all-start.5) | async-done | bytes 557088 | tf_op jit(solution)/shard_map/all_to_all | solution.py:45
  225.6 0.8 multiply_subtract_fusion
  226.6 0.8 fusion.19
  227.5 0.4 fusion.67
  227.8 0.6 broadcast_add_fusion
  (134 shorter events, 5.4 us)
Async XLA Ops:
  0.6 165.2 %copy-start = (bf16[128,256]{1,0:T(8,128)(2,1)S(1)}, bf16[128,256]{1,0:T(8,128)(2,1)}, u32[]{:S(2)}) copy-start(bf16[128,256]{1,0:T(8,128)(2,1)} %param.24) | copy-start | bytes 196612
  4.5 13.7 %copy-start.27 = (bf16[64,256]{1,0:T(8,128)(2,1)S(1)}, bf16[64,256]{1,0:T(8,128)(2,1)}, u32[]{:S(2)}) copy-start(bf16[64,256]{1,0:T(8,128)(2,1)} %param.23) | copy-start | bytes 98308
  4.5 34.8 %copy-start.26 = (f32[128,128]{1,0:T(8,128)S(1)}, f32[128,128]{1,0:T(8,128)}, u32[]{:S(2)}) copy-start(f32[128,128]{1,0:T(8,128)} %param.28) | copy-start | bytes 196612
  4.5 37.2 %copy-start.24 = (bf16[128,128]{1,0:T(8,128)(2,1)S(1)}, bf16[128,128]{1,0:T(8,128)(2,1)}, u32[]{:S(2)}) copy-start(bf16[128,128]{1,0:T(8,128)(2,1)} %param.25) | copy-start | bytes 98308
  4.5 38.6 %copy-start.2 = (bf16[1,2048,128]{2,1,0:T(8,128)(2,1)S(1)}, bf16[1,2048,128]{2,1,0:T(8,128)(2,1)}, u32[]{:S(2)}) copy-start(bf16[1,2048,128]{2,1,0:T(8,128)(2,1)} %param.20) | copy-start | bytes 1572868
  4.5 53.8 %all-to-all-start = ((bf16[32,24,1024]{2,1,0:T(8,128)(2,1)}), bf16[32,24,1024]{2,1,0:T(8,128)(2,1)}, u32[]{:S(2)}, u32[]{:S(2)}) async-start(bf16[32,24,1024]{2,1,0:T(8,128)(2,1)} %bitcast.320), calls=%async_computation | async-start | bytes 3145728 | tf_op jit(solution)/shard_map/all_to_all | solution.py:288
  18.2 25.9 %copy-start.1 = (bf16[1,2048,128]{2,1,0:T(8,128)(2,1)S(1)}, bf16[1,2048,128]{2,1,0:T(8,128)(2,1)}, u32[]{:S(2)}) copy-start(bf16[1,2048,128]{2,1,0:T(8,128)(2,1)} %param.21) | copy-start | bytes 1572868
  31.9 99.1 %collective-permute-start.8 = (bf16[256,256]{1,0:T(8,128)(2,1)}, bf16[256,256]{1,0:T(8,128)(2,1)}, u32[]{:S(2)}, u32[]{:S(2)}) collective-permute-start(bf16[256,256]{1,0:T(8,128)(2,1)} %all_gather.7.refs_0_), channel_id=1, source_target_pairs={{0,448},{64,0},{128,64},{192,128},{256,192},{320,256},{384,320},{4... | collective-permute-start | bytes 393224 | tf_op jit(solution)/shard_map/ppermute | solution.py:345
  37.3 98.0 %collective-permute-start.2 = (bf16[256,256]{1,0:T(8,128)(2,1)}, bf16[256,256]{1,0:T(8,128)(2,1)}, u32[]{:S(2)}, u32[]{:S(2)}) collective-permute-start(bf16[256,256]{1,0:T(8,128)(2,1)} %all_gather.7.refs_0_), channel_id=1, source_target_pairs={{0,64},{64,128},{128,192},{192,256},{256,320},{320,384},{384,448},... | collective-permute-start | bytes 393224 | tf_op jit(solution)/shard_map/ppermute | solution.py:345
  43.1 2.8 %copy-start.8 = (bf16[1,128,2048]{2,1,0:T(8,128)(2,1)S(1)}, bf16[1,128,2048]{2,1,0:T(8,128)(2,1)}, u32[]{:S(2)}) copy-start(bf16[1,128,2048]{2,1,0:T(8,128)(2,1)} %param.22) | copy-start | bytes 1572868
  47.5 14.4 %copy-start.9 = (bf16[128,128]{1,0:T(8,128)(2,1)S(1)}, bf16[128,128]{1,0:T(8,128)(2,1)}, u32[]{:S(2)}) copy-start(bf16[128,128]{1,0:T(8,128)(2,1)} %param.26) | copy-start | bytes 98308
  47.6 15.0 %copy-start.7 = (bf16[128,256]{1,0:T(8,128)(2,1)S(1)}, bf16[128,256]{1,0:T(8,128)(2,1)}, u32[]{:S(2)}) copy-start(bf16[128,256]{1,0:T(8,128)(2,1)} %param.27) | copy-start | bytes 196612
  58.3 6.9 %collective-permute-start = (bf16[768,1024]{1,0:T(8,128)(2,1)}, bf16[768,1024]{1,0:T(8,128)(2,1)S(1)}, u32[]{:S(2)}, u32[]{:S(2)}) collective-permute-start(bf16[768,1024]{1,0:T(8,128)(2,1)} %bitcast.10), channel_id=1, source_target_pairs={{0,1},{1,0},{2,3},{3,2},{4,5},{5,4},{6,7},{7,6},{8,9},{9,8},{10,11... | collective-permute-start | bytes 4718600 | tf_op jit(solution)/shard_map/ppermute | solution.py:291
  60.6 10.3 %copy-start.29 = (f32[128]{0:T(128)}, f32[128]{0:T(128)S(1)}, u32[]{:S(2)}) copy-start(f32[128]{0:T(128)S(1)} %fusion.131) | copy-start | bytes 1540
  65.3 1.2 copy-start.3
  66.9 11.4 %copy-start.14 = (bf16[768,128]{1,0:T(8,128)(2,1)}, bf16[768,128]{1,0:T(8,128)(2,1)S(1)}, u32[]{:S(2)}) copy-start(bf16[768,128]{1,0:T(8,128)(2,1)S(1)} %get-tuple-element.38) | copy-start | bytes 589828
  67.2 0.7 copy-start.16
  67.2 0.7 copy-start.18
  67.2 3.5 %copy-start.28 = (f32[2,128]{1,0:T(2,128)S(1)}, f32[2,128]{1,0:T(2,128)}, u32[]{:S(2)}) copy-start(f32[2,128]{1,0:T(2,128)} %reduce_window_sum.35) | copy-start | bytes 3076
  67.3 3.5 %copy-start.32 = (f32[128]{0:T(128)S(1)}, f32[128]{0:T(128)}, u32[]{:S(2)}) copy-start(f32[128]{0:T(128)} %get-tuple-element.72) | copy-start | bytes 1540
  67.3 3.6 %copy-start.5 = (f32[1,1,128,256]{3,2,1,0:T(8,128)S(1)}, f32[1,1,128,256]{3,2,1,0:T(8,128)}, u32[]{:S(2)}) copy-start(f32[1,1,128,256]{3,2,1,0:T(8,128)} %param.29) | copy-start | bytes 393220
  67.3 4.3 %copy-start.10 = (f32[128,128]{1,0:T(8,128)S(1)}, f32[128,128]{1,0:T(8,128)}, u32[]{:S(2)}) copy-start(f32[128,128]{1,0:T(8,128)} %get-tuple-element.76) | copy-start | bytes 196612
  68.4 10.4 %collective-permute-start.1 = (bf16[384,1024]{1,0:T(8,128)(2,1)S(1)}, bf16[384,1024]{1,0:T(8,128)(2,1)S(1)}, u32[]{:S(2)}, u32[]{:S(2)}) collective-permute-start(bf16[384,1024]{1,0:T(8,128)(2,1)S(1)} %convolution_convert_fusion.1), channel_id=1, source_target_pairs={{0,1},{1,0},{2,3},{3,2},{4,5},{5,4},{6,7},{7,6},{8,9},{9,8},{10,11... | collective-permute-start | bytes 2359304 | tf_op jit(solution)/shard_map/ppermute | solution.py:334
  75.3 81.4 %collective-permute-start.6 = (bf16[256,256]{1,0:T(8,128)(2,1)}, bf16[256,256]{1,0:T(8,128)(2,1)}, u32[]{:S(2)}, u32[]{:S(2)}) collective-permute-start(bf16[256,256]{1,0:T(8,128)(2,1)} %all_gather.7.refs_0_), channel_id=1, source_target_pairs={{0,320},{64,384},{128,448},{192,0},{256,64},{320,128},{384,192},{4... | collective-permute-start | bytes 393224 | tf_op jit(solution)/shard_map/ppermute | solution.py:345
  79.2 8.3 %copy-start.4 = (bf16[768,1024]{1,0:T(8,128)(2,1)S(1)}, bf16[768,1024]{1,0:T(8,128)(2,1)}, u32[]{:S(2)}) copy-start(bf16[768,1024]{1,0:T(8,128)(2,1)} %copy-done.3) | copy-start | bytes 4718596
  80.3 7.3 %copy-start.15 = (bf16[768,128]{1,0:T(8,128)(2,1)S(1)}, bf16[768,128]{1,0:T(8,128)(2,1)}, u32[]{:S(2)}) copy-start(bf16[768,128]{1,0:T(8,128)(2,1)} %copy-done.14) | copy-start | bytes 589828
  80.3 7.3 %copy-start.35 = (bf16[1,128]{1,0:T(2,128)(2,1)S(1)}, bf16[1,128]{1,0:T(2,128)(2,1)}, u32[]{:S(2)}) copy-start(bf16[1,128]{1,0:T(2,128)(2,1)} %slice.366) | copy-start | bytes 772
  80.3 30.3 %all-to-all-start.1 = ((bf16[8,384,128]{2,1,0:T(8,128)(2,1)}), bf16[8,384,128]{2,1,0:T(8,128)(2,1)S(1)}, u32[]{:S(2)}, u32[]{:S(2)}) async-start(bf16[8,384,128]{2,1,0:T(8,128)(2,1)} %bitcast.310), calls=%async_computation.1 | async-start | bytes 1572864 | tf_op jit(solution)/shard_map/all_to_all | solution.py:337
  87.6 0.9 copy-start.17
  87.6 1.0 copy-start.19
  92.4 38.4 %copy-start.33 = (s32[128]{0:T(128)S(1)}, s32[128]{0:T(128)}, u32[]{:S(2)}) copy-start(s32[128]{0:T(128)} %get-tuple-element.82) | copy-start | bytes 1540
  92.4 38.4 %copy-start.34 = (s32[128]{0:T(128)S(1)}, s32[128]{0:T(128)}, u32[]{:S(2)}) copy-start(s32[128]{0:T(128)} %get-tuple-element.83) | copy-start | bytes 1540
  111.4 19.3 %all-to-all-start.2 = ((bf16[32,12,128]{2,1,0:T(8,128)(2,1)}), bf16[32,12,128]{2,1,0:T(8,128)(2,1)S(1)}, u32[]{:S(2)}, u32[]{:S(2)}) async-start(bf16[32,12,128]{2,1,0:T(8,128)(2,1)} %reshape.572), calls=%async_computation.2 | async-start | bytes 262144 | tf_op jit(solution)/shard_map/all_to_all | solution.py:360
  120.9 35.8 %collective-permute-start.7 = (bf16[256,256]{1,0:T(8,128)(2,1)}, bf16[256,256]{1,0:T(8,128)(2,1)S(1)}, u32[]{:S(2)}, u32[]{:S(2)}) collective-permute-start(bf16[256,256]{1,0:T(8,128)(2,1)} %all_gather.7.refs_0_), channel_id=1, source_target_pairs={{0,384},{64,448},{128,0},{192,64},{256,128},{320,192},{384,256},{4... | collective-permute-start | bytes 393224 | tf_op jit(solution)/shard_map/ppermute | solution.py:345
  126.4 30.3 %collective-permute-start.5 = (bf16[256,256]{1,0:T(8,128)(2,1)}, bf16[256,256]{1,0:T(8,128)(2,1)S(1)}, u32[]{:S(2)}, u32[]{:S(2)}) collective-permute-start(bf16[256,256]{1,0:T(8,128)(2,1)} %all_gather.7.refs_0_), channel_id=1, source_target_pairs={{0,256},{64,320},{128,384},{192,448},{256,0},{320,64},{384,128},{4... | collective-permute-start | bytes 393224 | tf_op jit(solution)/shard_map/ppermute | solution.py:345
  131.0 25.8 %collective-permute-start.4 = (bf16[256,256]{1,0:T(8,128)(2,1)}, bf16[256,256]{1,0:T(8,128)(2,1)S(1)}, u32[]{:S(2)}, u32[]{:S(2)}) collective-permute-start(bf16[256,256]{1,0:T(8,128)(2,1)} %all_gather.7.refs_0_), channel_id=1, source_target_pairs={{0,192},{64,256},{128,320},{192,384},{256,448},{320,0},{384,64},{4... | collective-permute-start | bytes 393224 | tf_op jit(solution)/shard_map/ppermute | solution.py:345
  135.3 21.5 %collective-permute-start.3 = (bf16[256,256]{1,0:T(8,128)(2,1)}, bf16[256,256]{1,0:T(8,128)(2,1)S(1)}, u32[]{:S(2)}, u32[]{:S(2)}) collective-permute-start(bf16[256,256]{1,0:T(8,128)(2,1)} %all_gather.7.refs_0_), channel_id=1, source_target_pairs={{0,128},{64,192},{128,256},{192,320},{256,384},{320,448},{384,0},{... | collective-permute-start | bytes 393224 | tf_op jit(solution)/shard_map/ppermute | solution.py:345
  156.8 0.7 copy-start.20
  156.8 0.7 copy-start.21
  156.8 0.7 copy-start.22
  156.8 0.8 copy-start.23
  161.0 16.2 %all-to-all-start.4 = ((bf16[4,136,256]{2,1,0:T(8,128)(2,1)}), bf16[4,136,256]{2,1,0:T(8,128)(2,1)S(1)}, u32[]{:S(2)}, u32[]{:S(2)}) async-start(bf16[4,136,256]{2,1,0:T(8,128)(2,1)} %get-tuple-element.27), calls=%async_computation.4 | async-start | bytes 557056 | tf_op jit(solution)/shard_map/all_to_all | solution.py:404
  167.4 9.9 %collective-permute-start.9 = (bf16[8,64,256]{2,1,0:T(8,128)(2,1)S(1)}, bf16[8,64,256]{2,1,0:T(8,128)(2,1)S(1)}, u32[]{:S(2)}, u32[]{:S(2)}) collective-permute-start(bf16[8,64,256]{2,1,0:T(8,128)(2,1)S(1)} %get-tuple-element.48), channel_id=1, source_target_pairs={{0,16},{16,32},{32,48},{48,0},{1,17},{17,33},{33,49},{49,1},{2,18}... | collective-permute-start | bytes 786440 | tf_op jit(solution)/shard_map/ppermute | solution.py:421
  170.8 10.5 %collective-permute-start.11 = (bf16[8,64,256]{2,1,0:T(8,128)(2,1)S(1)}, bf16[8,64,256]{2,1,0:T(8,128)(2,1)S(1)}, u32[]{:S(2)}, u32[]{:S(2)}) collective-permute-start(bf16[8,64,256]{2,1,0:T(8,128)(2,1)S(1)} %get-tuple-element.49), channel_id=1, source_target_pairs={{0,48},{16,0},{32,16},{48,32},{1,49},{17,1},{33,17},{49,33},{2,50}... | collective-permute-start | bytes 786440 | tf_op jit(solution)/shard_map/ppermute | solution.py:421
  173.3 13.5 %collective-permute-start.10 = (bf16[8,64,256]{2,1,0:T(8,128)(2,1)S(1)}, bf16[8,64,256]{2,1,0:T(8,128)(2,1)}, u32[]{:S(2)}, u32[]{:S(2)}) collective-permute-start(bf16[8,64,256]{2,1,0:T(8,128)(2,1)S(1)} %get-tuple-element.50), channel_id=1, source_target_pairs={{0,32},{16,48},{32,0},{48,16},{1,33},{17,49},{33,1},{49,17},{2,34}... | collective-permute-start | bytes 786440 | tf_op jit(solution)/shard_map/ppermute | solution.py:421
  188.5 20.6 %copy-start.6 = (bf16[128,256]{1,0:T(8,128)(2,1)S(1)}, bf16[128,256]{1,0:T(8,128)(2,1)}, u32[]{:S(2)}) copy-start(bf16[128,256]{1,0:T(8,128)(2,1)} %get-tuple-element.26) | copy-start | bytes 196612
  188.5 20.9 %copy-start.11 = (f32[128,128]{1,0:T(8,128)S(1)}, f32[128,128]{1,0:T(8,128)}, u32[]{:S(2)}) copy-start(f32[128,128]{1,0:T(8,128)} %get-tuple-element.76) | copy-start | bytes 196612
  188.5 16.1 %all-to-all-start.3 = ((bf16[8,64,256]{2,1,0:T(8,128)(2,1)}), bf16[8,64,256]{2,1,0:T(8,128)(2,1)S(1)}, u32[]{:S(2)}, u32[]{:S(2)}) async-start(bf16[8,64,256]{2,1,0:T(8,128)(2,1)} %fusion.40), calls=%async_computation.3 | async-start | bytes 524288 | tf_op jit(solution)/shard_map/all_to_all | solution.py:426
  205.5 6.1 %copy-start.12 = (f32[2,64,128]{2,1,0:T(8,128)S(1)}, f32[2,64,128]{2,1,0:T(8,128)}, u32[]{:S(2)}) copy-start(f32[2,64,128]{2,1,0:T(8,128)} %get-tuple-element.75) | copy-start | bytes 196612
  205.5 19.3 %all-to-all-start.5 = ((bf16[8,136,256]{2,1,0:T(8,128)(2,1)}), bf16[8,136,256]{2,1,0:T(8,128)(2,1)S(1)}, u32[]{:S(2)}, u32[]{:S(2)}) async-start(bf16[8,136,256]{2,1,0:T(8,128)(2,1)} %broadcast_in_dim.109), calls=%async_computation.5 | async-start | bytes 1114112 | tf_op jit(solution)/shard_map/all_to_all | solution.py:45
  216.6 9.0 %copy-start.13 = (bf16[1,128,256]{2,1,0:T(8,128)(2,1)S(1)}, bf16[1,128,256]{2,1,0:T(8,128)(2,1)}, u32[]{:S(2)}) copy-start(bf16[1,128,256]{2,1,0:T(8,128)(2,1)} %multiply_add_fusion.3) | copy-start | bytes 196612
  216.6 9.0 %copy-start.25 = (bf16[128,128]{1,0:T(8,128)(2,1)S(1)}, bf16[128,128]{1,0:T(8,128)(2,1)}, u32[]{:S(2)}) copy-start(bf16[128,128]{1,0:T(8,128)(2,1)} %param.25) | copy-start | bytes 98308
  224.8 2.6 %copy-start.30 = (f32[128]{0:T(128)S(1)}, f32[128]{0:T(128)}, u32[]{:S(2)}) copy-start(f32[128]{0:T(128)} %copy-done.29) | copy-start | bytes 1540
  224.8 2.6 %copy-start.31 = (f32[128]{0:T(128)S(1)}, f32[128]{0:T(128)}, u32[]{:S(2)}) copy-start(f32[128]{0:T(128)} %get-tuple-element.67) | copy-start | bytes 1540

commit v7 on v6

--- a/solution.py
+++ b/solution.py
@@ -8,7 +8,6 @@
 
 
 KEY_CHANNELS = 128
-DV = 256
 CAPACITY = 12
 BLOCK = 64
 SP = ("z", "x")
@@ -43,16 +42,6 @@
     count = lax.axis_size(axis)
     copies = jnp.broadcast_to(array[None], (count, *array.shape))
     return lax.all_to_all(copies, axis, 0, 0, tiled=True)
-
-
-def with_decay(state, decay):
-    row = jnp.pad(decay[None, :], ((0, 7), (0, DV - KEY_CHANNELS)))
-    return jnp.concatenate([state, row], axis=0).astype(jnp.bfloat16)
-
-
-def split_decay(filled):
-    decays = filled[:, KEY_CHANNELS, :KEY_CHANNELS].astype(jnp.float32)
-    return filled[:, :KEY_CHANNELS], decays
 
 
 def into_blocks(values):
@@ -197,7 +186,7 @@
 
 
 def resid_mixed_kernel(
-    place_ref, normed_ref, cot_ref, resid_ref, gain_ref, query_ref, decay_ref, *refs
+    place_ref, normed_ref, cot_ref, resid_ref, gain_ref, query_ref, *refs
 ):
     blocks, (out_ref, mixed_ref, near_ref) = refs[:8], refs[8:]
     tokens = resid_ref.shape[0]
@@ -220,13 +209,11 @@
     mixed = total.astype(jnp.bfloat16)
     mixed_ref[...] = mixed
     state = jnp.dot(query_ref[...], mixed, preferred_element_type=jnp.float32)
-    keys = state.shape[0]
     for k in range(near_ref.shape[0]):
-        near_ref[k, :keys, :] = state.astype(jnp.bfloat16)
-        near_ref[k, keys:, :] = decay_ref[...].astype(jnp.bfloat16)
-
-
-def resid_mixed(place, grad_normed, cotangent, resid, gain, blocks, query_cols, decay_row, copies):
+        near_ref[k] = state.astype(jnp.bfloat16)
+
+
+def resid_mixed(place, grad_normed, cotangent, resid, gain, blocks, query_cols, copies):
     vmem = pl.BlockSpec(memory_space=pltpu.VMEM)
     return pl.pallas_call(
         resid_mixed_kernel,
@@ -234,10 +221,10 @@
             jax.ShapeDtypeStruct(resid.shape, jnp.bfloat16),
             jax.ShapeDtypeStruct((resid.shape[0], blocks[0].shape[1]), jnp.bfloat16),
             jax.ShapeDtypeStruct(
-                (copies, query_cols.shape[0] + decay_row.shape[0], blocks[0].shape[1]), jnp.bfloat16
+                (copies, query_cols.shape[0], blocks[0].shape[1]), jnp.bfloat16
             ),
         ),
-        in_specs=[pl.BlockSpec(memory_space=pltpu.SMEM)] + [vmem] * 14,
+        in_specs=[pl.BlockSpec(memory_space=pltpu.SMEM)] + [vmem] * 13,
         out_specs=(vmem, vmem, vmem),
         name="resid_mixed",
     )(
@@ -247,7 +234,6 @@
         resid,
         gain.reshape(1, -1),
         query_cols,
-        decay_row,
         *blocks,
     )
 
@@ -337,11 +323,10 @@
     swapped = lax.all_to_all(parts, "y", 0, 0, tiled=True)
     summed = sum_parts(swapped).astype(jnp.bfloat16)
     proj_tied, _ = lax.optimization_barrier((proj_near, parts))
-    proj_early, _ = lax.optimization_barrier((proj_near, own))
     z_place = lax.axis_index("z")
     blocks = [proj_near] + [None] * 7
     for k in range(1, 8):
-        sent_block = proj_near if k in (1, 7) else proj_early if k == 5 else proj_tied
+        sent_block = proj_near if k in (1, 7) else proj_tied
         blocks[k] = lax.ppermute(sent_block, "z", [(i, (i + k) % 8) for i in range(8)])
 
     def beside(values):
@@ -357,10 +342,27 @@
     grad_out_w = named_dot(beside(hidden), rows_cot)
     grad_down_w = jnp.concatenate([grad_out_w[:width], grad_out_w[width:]], axis=1)
 
-    returned = lax.all_to_all(
-        summed.reshape(experts, capacity, -1), SP, split_axis=0, concat_axis=0, tiled=True
-    )
-    flat_rows = returned.reshape(slots, -1)
+    query_scale = KEY_CHANNELS ** (-0.5)
+    query_rows = query.astype(jnp.float32) * query_scale
+    span_log = jnp.cumsum(into_blocks(log_decay), axis=1)
+    span_log = jnp.concatenate([span_log[0], span_log[1] + span_log[0, -1:]], axis=0)
+    query_cols = jnp.transpose(query_rows * jnp.exp(span_log)).astype(jnp.bfloat16)
+    own_decay = jnp.exp(span_log[-1:]).astype(jnp.bfloat16)
+    chunks = jnp.concatenate(
+        [
+            summed.reshape(experts, capacity, -1),
+            jnp.broadcast_to(own_decay[None], (experts, 4, KEY_CHANNELS)),
+        ],
+        axis=1,
+    )
+    returned = lax.all_to_all(chunks, SP, split_axis=0, concat_axis=0, tiled=True)
+    flat_rows = returned[:, :capacity].reshape(slots, -1)
+    decays = returned[:, capacity].astype(jnp.float32)
+    decays = decays.reshape(lax.axis_size("z"), lax.axis_size("x"), KEY_CHANNELS)
+    near_decays = lax.dynamic_index_in_dim(
+        decays, lax.axis_index("z").astype(jnp.uint32), 0, keepdims=False
+    )
+    far_decays = jnp.prod(decays, axis=1)
     slot_index = lax.broadcasted_iota(jnp.int32, (slots, tokens_here), 0)
     slot_tokens = ((slot_index == slot_a[None, :]) | (slot_index == slot_b[None, :])).astype(
         jnp.bfloat16
@@ -372,14 +374,6 @@
         ("y", "c"),
         axis=1,
         tiled=True,
-    )
-    query_scale = KEY_CHANNELS ** (-0.5)
-    query_rows = query.astype(jnp.float32) * query_scale
-    span_log = jnp.cumsum(into_blocks(log_decay), axis=1)
-    span_log = jnp.concatenate([span_log[0], span_log[1] + span_log[0, -1:]], axis=0)
-    query_cols = jnp.transpose(query_rows * jnp.exp(span_log)).astype(jnp.bfloat16)
-    decay_row = jnp.pad(
-        jnp.exp(span_log[-1:]), ((0, 7), (0, out_proj.shape[1] - KEY_CHANNELS))
     )
     grad_resid, grad_mixed, near_sent = resid_mixed(
         z_place,
@@ -389,7 +383,6 @@
         norm_gain,
         blocks,
         query_cols,
-        decay_row,
         lax.axis_size("x"),
     )
     share = lax.dot_general(
@@ -402,11 +395,9 @@
         query_rows, key_rows, value_rows, grad_rows, log_decay, span_state[0, 0]
     )
     near_filled = lax.all_to_all(near_sent, "x", 0, 0, tiled=True)
-    near_states, near_decays = split_decay(near_filled)
-    near_sum, near_factor = later_sum(near_states, near_decays, lax.axis_index("x"))
-    group_sum, group_factor = later_sum(near_states, near_decays, -1)
-    far_filled = to_all(with_decay(group_sum, group_factor), "z")
-    far_states, far_decays = split_decay(far_filled)
+    near_sum, near_factor = later_sum(near_filled, near_decays, lax.axis_index("x"))
+    group_sum, _ = later_sum(near_filled, near_decays, -1)
+    far_filled = to_all(group_sum.astype(jnp.bfloat16), "z")
     z_count, x_count = lax.axis_size("z"), lax.axis_size("x")
     share_rows = model_width // sp_count
     share_x = share.reshape(z_count, x_count, share_rows, -1).transpose(1, 0, 2, 3)
@@ -425,7 +416,7 @@
     share_z = share_sum.astype(jnp.bfloat16)
     share_z = lax.all_to_all(share_z, "z", 0, 0, tiled=True)
     grad_out_proj = sum_parts(share_z)
-    far_sum, _ = later_sum(far_states, far_decays, lax.axis_index("z"))
+    far_sum, _ = later_sum(far_filled, far_decays, lax.axis_index("z"))
     exit_cot = near_sum + near_factor[:, None] * far_sum
     grad_query, grad_key, grad_value, grad_log_decay = span_backward(
         query_rows, key_rows, value_rows, grad_rows, kept_terms, exit_cot

time: 230 us -> 243 us (1.057)
  the two profiles are of different devices: /device:TPU:2 before, /device:TPU:8 now
where the time goes in v7:
time: 243 us; the launch traced here: 242 us
  starting transfers between devices  86.8 us (36%)
  waiting for transfers between devices  61.7 us (25%)
  blocking collectives  33.7 us (14%)
  other arithmetic  25.4 us (10%)
  local copies, waits for them, and re-layouts  12.9 us (5%)
  matrix products  12.2 us (5%)
  Pallas kernels  7.29 us (3%)
    ppermute x7, starting transfers between devices, on_device_body(): lax.ppermute(sent_block, 'z', [(i, (i + k) % 8) for i in range(8)])  30.5 us
    all_gather x1, blocking collectives, on_device_body(): lax.all_gather(lax.dot_general(slot_tokens, flat_rows, (((0,), (0,)), (()...  18.6 us
    all_to_all x1, waiting for transfers between devices, on_device_body(): swapped = lax.all_to_all(parts, 'y', 0, 0, tiled=True)  17.5 us
    all_gather x1, blocking collectives, on_device_body(): proj_near = lax.all_gather(proj_near, 'x', axis=0, tiled=True)  15.1 us
    all_to_all x1, waiting for transfers between devices, on_device_body(): own = lax.all_to_all(sent, SP, 0, 0, tiled=True).reshape(2 * slots, half)  14.5 us
    all_to_all x1, starting transfers between devices, on_device_body(): own = lax.all_to_all(sent, SP, 0, 0, tiled=True).reshape(2 * slots, half)  13.3 us
    ppermute x3, starting transfers between devices, on_device_body(): lax.ppermute(for_place(k), 'x', [(i, (i + k) % 4) for i in range(4)])  11 us
    all_to_all x1, waiting for transfers between devices, on_device_body(): share_z = lax.all_to_all(share_z, 'z', 0, 0, tiled=True)  10.2 us
  transfers between devices with their start and end apart: 18, of which 7 were waited for; matrix products, arithmetic and copies ran while one was open for 18% of the time, Pallas kernels for 0%

profile of v7, /device:TPU:8, one launch (start us, length us, event | category | flops | bytes accessed | tf_op | source)
XLA Modules:
  0.0 241.8 jit_solution(4278040080699694098)
XLA Ops:
  0.7 3.9 %dispatch_rows.1 = (bf16[768,1024]{1,0:T(8,128)(2,1)}, s32[8,128]{1,0:T(8,128)}) custom-call(s32[1]{0:T(128)} %bitcast.5.core_ref, s32[2,128]{1,0:T(2,128)} %bitcast.346, f32[2,128]{1,0:T(2,128)} %bitcast.347, bf16[128,2048]{1,0:T(8,128)(2,1)} %resid_ref.3, bf16[128,2048]{1,0:T(8,128)(2,1)} %cot_ref.3, f32[1,2048]{1,0:T(1,128)} %bitcast.338), custom_call_target="tpu_custom_call" | custom-call | tf_op jit(solution)/shard_map/dispatch_rows/pallas_call | solution.py:175
  4.5 13.3 %all-to-all-start = ((bf16[32,24,1024]{2,1,0:T(8,128)(2,1)}), bf16[32,24,1024]{2,1,0:T(8,128)(2,1)S(1)}, u32[]{:S(2)}, u32[]{:S(2)}) async-start(bf16[32,24,1024]{2,1,0:T(8,128)(2,1)} %bitcast.310), calls=%async_computation | async-start | bytes 3145728 | tf_op jit(solution)/shard_map/all_to_all | solution.py:274
  17.9 15.1 %all_gather.7.refs_0_ = bf16[256,256]{1,0:T(8,128)(2,1)} all-gather(bf16[64,256]{1,0:T(8,128)(2,1)S(1)} %copy-done.24), channel_id=1, replica_groups=mesh['z'=8,'x'=4,'y'=8,'c'=2] {'x'}, dimensions={0}, use_global_device_ids=true | all-gather | bytes 163840 | tf_op jit(solution)/shard_map/all_gather | solution.py:276
  32.9 5.4 %collective-permute-start.8 = (bf16[256,256]{1,0:T(8,128)(2,1)}, bf16[256,256]{1,0:T(8,128)(2,1)}, u32[]{:S(2)}, u32[]{:S(2)}) collective-permute-start(bf16[256,256]{1,0:T(8,128)(2,1)} %all_gather.7.refs_0_), channel_id=1, source_target_pairs={{0,448},{64,0},{128,64},{192,128},{256,192},{320,256},{384,320},{4... | collective-permute-start | bytes 393224 | tf_op jit(solution)/shard_map/ppermute | solution.py:330
  38.4 1.9 collective-permute-start.2
  40.8 0.6 fusion.122
  41.5 0.7 convert_multiply_fusion.15
  42.2 0.8 fusion.136
  43.0 0.7 fusion.134
  43.8 14.5 %all-to-all-done = bf16[32,24,1024]{2,1,0:T(8,128)(2,1)S(1)} async-done(((bf16[32,24,1024]{2,1,0:T(8,128)(2,1)}), bf16[32,24,1024]{2,1,0:T(8,128)(2,1)S(1)}, u32[]{:S(2)}, u32[]{:S(2)}) %all-to-all-start) | async-done | bytes 1572896 | tf_op jit(solution)/shard_map/all_to_all | solution.py:274
  58.4 1.9 collective-permute-start
  60.3 0.6 slice_reduce_fusion
  60.9 1.6 copy.79
  62.5 1.8 copy.99
  64.3 0.8 copy.100
  65.4 1.7 broadcast_select_fusion
  67.5 1.3 slice_bitcast_fusion.4
  68.8 1.0 fusion.138
  69.8 2.4 %broadcast_select_fusion.2 = (f32[768,512]{1,0:T(8,128)S(1)}, f32[768,512]{1,0:T(8,128)S(1)}) fusion(f32[768,512]{1,0:T(8,128)S(1)} %fusion.138, pred[]{:T(512)S(6)} %eq.48, bf16[768,1024]{1,0:T(8,128)(2,1)} %collective-permute-done, bf16[1024,512]{0,1:T(8,128)(2,1)S(1)} %get-tuple-element.18), kind=kOutput, calls=%fused_computation.53 | convolution fusion | flops 805699584 | bytes 7340033 | tf_op jit(solution)/shard_map/dot_general | solution.py:290
  73.9 2.4 collective-permute-start.1
  76.3 0.6 subtract_exponential_fusion.1
  77.2 3.8 %fusion = (bf16[2,64,64]{2,1,0:T(8,128)(2,1)S(1)}, f32[2,64,128,64]{2,3,1,0:T(8,128)}) fusion(f32[2,128,64]{1,2,0:T(8,128)S(1)} %get-tuple-element.74, f32[2,128,64]{1,2,0:T(8,128)S(1)} %bitcast.320, f32[2,64,128]{2,1,0:T(8,128)S(1)} %reduce_window_sum.34, pred[64,64]{1,0:T(8,128)(4,1)S(1)} %iota_compare_fusion.8), kind=kLoop, calls=%fused_computation.1 | loop fusion | flops 5234688 | bytes 4411392 | tf_op jit(solution)/shard_map/ntd,nsd,ntsd->nts/dot_general | solution.py:86
  81.4 1.0 copy.108
  82.5 7.6 %all-to-all-start.1 = ((bf16[8,384,128]{2,1,0:T(8,128)(2,1)}), bf16[8,384,128]{2,1,0:T(8,128)(2,1)S(1)}, u32[]{:S(2)}, u32[]{:S(2)}) async-start(bf16[8,384,128]{2,1,0:T(8,128)(2,1)} %bitcast.295), calls=%async_computation.1 | async-start | bytes 1572864 | tf_op jit(solution)/shard_map/all_to_all | solution.py:323
  90.2 0.7 slice.338
  91.0 2.1 fusion.14
  93.1 1.1 fusion.11
  94.4 17.5 %all-to-all-done.1 = bf16[8,384,128]{2,1,0:T(8,128)(2,1)S(1)} async-done(((bf16[8,384,128]{2,1,0:T(8,128)(2,1)}), bf16[8,384,128]{2,1,0:T(8,128)(2,1)S(1)}, u32[]{:S(2)}, u32[]{:S(2)}) %all-to-all-start.1) | async-done | bytes 786464 | tf_op jit(solution)/shard_map/all_to_all | solution.py:323
  112.0 0.7 pad_maximum_fusion.2
  112.7 5.2 %all-to-all-start.2 = ((bf16[32,16,128]{2,1,0:T(8,128)(2,1)}), bf16[32,16,128]{2,1,0:T(8,128)(2,1)S(1)}, u32[]{:S(2)}, u32[]{:S(2)}) async-start(bf16[32,16,128]{2,1,0:T(8,128)(2,1)} %pad_maximum_fusion.2), calls=%async_computation.2 | async-start | bytes 262144 | tf_op jit(solution)/shard_map/all_to_all | solution.py:358
  117.9 0.8 maximum_bitcast_fusion.2
  118.7 1.0 maximum_bitcast_fusion
  119.8 5.8 %collective-permute-start.7 = (bf16[256,256]{1,0:T(8,128)(2,1)}, bf16[256,256]{1,0:T(8,128)(2,1)S(1)}, u32[]{:S(2)}, u32[]{:S(2)}) collective-permute-start(bf16[256,256]{1,0:T(8,128)(2,1)} %all_gather.7.refs_0_), channel_id=1, source_target_pairs={{0,384},{64,448},{128,0},{192,64},{256,128},{320,192},{384,256},{4... | collective-permute-start | bytes 393224 | tf_op jit(solution)/shard_map/ppermute | solution.py:330
  125.6 4.2 %collective-permute-start.6 = (bf16[256,256]{1,0:T(8,128)(2,1)}, bf16[256,256]{1,0:T(8,128)(2,1)S(1)}, u32[]{:S(2)}, u32[]{:S(2)}) collective-permute-start(bf16[256,256]{1,0:T(8,128)(2,1)} %all_gather.7.refs_0_), channel_id=1, source_target_pairs={{0,320},{64,384},{128,448},{192,0},{256,64},{320,128},{384,192},{4... | collective-permute-start | bytes 393224 | tf_op jit(solution)/shard_map/ppermute | solution.py:330
  129.9 4.6 %collective-permute-start.5 = (bf16[256,256]{1,0:T(8,128)(2,1)}, bf16[256,256]{1,0:T(8,128)(2,1)S(1)}, u32[]{:S(2)}, u32[]{:S(2)}) collective-permute-start(bf16[256,256]{1,0:T(8,128)(2,1)} %all_gather.7.refs_0_), channel_id=1, source_target_pairs={{0,256},{64,320},{128,384},{192,448},{256,0},{320,64},{384,128},{4... | collective-permute-start | bytes 393224 | tf_op jit(solution)/shard_map/ppermute | solution.py:330
  134.8 18.6 %all_gather.6.normed_ref = bf16[128,2048]{1,0:T(8,128)(2,1)} all-gather(bf16[128,128]{1,0:T(8,128)(2,1)S(1)} %convolution_convert_fusion.2), channel_id=1, replica_groups=mesh['z'=8,'x'=4,'y'=8,'c'=2] {'y','c'}, dimensions={1}, use_global_device_ids=true | all-gather | bytes 557056 | tf_op jit(solution)/shard_map/all_gather | solution.py:370
  153.4 3.0 %collective-permute-start.4 = (bf16[256,256]{1,0:T(8,128)(2,1)}, bf16[256,256]{1,0:T(8,128)(2,1)S(1)}, u32[]{:S(2)}, u32[]{:S(2)}) collective-permute-start(bf16[256,256]{1,0:T(8,128)(2,1)} %all_gather.7.refs_0_), channel_id=1, source_target_pairs={{0,192},{64,256},{128,320},{192,384},{256,448},{320,0},{384,64},{4... | collective-permute-start | bytes 393224 | tf_op jit(solution)/shard_map/ppermute | solution.py:330
  156.4 5.5 %collective-permute-start.3 = (bf16[256,256]{1,0:T(8,128)(2,1)}, bf16[256,256]{1,0:T(8,128)(2,1)S(1)}, u32[]{:S(2)}, u32[]{:S(2)}) collective-permute-start(bf16[256,256]{1,0:T(8,128)(2,1)} %all_gather.7.refs_0_), channel_id=1, source_target_pairs={{0,128},{64,192},{128,256},{192,320},{256,384},{320,448},{384,0},{... | collective-permute-start | bytes 393224 | tf_op jit(solution)/shard_map/ppermute | solution.py:330
  162.1 8.8 %collective-permute-done.4.refs_3_ = bf16[256,256]{1,0:T(8,128)(2,1)S(1)} collective-permute-done((bf16[256,256]{1,0:T(8,128)(2,1)}, bf16[256,256]{1,0:T(8,128)(2,1)S(1)}, u32[]{:S(2)}, u32[]{:S(2)}) %collective-permute-start.4) | collective-permute-done | bytes 131104 | tf_op jit(solution)/shard_map/ppermute | solution.py:330
  170.9 0.6 copy-done.21
  171.5 3.4 %resid_mixed.1 = (bf16[128,2048]{1,0:T(8,128)(2,1)}, bf16[128,256]{1,0:T(8,128)(2,1)}, bf16[4,128,256]{2,1,0:T(8,128)(2,1)}) custom-call(s32[1]{0:T(128)} %bitcast.21.place_ref, bf16[128,2048]{1,0:T(8,128)(2,1)} %all_gather.6.normed_ref, bf16[128,2048]{1,0:T(8,128)(2,1)} %cot_ref.3, bf16[128,2048]{1,0:T(8,128)(2,1)} %resid_ref.3, f32[1,2048]{1,0:T(1,128)} %bitcast.339, ...), custom_call_target="tpu_custom_call" | custom-call | tf_op jit(solution)/shard_map/resid_mixed/pallas_call | solution.py:218
  175.0 1.5 convolution_convert_fusion
  176.6 3.7 %collective-permute-start.9 = (bf16[8,64,256]{2,1,0:T(8,128)(2,1)S(1)}, bf16[8,64,256]{2,1,0:T(8,128)(2,1)S(1)}, u32[]{:S(2)}, u32[]{:S(2)}) collective-permute-start(bf16[8,64,256]{2,1,0:T(8,128)(2,1)S(1)} %get-tuple-element.46), channel_id=1, source_target_pairs={{0,16},{16,32},{32,48},{48,0},{1,17},{17,33},{33,49},{49,1},{2,18}... | collective-permute-start | bytes 786440 | tf_op jit(solution)/shard_map/ppermute | solution.py:412
  180.3 3.5 %collective-permute-start.11 = (bf16[8,64,256]{2,1,0:T(8,128)(2,1)S(1)}, bf16[8,64,256]{2,1,0:T(8,128)(2,1)S(1)}, u32[]{:S(2)}, u32[]{:S(2)}) collective-permute-start(bf16[8,64,256]{2,1,0:T(8,128)(2,1)S(1)} %get-tuple-element.47), channel_id=1, source_target_pairs={{0,48},{16,0},{32,16},{48,32},{1,49},{17,1},{33,17},{49,33},{2,50}... | collective-permute-start | bytes 786440 | tf_op jit(solution)/shard_map/ppermute | solution.py:412
  183.8 3.8 %collective-permute-start.10 = (bf16[8,64,256]{2,1,0:T(8,128)(2,1)S(1)}, bf16[8,64,256]{2,1,0:T(8,128)(2,1)}, u32[]{:S(2)}, u32[]{:S(2)}) collective-permute-start(bf16[8,64,256]{2,1,0:T(8,128)(2,1)S(1)} %get-tuple-element.48), channel_id=1, source_target_pairs={{0,32},{16,48},{32,0},{48,16},{1,33},{17,49},{33,1},{49,17},{2,34}... | collective-permute-start | bytes 786440 | tf_op jit(solution)/shard_map/ppermute | solution.py:412
  187.7 0.6 broadcast_select_fusion.22
  188.3 0.6 bitcast_multiply_fusion.3
  189.4 0.6 broadcast_select_fusion.11
  189.9 0.6 broadcast_select_fusion.7
  190.5 0.5 slice_bitcast_fusion.2
  191.1 3.4 %all-to-all-start.4 = ((bf16[4,128,256]{2,1,0:T(8,128)(2,1)}), bf16[4,128,256]{2,1,0:T(8,128)(2,1)S(1)}, u32[]{:S(2)}, u32[]{:S(2)}) async-start(bf16[4,128,256]{2,1,0:T(8,128)(2,1)} %get-tuple-element.25), calls=%async_computation.4 | async-start | bytes 524288 | tf_op jit(solution)/shard_map/all_to_all | solution.py:397
  194.8 1.8 fusion.40
  196.6 4.5 %all-to-all-done.4 = bf16[4,128,256]{2,1,0:T(8,128)(2,1)S(1)} async-done(((bf16[4,128,256]{2,1,0:T(8,128)(2,1)}), bf16[4,128,256]{2,1,0:T(8,128)(2,1)S(1)}, u32[]{:S(2)}, u32[]{:S(2)}) %all-to-all-start.4) | async-done | bytes 262176 | tf_op jit(solution)/shard_map/all_to_all | solution.py:397
  201.1 8.1 %all-to-all-start.3 = ((bf16[8,64,256]{2,1,0:T(8,128)(2,1)}), bf16[8,64,256]{2,1,0:T(8,128)(2,1)S(1)}, u32[]{:S(2)}, u32[]{:S(2)}) async-start(bf16[8,64,256]{2,1,0:T(8,128)(2,1)} %fusion.40), calls=%async_computation.3 | async-start | bytes 524288 | tf_op jit(solution)/shard_map/all_to_all | solution.py:417
  209.5 10.2 %all-to-all-done.3 = bf16[8,64,256]{2,1,0:T(8,128)(2,1)S(1)} async-done(((bf16[8,64,256]{2,1,0:T(8,128)(2,1)}), bf16[8,64,256]{2,1,0:T(8,128)(2,1)S(1)}, u32[]{:S(2)}, u32[]{:S(2)}) %all-to-all-start.3) | async-done | bytes 262176 | tf_op jit(solution)/shard_map/all_to_all | solution.py:417
  219.7 0.8 broadcast_in_dim.121
  220.5 3.5 %all-to-all-start.5 = ((bf16[8,128,256]{2,1,0:T(8,128)(2,1)}), bf16[8,128,256]{2,1,0:T(8,128)(2,1)S(1)}, u32[]{:S(2)}, u32[]{:S(2)}) async-start(bf16[8,128,256]{2,1,0:T(8,128)(2,1)} %broadcast_in_dim.121), calls=%async_computation.5 | async-start | bytes 1048576 | tf_op jit(solution)/shard_map/all_to_all | solution.py:44
  224.4 2.0 multiply_reduce_fusion
  226.4 4.9 %fusion.1 = f32[2,64,128]{2,1,0:T(8,128)S(1)} fusion(f32[2,64,128,64]{2,3,1,0:T(8,128)} %get-tuple-element.64, f32[2,64,128]{2,1,0:T(8,128)S(1)} %get-tuple-element.75, f32[2,64,64]{2,1,0:T(8,128)S(1)} %copy.78), kind=kLoop, calls=%fused_computation.3 | loop fusion | flops 3129344 | bytes 4358144 | tf_op jit(solution)/shard_map/nts,nsd,ntsd->ntd/dot_general | solution.py:89
  231.4 0.7 convert_reduce_fusion
  232.0 6.0 %all-to-all-done.5 = bf16[8,128,256]{2,1,0:T(8,128)(2,1)S(1)} async-done(((bf16[8,128,256]{2,1,0:T(8,128)(2,1)}), bf16[8,128,256]{2,1,0:T(8,128)(2,1)S(1)}, u32[]{:S(2)}, u32[]{:S(2)}) %all-to-all-start.5) | async-done | bytes 524320 | tf_op jit(solution)/shard_map/all_to_all | solution.py:44
  238.9 0.8 multiply_subtract_fusion
  239.9 0.8 fusion.19
  241.1 0.6 broadcast_add_fusion
  (155 shorter events, 7.1 us)
Async XLA Ops:
  0.6 174.3 %copy-start = (bf16[128,256]{1,0:T(8,128)(2,1)S(1)}, bf16[128,256]{1,0:T(8,128)(2,1)}, u32[]{:S(2)}) copy-start(bf16[128,256]{1,0:T(8,128)(2,1)} %param.24) | copy-start | bytes 196612
  4.5 13.3 %copy-start.24 = (bf16[64,256]{1,0:T(8,128)(2,1)S(1)}, bf16[64,256]{1,0:T(8,128)(2,1)}, u32[]{:S(2)}) copy-start(bf16[64,256]{1,0:T(8,128)(2,1)} %param.23) | copy-start | bytes 98308
  4.5 35.8 %copy-start.25 = (bf16[128,128]{1,0:T(8,128)(2,1)S(1)}, bf16[128,128]{1,0:T(8,128)(2,1)}, u32[]{:S(2)}) copy-start(bf16[128,128]{1,0:T(8,128)(2,1)} %param.25) | copy-start | bytes 98308
  4.5 35.9 %copy-start.23 = (f32[128,128]{1,0:T(8,128)S(1)}, f32[128,128]{1,0:T(8,128)}, u32[]{:S(2)}) copy-start(f32[128,128]{1,0:T(8,128)} %param.28) | copy-start | bytes 196612
  4.5 37.7 %copy-start.12 = (bf16[1,128,2048]{2,1,0:T(8,128)(2,1)S(1)}, bf16[1,128,2048]{2,1,0:T(8,128)(2,1)}, u32[]{:S(2)}) copy-start(bf16[1,128,2048]{2,1,0:T(8,128)(2,1)} %param.22) | copy-start | bytes 1572868
  4.5 53.8 %all-to-all-start = ((bf16[32,24,1024]{2,1,0:T(8,128)(2,1)}), bf16[32,24,1024]{2,1,0:T(8,128)(2,1)S(1)}, u32[]{:S(2)}, u32[]{:S(2)}) async-start(bf16[32,24,1024]{2,1,0:T(8,128)(2,1)} %bitcast.310), calls=%async_computation | async-start | bytes 3145728 | tf_op jit(solution)/shard_map/all_to_all | solution.py:274
  17.8 25.2 %copy-start.2 = (bf16[1,2048,128]{2,1,0:T(8,128)(2,1)S(1)}, bf16[1,2048,128]{2,1,0:T(8,128)(2,1)}, u32[]{:S(2)}) copy-start(bf16[1,2048,128]{2,1,0:T(8,128)(2,1)} %param.20) | copy-start | bytes 1572868
  17.9 25.9 %copy-start.1 = (bf16[1,2048,128]{2,1,0:T(8,128)(2,1)S(1)}, bf16[1,2048,128]{2,1,0:T(8,128)(2,1)}, u32[]{:S(2)}) copy-start(bf16[1,2048,128]{2,1,0:T(8,128)(2,1)} %param.21) | copy-start | bytes 1572868
  32.9 120.5 %collective-permute-start.8 = (bf16[256,256]{1,0:T(8,128)(2,1)}, bf16[256,256]{1,0:T(8,128)(2,1)}, u32[]{:S(2)}, u32[]{:S(2)}) collective-permute-start(bf16[256,256]{1,0:T(8,128)(2,1)} %all_gather.7.refs_0_), channel_id=1, source_target_pairs={{0,448},{64,0},{128,64},{192,128},{256,192},{320,256},{384,320},{4... | collective-permute-start | bytes 393224 | tf_op jit(solution)/shard_map/ppermute | solution.py:330
  38.4 118.0 %collective-permute-start.2 = (bf16[256,256]{1,0:T(8,128)(2,1)}, bf16[256,256]{1,0:T(8,128)(2,1)}, u32[]{:S(2)}, u32[]{:S(2)}) collective-permute-start(bf16[256,256]{1,0:T(8,128)(2,1)} %all_gather.7.refs_0_), channel_id=1, source_target_pairs={{0,64},{64,128},{128,192},{192,256},{256,320},{320,384},{384,448},... | collective-permute-start | bytes 393224 | tf_op jit(solution)/shard_map/ppermute | solution.py:330
  40.8 2.3 copy-start.6
  41.5 1.6 copy-start.8
  58.4 11.5 %collective-permute-start = (bf16[768,1024]{1,0:T(8,128)(2,1)S(1)}, bf16[768,1024]{1,0:T(8,128)(2,1)}, u32[]{:S(2)}, u32[]{:S(2)}) collective-permute-start(bf16[768,1024]{1,0:T(8,128)(2,1)S(1)} %bitcast.306), channel_id=1, source_target_pairs={{0,1},{1,0},{2,3},{3,2},{4,5},{5,4},{6,7},{7,6},{8,9},{9,8},{10,11... | collective-permute-start | bytes 4718600 | tf_op jit(solution)/shard_map/ppermute | solution.py:277
  67.1 1.6 copy-start.13
  73.1 4.1 %copy-start.16 = (bf16[768,128]{1,0:T(8,128)(2,1)}, bf16[768,128]{1,0:T(8,128)(2,1)S(1)}, u32[]{:S(2)}) copy-start(bf16[768,128]{1,0:T(8,128)(2,1)S(1)} %get-tuple-element.39) | copy-start | bytes 589828
  73.1 17.1 %copy-start.14 = (bf16[768,128]{1,0:T(8,128)(2,1)}, bf16[768,128]{1,0:T(8,128)(2,1)S(1)}, u32[]{:S(2)}) copy-start(bf16[768,128]{1,0:T(8,128)(2,1)S(1)} %get-tuple-element.38) | copy-start | bytes 589828
  73.1 3.2 %copy-start.40 = (f32[128]{0:T(128)S(1)}, f32[128]{0:T(128)}, u32[]{:S(2)}) copy-start(f32[128]{0:T(128)} %get-tuple-element.70) | copy-start | bytes 1540
  73.1 3.8 %copy-start.11 = (bf16[128,256]{1,0:T(8,128)(2,1)S(1)}, bf16[128,256]{1,0:T(8,128)(2,1)}, u32[]{:S(2)}) copy-start(bf16[128,256]{1,0:T(8,128)(2,1)} %param.27) | copy-start | bytes 196612
  73.1 4.0 %copy-start.5 = (f32[128,128]{1,0:T(8,128)S(1)}, f32[128,128]{1,0:T(8,128)}, u32[]{:S(2)}) copy-start(f32[128,128]{1,0:T(8,128)} %copy.79) | copy-start | bytes 196612
  73.9 7.1 %collective-permute-start.1 = (bf16[384,1024]{1,0:T(8,128)(2,1)S(1)}, bf16[384,1024]{1,0:T(8,128)(2,1)S(1)}, u32[]{:S(2)}, u32[]{:S(2)}) collective-permute-start(bf16[384,1024]{1,0:T(8,128)(2,1)S(1)} %convolution_convert_fusion.1), channel_id=1, source_target_pairs={{0,1},{1,0},{2,3},{3,2},{4,5},{5,4},{6,7},{7,6},{8,9},{9,8},{10,11... | collective-permute-start | bytes 2359304 | tf_op jit(solution)/shard_map/ppermute | solution.py:320
  81.4 8.6 %copy-start.9 = (f32[64,128]{0,1:T(8,128)S(1)}, f32[64,128]{0,1:T(8,128)}, u32[]{:S(2)}) copy-start(f32[64,128]{0,1:T(8,128)} %copy-done.8) | copy-start | bytes 98308
  82.5 29.4 %all-to-all-start.1 = ((bf16[8,384,128]{2,1,0:T(8,128)(2,1)}), bf16[8,384,128]{2,1,0:T(8,128)(2,1)S(1)}, u32[]{:S(2)}, u32[]{:S(2)}) async-start(bf16[8,384,128]{2,1,0:T(8,128)(2,1)} %bitcast.295), calls=%async_computation.1 | async-start | bytes 1572864 | tf_op jit(solution)/shard_map/all_to_all | solution.py:323
  90.9 2.1 copy-start.15
  90.9 2.2 copy-start.17
  112.7 21.8 %all-to-all-start.2 = ((bf16[32,16,128]{2,1,0:T(8,128)(2,1)}), bf16[32,16,128]{2,1,0:T(8,128)(2,1)S(1)}, u32[]{:S(2)}, u32[]{:S(2)}) async-start(bf16[32,16,128]{2,1,0:T(8,128)(2,1)} %pad_maximum_fusion.2), calls=%async_computation.2 | async-start | bytes 262144 | tf_op jit(solution)/shard_map/all_to_all | solution.py:358
  117.9 16.7 %copy-start.43 = (s32[128]{0:T(128)S(1)}, s32[128]{0:T(128)}, u32[]{:S(2)}) copy-start(s32[128]{0:T(128)} %get-tuple-element.82) | copy-start | bytes 1540
  117.9 16.7 %copy-start.44 = (s32[128]{0:T(128)S(1)}, s32[128]{0:T(128)}, u32[]{:S(2)}) copy-start(s32[128]{0:T(128)} %get-tuple-element.83) | copy-start | bytes 1540
  119.8 42.2 %collective-permute-start.7 = (bf16[256,256]{1,0:T(8,128)(2,1)}, bf16[256,256]{1,0:T(8,128)(2,1)S(1)}, u32[]{:S(2)}, u32[]{:S(2)}) collective-permute-start(bf16[256,256]{1,0:T(8,128)(2,1)} %all_gather.7.refs_0_), channel_id=1, source_target_pairs={{0,384},{64,448},{128,0},{192,64},{256,128},{320,192},{384,256},{4... | collective-permute-start | bytes 393224 | tf_op jit(solution)/shard_map/ppermute | solution.py:330
  125.6 36.4 %collective-permute-start.6 = (bf16[256,256]{1,0:T(8,128)(2,1)}, bf16[256,256]{1,0:T(8,128)(2,1)S(1)}, u32[]{:S(2)}, u32[]{:S(2)}) collective-permute-start(bf16[256,256]{1,0:T(8,128)(2,1)} %all_gather.7.refs_0_), channel_id=1, source_target_pairs={{0,320},{64,384},{128,448},{192,0},{256,64},{320,128},{384,192},{4... | collective-permute-start | bytes 393224 | tf_op jit(solution)/shard_map/ppermute | solution.py:330
  129.9 32.2 %collective-permute-start.5 = (bf16[256,256]{1,0:T(8,128)(2,1)}, bf16[256,256]{1,0:T(8,128)(2,1)S(1)}, u32[]{:S(2)}, u32[]{:S(2)}) collective-permute-start(bf16[256,256]{1,0:T(8,128)(2,1)} %all_gather.7.refs_0_), channel_id=1, source_target_pairs={{0,256},{64,320},{128,384},{192,448},{256,0},{320,64},{384,128},{4... | collective-permute-start | bytes 393224 | tf_op jit(solution)/shard_map/ppermute | solution.py:330
  153.4 17.4 %collective-permute-start.4 = (bf16[256,256]{1,0:T(8,128)(2,1)}, bf16[256,256]{1,0:T(8,128)(2,1)S(1)}, u32[]{:S(2)}, u32[]{:S(2)}) collective-permute-start(bf16[256,256]{1,0:T(8,128)(2,1)} %all_gather.7.refs_0_), channel_id=1, source_target_pairs={{0,192},{64,256},{128,320},{192,384},{256,448},{320,0},{384,64},{4... | collective-permute-start | bytes 393224 | tf_op jit(solution)/shard_map/ppermute | solution.py:330
  156.4 14.4 %collective-permute-start.3 = (bf16[256,256]{1,0:T(8,128)(2,1)}, bf16[256,256]{1,0:T(8,128)(2,1)S(1)}, u32[]{:S(2)}, u32[]{:S(2)}) collective-permute-start(bf16[256,256]{1,0:T(8,128)(2,1)} %all_gather.7.refs_0_), channel_id=1, source_target_pairs={{0,128},{64,192},{128,256},{192,320},{256,384},{320,448},{384,0},{... | collective-permute-start | bytes 393224 | tf_op jit(solution)/shard_map/ppermute | solution.py:330
  162.0 8.8 %copy-start.18 = (bf16[256,256]{1,0:T(8,128)(2,1)}, bf16[256,256]{1,0:T(8,128)(2,1)S(1)}, u32[]{:S(2)}) copy-start(bf16[256,256]{1,0:T(8,128)(2,1)S(1)} %collective-permute-done.7.refs_6_) | copy-start | bytes 393220
  162.0 8.8 %copy-start.19 = (bf16[256,256]{1,0:T(8,128)(2,1)}, bf16[256,256]{1,0:T(8,128)(2,1)S(1)}, u32[]{:S(2)}) copy-start(bf16[256,256]{1,0:T(8,128)(2,1)S(1)} %collective-permute-done.6.refs_5_) | copy-start | bytes 393220
  162.0 8.8 %copy-start.20 = (bf16[256,256]{1,0:T(8,128)(2,1)}, bf16[256,256]{1,0:T(8,128)(2,1)S(1)}, u32[]{:S(2)}) copy-start(bf16[256,256]{1,0:T(8,128)(2,1)S(1)} %collective-permute-done.5.refs_4_) | copy-start | bytes 393220
  170.8 0.7 copy-start.21
  170.8 0.7 copy-start.22
  175.0 19.5 %copy-start.4 = (bf16[128,256]{1,0:T(8,128)(2,1)S(1)}, bf16[128,256]{1,0:T(8,128)(2,1)}, u32[]{:S(2)}) copy-start(bf16[128,256]{1,0:T(8,128)(2,1)} %get-tuple-element.24) | copy-start | bytes 196612
  176.6 32.6 %copy-start.3 = (f32[1,1,128,256]{3,2,1,0:T(8,128)S(1)}, f32[1,1,128,256]{3,2,1,0:T(8,128)}, u32[]{:S(2)}) copy-start(f32[1,1,128,256]{3,2,1,0:T(8,128)} %param.29) | copy-start | bytes 393220
  176.6 18.0 %collective-permute-start.9 = (bf16[8,64,256]{2,1,0:T(8,128)(2,1)S(1)}, bf16[8,64,256]{2,1,0:T(8,128)(2,1)S(1)}, u32[]{:S(2)}, u32[]{:S(2)}) collective-permute-start(bf16[8,64,256]{2,1,0:T(8,128)(2,1)S(1)} %get-tuple-element.46), channel_id=1, source_target_pairs={{0,16},{16,32},{32,48},{48,0},{1,17},{17,33},{33,49},{49,1},{2,18}... | collective-permute-start | bytes 786440 | tf_op jit(solution)/shard_map/ppermute | solution.py:412
  180.3 14.5 %collective-permute-start.11 = (bf16[8,64,256]{2,1,0:T(8,128)(2,1)S(1)}, bf16[8,64,256]{2,1,0:T(8,128)(2,1)S(1)}, u32[]{:S(2)}, u32[]{:S(2)}) collective-permute-start(bf16[8,64,256]{2,1,0:T(8,128)(2,1)S(1)} %get-tuple-element.47), channel_id=1, source_target_pairs={{0,48},{16,0},{32,16},{48,32},{1,49},{17,1},{33,17},{49,33},{2,50}... | collective-permute-start | bytes 786440 | tf_op jit(solution)/shard_map/ppermute | solution.py:412
  183.8 11.0 %collective-permute-start.10 = (bf16[8,64,256]{2,1,0:T(8,128)(2,1)S(1)}, bf16[8,64,256]{2,1,0:T(8,128)(2,1)}, u32[]{:S(2)}, u32[]{:S(2)}) collective-permute-start(bf16[8,64,256]{2,1,0:T(8,128)(2,1)S(1)} %get-tuple-element.48), channel_id=1, source_target_pairs={{0,32},{16,48},{32,0},{48,16},{1,33},{17,49},{33,1},{49,17},{2,34}... | collective-permute-start | bytes 786440 | tf_op jit(solution)/shard_map/ppermute | solution.py:412
  191.1 10.1 %all-to-all-start.4 = ((bf16[4,128,256]{2,1,0:T(8,128)(2,1)}), bf16[4,128,256]{2,1,0:T(8,128)(2,1)S(1)}, u32[]{:S(2)}, u32[]{:S(2)}) async-start(bf16[4,128,256]{2,1,0:T(8,128)(2,1)} %get-tuple-element.25), calls=%async_computation.4 | async-start | bytes 524288 | tf_op jit(solution)/shard_map/all_to_all | solution.py:397
  194.7 14.6 %copy-start.36 = (f32[128]{0:T(128)S(1)}, f32[128]{0:T(128)}, u32[]{:S(2)}) copy-start(f32[128]{0:T(128)} %get-tuple-element.93) | copy-start | bytes 1540
  194.7 14.6 %copy-start.37 = (f32[128]{0:T(128)S(1)}, f32[128]{0:T(128)}, u32[]{:S(2)}) copy-start(f32[128]{0:T(128)} %get-tuple-element.26) | copy-start | bytes 1540
  194.7 14.6 %copy-start.38 = (f32[128]{0:T(128)S(1)}, f32[128]{0:T(128)}, u32[]{:S(2)}) copy-start(f32[128]{0:T(128)} %get-tuple-element.27) | copy-start | bytes 1540
  194.7 14.6 %copy-start.42 = (f32[128]{0:T(128)S(1)}, f32[128]{0:T(128)}, u32[]{:S(2)}) copy-start(f32[128]{0:T(128)} %slice_bitcast_fusion.2) | copy-start | bytes 1540
  196.6 27.4 %copy-start.41 = (f32[128]{0:T(128)S(1)}, f32[128]{0:T(128)}, u32[]{:S(2)}) copy-start(f32[128]{0:T(128)} %get-tuple-element.35) | copy-start | bytes 1540
  196.6 27.5 %copy-start.7 = (f32[1,64,128]{1,2,0:T(8,128)S(1)}, f32[1,64,128]{1,2,0:T(8,128)}, u32[]{:S(2)}) copy-start(f32[1,64,128]{1,2,0:T(8,128)} %copy-done.6) | copy-start | bytes 98308
  196.6 27.5 %copy-start.10 = (f32[128,128]{0,1:T(8,128)S(1)}, f32[128,128]{0,1:T(8,128)}, u32[]{:S(2)}) copy-start(f32[128,128]{0,1:T(8,128)} %get-tuple-element.76) | copy-start | bytes 196612
  201.1 18.6 %all-to-all-start.3 = ((bf16[8,64,256]{2,1,0:T(8,128)(2,1)}), bf16[8,64,256]{2,1,0:T(8,128)(2,1)S(1)}, u32[]{:S(2)}, u32[]{:S(2)}) async-start(bf16[8,64,256]{2,1,0:T(8,128)(2,1)} %fusion.40), calls=%async_computation.3 | async-start | bytes 524288 | tf_op jit(solution)/shard_map/all_to_all | solution.py:417
  220.5 17.5 %all-to-all-start.5 = ((bf16[8,128,256]{2,1,0:T(8,128)(2,1)}), bf16[8,128,256]{2,1,0:T(8,128)(2,1)S(1)}, u32[]{:S(2)}, u32[]{:S(2)}) async-start(bf16[8,128,256]{2,1,0:T(8,128)(2,1)} %broadcast_in_dim.121), calls=%async_computation.5 | async-start | bytes 1048576 | tf_op jit(solution)/shard_map/all_to_all | solution.py:44
  226.3 11.7 %copy-start.27 = (f32[128]{0:T(128)S(1)}, f32[128]{0:T(128)}, u32[]{:S(2)}) copy-start(f32[128]{0:T(128)} %get-tuple-element.86) | copy-start | bytes 1540
  226.3 11.7 %copy-start.28 = (f32[128]{0:T(128)S(1)}, f32[128]{0:T(128)}, u32[]{:S(2)}) copy-start(f32[128]{0:T(128)} %get-tuple-element.87) | copy-start | bytes 1540
  226.4 11.7 %copy-start.29 = (f32[128]{0:T(128)S(1)}, f32[128]{0:T(128)}, u32[]{:S(2)}) copy-start(f32[128]{0:T(128)} %get-tuple-element.88) | copy-start | bytes 1540
  226.4 11.7 %copy-start.30 = (f32[128]{0:T(128)S(1)}, f32[128]{0:T(128)}, u32[]{:S(2)}) copy-start(f32[128]{0:T(128)} %get-tuple-element.28) | copy-start | bytes 1540
  226.4 11.7 %copy-start.31 = (f32[128]{0:T(128)S(1)}, f32[128]{0:T(128)}, u32[]{:S(2)}) copy-start(f32[128]{0:T(128)} %get-tuple-element.30) | copy-start | bytes 1540
  226.4 11.7 %copy-start.32 = (f32[128]{0:T(128)S(1)}, f32[128]{0:T(128)}, u32[]{:S(2)}) copy-start(f32[128]{0:T(128)} %get-tuple-element.32) | copy-start | bytes 1540
  226.4 11.7 %copy-start.33 = (f32[128]{0:T(128)S(1)}, f32[128]{0:T(128)}, u32[]{:S(2)}) copy-start(f32[128]{0:T(128)} %get-tuple-element.78) | copy-start | bytes 1540
  226.4 11.7 %copy-start.34 = (f32[128]{0:T(128)S(1)}, f32[128]{0:T(128)}, u32[]{:S(2)}) copy-start(f32[128]{0:T(128)} %get-tuple-element.34) | copy-start | bytes 1540
  226.4 11.7 %copy-start.35 = (f32[128]{0:T(128)S(1)}, f32[128]{0:T(128)}, u32[]{:S(2)}) copy-start(f32[128]{0:T(128)} %get-tuple-element.79) | copy-start | bytes 1540
  226.4 12.0 %copy-start.26 = (f32[2,128]{1,0:T(2,128)S(1)}, f32[2,128]{1,0:T(2,128)}, u32[]{:S(2)}) copy-start(f32[2,128]{1,0:T(2,128)} %subtract_exponential_fusion.1) | copy-start | bytes 3076
  238.1 2.6 %copy-start.39 = (f32[128]{0:T(128)S(1)}, f32[128]{0:T(128)}, u32[]{:S(2)}) copy-start(f32[128]{0:T(128)} %get-tuple-element.65) | copy-start | bytes 1540
